TPU v7x, 512 devices: a whole 4x8x8 slice. The times are simulated.
512 devices in a mesh: sp: 64 (over z, y), tp: 8 (over x, core).
Axes of the slice: x: 4, y: 8, z: 8, core: 2. Of those that a mesh axis runs over, the one named last changes fastest.
Arguments:
- queries: bfloat16 [32768, 2048], P('sp', 'tp'), may hold values from -6 to 6
- key_rows: bfloat16 [32768, 512], P('sp', 'tp'), may hold values from -6 to 6
- values: bfloat16 [32768, 512], P('sp', 'tp'), may hold values from -6 to 6
- sink_logit: float32 [32], P('tp'), may hold values from 4 to 10
- residual_in: bfloat16 [32768, 2048], P(('sp', 'tp')), may hold values from -6 to 6
- out_weight: bfloat16 [2048, 2048], P('tp'), may hold values from -0.125 to 0.125
- norm_gain: float32 [2048], replicated, may hold values from 0.1 to 1.9
- gate_weight: bfloat16 [2048, 5632], P('sp', 'tp'), may hold values from -0.125 to 0.125
- up_weight: bfloat16 [2048, 5632], P('sp', 'tp'), may hold values from -0.125 to 0.125
- down_weight: bfloat16 [5632, 2048], P('tp', 'sp'), may hold values from -0.078125 to 0.078125
Outputs:
- layer_out: bfloat16 [32768, 2048], P(('sp', 'tp'))
All inputs are finite; a program needn't handle non-finite values.
Results may differ from a plain program's by a relative error of at most 0.013.
Values may be sent and summed in bfloat16 or wider, within the bound.
No kernel may reach another device: no remote copies, remote signals or barrier semaphores. Data moves between devices by JAX's collectives and lax.ppermute only.
A program may use at most 64 MiB of HBM per device.

v0:
```python
import jax
import jax.numpy as jnp
from jax import lax
from jax.sharding import PartitionSpec as P

HEAD_DIM = 64
WINDOW = 128


def rows_first(arrays, axis, dims):
    turned = [jnp.moveaxis(a, dim, 0) for a, dim in zip(arrays, dims)]
    both = jnp.concatenate([t.reshape(len(t), -1) for t in turned], axis=1)
    filled, at, gathered = (lax.all_gather(both, axis, axis=0, tiled=True), 0, [])
    for t, dim in zip(turned, dims):
        section = filled[:, at : at + t[0].size].reshape(-1, *t.shape[1:])
        gathered.append(jnp.moveaxis(section, 0, dim))
        at += t[0].size
    return tuple(gathered)


def with_halo(block, sides, width):
    for axis, dim in sides:
        count = lax.axis_size(axis)
        forward = [(i, i + 1) for i in range(count - 1)]
        backward = [(target, source) for source, target in forward]
        low = lax.ppermute(
            lax.slice_in_dim(block, block.shape[dim] - width, None, axis=dim), axis, forward
        )
        high = lax.ppermute(lax.slice_in_dim(block, 0, width, axis=dim), axis, backward)
        block = jnp.concatenate([low, block, high], axis=dim)
    return block


def in_blocks(array, dim, length):
    shape = array.shape
    pieces = array.reshape(*shape[:dim], length, shape[dim] // length, *shape[dim + 1 :])
    return jnp.moveaxis(pieces, dim, 0)


def sent_and_summed(array, axis, dim):
    length = lax.axis_size(axis)
    pieces = lax.all_to_all(in_blocks(array, dim, length), axis, 0, 0, tiled=True)
    return jnp.sum(pieces.astype(jnp.float32), axis=0)


def in_order(pieces, dim):
    pieces = jnp.moveaxis(pieces, 0, dim)
    shape = pieces.shape
    return pieces.reshape(*shape[:dim], shape[dim] * shape[dim + 1], *shape[dim + 2 :])


def from_everyone(array, axis):
    length = lax.axis_size(axis)
    return lax.all_to_all(
        jnp.broadcast_to(array[None], (length, *array.shape)), axis, 0, 0, tiled=True
    )


def gather_directly(array, axis, dim):
    return in_order(from_everyone(array, axis), dim)


def rms_scale(mixed_rows, norm_gain):
    inverse = lax.rsqrt(jnp.mean(mixed_rows * mixed_rows, axis=-1, keepdims=True) + 1e-06)
    return (mixed_rows * inverse * norm_gain).astype(jnp.bfloat16)


def attend_window(queries, padded, offset, total_rows, sink_logit):
    rows_here = queries.shape[0]
    block_count = rows_here // WINDOW
    heads_here = queries.shape[1] // HEAD_DIM
    kv_here = padded.shape[1] // (2 * HEAD_DIM)
    group_size = heads_here // kv_here
    blocks = padded.reshape(block_count + 2, WINDOW, padded.shape[1])
    banded = jnp.concatenate([blocks[:-2], blocks[1:-1], blocks[2:]], axis=1)
    key_band = banded[:, :, : kv_here * HEAD_DIM].reshape(
        block_count, 3 * WINDOW, kv_here, HEAD_DIM
    )
    value_band = banded[:, :, kv_here * HEAD_DIM :].reshape(
        block_count, 3 * WINDOW, kv_here, HEAD_DIM
    )
    grouped = queries.reshape(block_count, WINDOW, kv_here, group_size, HEAD_DIM)
    scores = jnp.einsum(
        "nqkgd,nskd->nkgqs", grouped, key_band, preferred_element_type=jnp.float32
    ) * HEAD_DIM ** (-0.5)
    block_start = offset + jnp.arange(block_count, dtype=jnp.int32)[:, None] * WINDOW
    query_pos = block_start + jnp.arange(WINDOW, dtype=jnp.int32)[None, :]
    key_pos = block_start - WINDOW + jnp.arange(3 * WINDOW, dtype=jnp.int32)[None, :]
    valid = jnp.abs(query_pos[:, :, None] - key_pos[:, None, :]) <= WINDOW
    valid = valid & ((key_pos >= 0) & (key_pos < total_rows))[:, None, :]
    scores = jnp.where(valid[:, None, None], scores, -1e30)
    sink_grid = sink_logit.reshape(kv_here, group_size)[None, :, :, None, None]
    peak = jnp.maximum(jnp.max(scores, axis=-1, keepdims=True), sink_grid)
    weights_raw = jnp.exp(scores - peak)
    denom = jnp.sum(weights_raw, axis=-1, keepdims=True) + jnp.exp(sink_grid - peak)
    probs = (weights_raw / denom).astype(jnp.bfloat16)
    output = jnp.einsum("nkgqs,nskd->nqkgd", probs, value_band, preferred_element_type=jnp.float32)
    return output.astype(jnp.bfloat16).reshape(rows_here, heads_here * HEAD_DIM)


def shards(
    queries,
    key_rows,
    values,
    sink_logit,
    residual_in,
    out_weight,
    norm_gain,
    gate_weight,
    up_weight,
    down_weight,
):
    rows_here = queries.shape[0]
    gate_full, up_full, down_full = rows_first(
        (gate_weight, up_weight, down_weight), "sp", (0, 0, 1)
    )
    joined = jnp.concatenate([key_rows, values], axis=1)
    padded = with_halo(joined, (("sp", 0),), WINDOW)
    offset = lax.axis_index("sp") * rows_here
    attended = attend_window(queries, padded, offset, rows_here * lax.axis_size("sp"), sink_logit)
    picked = attended
    mixed_rows = residual_in.astype(jnp.float32) + sent_and_summed(
        jnp.dot(picked, out_weight, preferred_element_type=jnp.float32).astype(jnp.bfloat16),
        "tp",
        0,
    )
    normed = gather_directly(rms_scale(mixed_rows, norm_gain), "tp", 0)
    gate_pre = jnp.dot(normed, gate_full, preferred_element_type=jnp.float32)
    up_pre = jnp.dot(normed, up_full, preferred_element_type=jnp.float32)
    hidden = (jax.nn.silu(gate_pre) * up_pre).astype(jnp.bfloat16)
    picked = hidden
    result = mixed_rows + sent_and_summed(
        jnp.dot(picked, down_full, preferred_element_type=jnp.float32).astype(jnp.bfloat16), "tp", 0
    )
    return result.astype(jnp.bfloat16)


def solution(mesh):
    return jax.shard_map(
        shards,
        mesh=mesh,
        in_specs=(
            P("sp", "tp"),
            P("sp", "tp"),
            P("sp", "tp"),
            P("tp"),
            P(("sp", "tp"), None),
            P("tp", None),
            P(),
            P("sp", "tp"),
            P("sp", "tp"),
            P("tp", "sp"),
        ),
        out_specs=P(("sp", "tp"), None),
        check_vma=False,
    )
```

profile of v0, /device:TPU:1, one launch (start us, length us, event | category | flops | bytes accessed | tf_op | source)
XLA Modules:
  0.0 170.4 jit_solution(4183434306201593121)
XLA Ops:
  6.5 0.0 copy-start
  6.5 0.0 all-gather.2.cloned.1.call-start
  6.5 1.7 concatenate.20
  8.2 0.0 all-gather.2.cloned.1.call-update
  8.3 1.0 copy.13
  9.2 1.0 copy.14
  10.2 0.1 fusion.33
  10.3 4.0 %collective-permute-start = (bf16[128,128]{1,0:T(8,128)(2,1)S(1)}, bf16[128,128]{1,0:T(8,128)(2,1)S(1)}, u32[]{:S(2)}, u32[]{:S(2)}) collective-permute-start(bf16[128,128]{1,0:T(8,128)(2,1)S(1)} %get-tuple-element.8), channel_id=1, source_target_pairs={{0,8},{8,16},{16,24},{24,32},{32,40},{40,48},{48,56},{56,64},{64,7... | collective-permute-start | bytes 98312 | tf_op jit(solution)/shard_map/ppermute | solution.py:26
  14.3 1.3 collective-permute-start.1
  15.6 0.1 compare_and_fusion
  15.7 0.1 iota_add_fusion.1
  15.8 0.1 iota_add_fusion
  15.9 0.6 fusion.27
  16.4 1.2 reshape.152
  17.7 0.0 copy-start.3
  17.7 0.0 collective-permute-done
  17.7 1.3 collective-permute-done.1
  19.0 0.2 pad_maximum_fusion.3
  19.1 0.1 copy.15
  19.3 0.1 copy.17
  19.4 0.1 copy.16
  19.6 0.1 pad_maximum_fusion
  19.6 0.7 fusion.10
  20.3 0.0 copy-done.3
  20.3 0.1 broadcast_maximum_fusion
  20.4 0.7 fusion.9
  21.1 0.1 exponential_add_fusion
  21.2 1.0 fusion.24
  22.1 0.2 copy.21
  22.3 0.0 copy-done
  22.4 0.7 convolution_convert_fusion
  23.1 0.0 copy-start.1
  23.1 0.0 copy-start.2
  23.1 34.0 %all_to_all.15 = bf16[8,64,2048]{2,1,0:T(8,128)(2,1)S(1)} all-to-all(bf16[8,64,2048]{2,1,0:T(8,128)(2,1)S(1)} %bitcast.57), channel_id=1, replica_groups=mesh['sp'=64,'tp'=8] {'tp'}, dimensions={0} | all-to-all | bytes 4194304 | tf_op jit(solution)/shard_map/all_to_all | solution.py:42
  57.1 0.4 convert_reduce_fusion.1
  57.5 0.0 copy-done.1
  57.5 0.2 multiply_reduce_fusion
  57.7 0.0 copy-done.2
  57.7 0.1 multiply_convert_fusion
  57.8 0.2 broadcast_in_dim.16
  58.1 30.4 %all_to_all.16 = bf16[8,64,2048]{2,1,0:T(8,128)(2,1)} all-to-all(bf16[8,64,2048]{2,1,0:T(8,128)(2,1)S(1)} %broadcast_in_dim.16), channel_id=1, replica_groups=mesh['sp'=64,'tp'=8] {'tp'}, dimensions={0} | all-to-all | bytes 4194304 | tf_op jit(solution)/shard_map/all_to_all | solution.py:54
  88.5 28.8 %all-gather.2.cloned.1.call-done = bf16[2048,2112]{1,0:T(8,128)(2,1)} async-done(((bf16[32,2112]{1,0:T(8,128)(2,1)}), bf16[2048,2112]{1,0:T(8,128)(2,1)}) %all-gather.2.cloned.1.call-update) | async-done | bytes 8650768 | tf_op jit(solution)/shard_map/all_gather | solution.py:13
  117.3 4.2 %fusion.4 = f32[512,704]{0,1:T(8,128)S(1)} fusion(bf16[512,2048]{1,0:T(8,128)(2,1)} %bitcast.58, bf16[2048,2112]{1,0:T(8,128)(2,1)} %all-gather.2.cloned.1.call-done), kind=kOutput, calls=%fused_computation.6 | convolution fusion | flops 1476395008 | bytes 6684672 | tf_op jit(solution)/shard_map/dot_general | solution.py:128
  121.5 9.7 %fusion.6 = bf16[512,2048]{1,0:T(8,128)(2,1)} fusion(bf16[2048,2112]{1,0:T(8,128)(2,1)} %all-gather.2.cloned.1.call-done, bf16[512,2048]{1,0:T(8,128)(2,1)} %bitcast.59, f32[512,704]{0,1:T(8,128)S(1)} %fusion.4), kind=kOutput, calls=%fused_computation.12 | convolution fusion | flops 2956001280 | bytes 11927552 | tf_op jit(solution)/shard_map/dot_general | solution.py:133
  131.1 31.3 %all_to_all.17 = bf16[8,64,2048]{2,1,0:T(8,128)(2,1)S(1)} all-to-all(bf16[8,64,2048]{2,1,0:T(8,128)(2,1)} %bitcast.60), channel_id=1, replica_groups=mesh['sp'=64,'tp'=8] {'tp'}, dimensions={0} | all-to-all | bytes 4194304 | tf_op jit(solution)/shard_map/all_to_all | solution.py:42
  162.4 0.4 convert_reduce_fusion
  162.8 0.8 add_convert_fusion
  (2 shorter events, 0.0 us)
Async XLA Ops:
  6.5 15.8 %copy-start = (bf16[256,2048]{1,0:T(8,128)(2,1)S(1)}, bf16[256,2048]{1,0:T(8,128)(2,1)}, u32[]{:S(2)}) copy-start(bf16[256,2048]{1,0:T(8,128)(2,1)} %param.15) | copy-start | bytes 3145732
  6.5 110.7 %all-gather.2.cloned.1.call-start = ((), (), s32[]{:S(2)}) async-start(), calls=%async_computation.3 | async-start | bytes 9052160 | tf_op jit(solution)/shard_map/all_gather | solution.py:13
  10.3 7.4 %collective-permute-start = (bf16[128,128]{1,0:T(8,128)(2,1)S(1)}, bf16[128,128]{1,0:T(8,128)(2,1)S(1)}, u32[]{:S(2)}, u32[]{:S(2)}) collective-permute-start(bf16[128,128]{1,0:T(8,128)(2,1)S(1)} %get-tuple-element.8), channel_id=1, source_target_pairs={{0,8},{8,16},{16,24},{24,32},{32,40},{40,48},{48,56},{56,64},{64,7... | collective-permute-start | bytes 98312 | tf_op jit(solution)/shard_map/ppermute | solution.py:26
  14.3 4.7 %collective-permute-start.1 = (bf16[128,128]{1,0:T(8,128)(2,1)S(1)}, bf16[128,128]{1,0:T(8,128)(2,1)S(1)}, u32[]{:S(2)}, u32[]{:S(2)}) collective-permute-start(bf16[128,128]{1,0:T(8,128)(2,1)S(1)} %get-tuple-element.9), channel_id=1, source_target_pairs={{8,0},{16,8},{24,16},{32,24},{40,32},{48,40},{56,48},{64,56},{72,6... | collective-permute-start | bytes 98312 | tf_op jit(solution)/shard_map/ppermute | solution.py:29
  17.7 2.6 %copy-start.3 = (f32[4]{0:T(128)S(1)}, f32[4]{0:T(128)}, u32[]{:S(2)}) copy-start(f32[4]{0:T(128)} %param.13) | copy-start | bytes 52
  23.1 34.4 %copy-start.1 = (bf16[64,2048]{1,0:T(8,128)(2,1)S(1)}, bf16[64,2048]{1,0:T(8,128)(2,1)}, u32[]{:S(2)}) copy-start(bf16[64,2048]{1,0:T(8,128)(2,1)} %param.14) | copy-start | bytes 786436
  23.1 34.6 %copy-start.2 = (f32[2048]{0:T(1024)S(1)}, f32[2048]{0:T(1024)}, u32[]{:S(2)}) copy-start(f32[2048]{0:T(1024)} %param.16) | copy-start | bytes 24580
Sparse Core Ops, SparseCore 0:
  10.3 106.8 all-gather.1
where the time goes:
time: 171 us; the launch traced here: 170 us
  blocking collectives  95.7 us (56%)
  waiting for transfers between devices  30.1 us (18%)
  matrix products  16.3 us (10%)
  between operations  13.6 us (8%)
  local copies, waits for them, and re-layouts  5.72 us (3%)
  starting transfers between devices  5.31 us (3%)
  other arithmetic  3.74 us (2%)
    all_to_all x2, blocking collectives, sent_and_summed(): lax.all_to_all(in_blocks(array, dim, length), axis, 0, 0, tiled=True)  65.3 us
    all_to_all x1, blocking collectives, from_everyone(): lax.all_to_all(jnp.broadcast_to(array[None], (length, *array.shape)), axi...  30.4 us
    all_gather x1, waiting for transfers between devices, rows_first(): lax.all_gather(both, axis, axis=0, tiled=True)  28.8 us
    dot_general x1, matrix products, shards(): jnp.dot(picked, down_full, preferred_element_type=jnp.float32)  9.66 us
    dot_general x1, matrix products, shards(): gate_pre = jnp.dot(normed, gate_full, preferred_element_type=jnp.float32)  4.21 us
    ppermute x1, starting transfers between devices, with_halo(): lax.ppermute(lax.slice_in_dim(block, block.shape[dim] - width, None, axis...  4.02 us
  transfers between devices with their start and end apart: 3, of which 2 were waited for; matrix products, arithmetic and copies ran while one was open for 5% of the time, Pallas kernels for 0%

commit v1 on v0

v1 whole, which is shorter than its diff:
```python
import functools

import jax
import jax.numpy as jnp
from jax import lax
from jax.experimental import pallas as pl
from jax.experimental.pallas import tpu as pltpu
from jax.sharding import PartitionSpec as P

HEAD_DIM = 64
WINDOW = 128
SIDE = 8
CORES = 2
LANES = 128


def device_index(sp, tp, tps):
    return sp * tps + tp


def line_groups(sps, tps, first):
    groups = []
    for tp in range(tps):
        along_y = (tp % CORES == 0) == first
        for fixed in range(sps // SIDE):
            line = [fixed * SIDE + k if along_y else k * SIDE + fixed for k in range(SIDE)]
            groups.append([device_index(sp, tp, tps) for sp in line])
    return groups


def x_groups(tps):
    return [[x * CORES + core for x in range(tps // CORES)] for core in range(CORES)]


def core_swap(tps):
    return [(i, i ^ 1) for i in range(tps)]


def ffn_kernel(core_ref, rows_ref, weights_ref, out_ref, held, hidden, sems, *, hid):
    full = hid // LANES
    rest = hid - full * LANES
    gated = 2 * hid
    parts = [(2 * LANES * j, 2 * LANES) for j in range(full)] + [(2 * LANES * full, 2 * rest)]
    parts.append((gated, hid))
    core = core_ref[0]

    def copies(part, swapped):
        at, size = parts[part]
        return [
            pltpu.make_async_copy(
                weights_ref.at[:, i, :, pl.ds(at, size)]
                if swapped
                else weights_ref.at[i, :, :, pl.ds(at, size)],
                held.at[i, :, :, pl.ds(at, size)],
                sems.at[part],
            )
            for i in range(SIDE)
        ]

    for swapped in (False, True):

        @pl.when(core == int(swapped))
        def _():
            for part in range(len(parts)):
                for copy in copies(part, swapped):
                    copy.start()

    depth = rows_ref.shape[1]
    for part in range(full + 1):
        at, size = parts[part]
        for copy in copies(part, False):
            copy.wait()
        tile = held[:, :, :, at : at + size].reshape(depth, size)
        both = jnp.dot(rows_ref[...], tile, preferred_element_type=jnp.float32)
        gate, up = both[:, : size // 2], both[:, size // 2 :]
        hidden[:, at // 2 : at // 2 + size // 2] = (gate / (1.0 + jnp.exp(-gate)) * up).astype(
            hidden.dtype
        )
    for copy in copies(full + 1, False):
        copy.wait()
    for i in range(SIDE):
        tile = held[i, :, :, gated : gated + hid].reshape(-1, hid)
        width = tile.shape[0]
        out_ref[:, i * width : (i + 1) * width] = lax.dot_general(
            hidden[...], tile, (((1,), (1,)), ((), ())), preferred_element_type=jnp.float32
        ).astype(out_ref.dtype)


def feed_forward(rows, weights, core, out_dtype):
    count, depth = rows.shape
    piece, width = weights.shape[2:]
    hid = width // 3
    parts = hid // LANES + 2
    return pl.pallas_call(
        functools.partial(ffn_kernel, hid=hid),
        out_shape=jax.ShapeDtypeStruct((count, depth), out_dtype),
        in_specs=[
            pl.BlockSpec(memory_space=pltpu.SMEM),
            pl.BlockSpec(memory_space=pltpu.VMEM),
            pl.BlockSpec(memory_space=pl.ANY),
        ],
        out_specs=pl.BlockSpec(memory_space=pltpu.VMEM),
        scratch_shapes=[
            pltpu.VMEM((SIDE, SIDE, piece, width), jnp.bfloat16),
            pltpu.VMEM((count, hid), jnp.bfloat16),
            pltpu.SemaphoreType.DMA((parts,)),
        ],
        cost_estimate=pl.CostEstimate(
            flops=2 * count * depth * width,
            bytes_accessed=2 * weights.size + 4 * rows.size,
            transcendentals=count * hid,
        ),
        compiler_params=pltpu.CompilerParams(vmem_limit_bytes=40 * 1024 * 1024),
        name="ffn",
    )(core, rows, weights)


def with_halo(block, axis, width):
    count = lax.axis_size(axis)
    forward = [(i, i + 1) for i in range(count - 1)]
    backward = [(target, source) for source, target in forward]
    low = lax.ppermute(block[-width:], axis, forward)
    high = lax.ppermute(block[:width], axis, backward)
    return jnp.concatenate([low, block, high], axis=0)


def attend_window(queries, padded, offset, total_rows, sink_logit):
    rows_here = queries.shape[0]
    block_count = rows_here // WINDOW
    heads_here = queries.shape[1] // HEAD_DIM
    kv_here = padded.shape[1] // (2 * HEAD_DIM)
    group_size = heads_here // kv_here
    blocks = padded.reshape(block_count + 2, WINDOW, padded.shape[1])
    banded = jnp.concatenate([blocks[:-2], blocks[1:-1], blocks[2:]], axis=1)
    key_band = banded[:, :, : kv_here * HEAD_DIM].reshape(
        block_count, 3 * WINDOW, kv_here, HEAD_DIM
    )
    value_band = banded[:, :, kv_here * HEAD_DIM :].reshape(
        block_count, 3 * WINDOW, kv_here, HEAD_DIM
    )
    grouped = queries.reshape(block_count, WINDOW, kv_here, group_size, HEAD_DIM)
    scores = jnp.einsum(
        "nqkgd,nskd->nkgqs", grouped, key_band, preferred_element_type=jnp.float32
    ) * HEAD_DIM ** (-0.5)
    block_start = offset + jnp.arange(block_count, dtype=jnp.int32)[:, None] * WINDOW
    query_pos = block_start + jnp.arange(WINDOW, dtype=jnp.int32)[None, :]
    key_pos = block_start - WINDOW + jnp.arange(3 * WINDOW, dtype=jnp.int32)[None, :]
    valid = jnp.abs(query_pos[:, :, None] - key_pos[:, None, :]) <= WINDOW
    valid = valid & ((key_pos >= 0) & (key_pos < total_rows))[:, None, :]
    scores = jnp.where(valid[:, None, None], scores, -1e30)
    sink_grid = sink_logit.reshape(kv_here, group_size)[None, :, :, None, None]
    peak = jnp.maximum(jnp.max(scores, axis=-1, keepdims=True), sink_grid)
    weights_raw = jnp.exp(scores - peak)
    denom = jnp.sum(weights_raw, axis=-1, keepdims=True) + jnp.exp(sink_grid - peak)
    probs = (weights_raw / denom).astype(jnp.bfloat16)
    output = jnp.einsum("nkgqs,nskd->nqkgd", probs, value_band, preferred_element_type=jnp.float32)
    return output.astype(jnp.bfloat16).reshape(rows_here, heads_here * HEAD_DIM)


def rms_scale(mixed_rows, norm_gain):
    inverse = lax.rsqrt(jnp.mean(mixed_rows * mixed_rows, axis=-1, keepdims=True) + 1e-06)
    return (mixed_rows * inverse * norm_gain).astype(jnp.bfloat16)


def joined_weights(gate_weight, up_weight, down_weight):
    hid = gate_weight.shape[1]
    pieces = []
    for at in range(0, hid, LANES):
        pieces += [gate_weight[:, at : at + LANES], up_weight[:, at : at + LANES]]
    return jnp.concatenate(pieces + [down_weight.T], axis=1)


def shards(
    queries,
    key_rows,
    values,
    sink_logit,
    residual_in,
    out_weight,
    norm_gain,
    gate_weight,
    up_weight,
    down_weight,
):
    rows_here, depth = queries.shape[0], residual_in.shape[1]
    sps, tps = lax.axis_size("sp"), lax.axis_size("tp")
    xs = tps // CORES
    own = rows_here // tps
    core = lax.axis_index("tp") % CORES
    both_axes = ("sp", "tp")

    mine = joined_weights(gate_weight, up_weight, down_weight)
    line = lax.all_to_all(
        jnp.broadcast_to(mine[None], (SIDE, *mine.shape)),
        both_axes,
        0,
        0,
        tiled=True,
        axis_index_groups=line_groups(sps, tps, True),
    )
    line, queries, key_rows, values = lax.optimization_barrier((line, queries, key_rows, values))
    weights = lax.all_gather(
        line, both_axes, axis=0, tiled=False, axis_index_groups=line_groups(sps, tps, False)
    )

    joined = jnp.concatenate([key_rows, values], axis=1)
    padded = with_halo(joined, "sp", WINDOW)
    offset = lax.axis_index("sp") * rows_here
    attended = attend_window(queries, padded, offset, rows_here * sps, sink_logit)

    by_core = attended.reshape(xs, CORES, own, attended.shape[1])
    even, odd = by_core[:, 0], by_core[:, 1]
    for_me = jnp.where(core == 0, even, odd).reshape(xs * own, -1)
    for_mate = jnp.where(core == 0, odd, even).reshape(xs * own, -1)

    def swap(array):
        return lax.ppermute(array, "tp", core_swap(tps))

    def summed(partial):
        pieces = lax.all_to_all(
            partial.reshape(xs, own, depth), "tp", 0, 0, tiled=True, axis_index_groups=x_groups(tps)
        )
        return jnp.sum(pieces.astype(jnp.float32), axis=0)

    mate_part = swap(
        jnp.dot(for_mate, out_weight, preferred_element_type=jnp.float32).astype(jnp.bfloat16)
    )
    my_part = jnp.dot(for_me, out_weight, preferred_element_type=jnp.float32)
    attn_sum = summed((my_part + mate_part.astype(jnp.float32)).astype(jnp.bfloat16))
    mixed_rows = residual_in.astype(jnp.float32) + attn_sum

    normed = rms_scale(mixed_rows, norm_gain)
    my_rows = lax.all_to_all(
        jnp.broadcast_to(normed[None], (xs, own, depth)),
        "tp",
        0,
        0,
        tiled=True,
        axis_index_groups=x_groups(tps),
    ).reshape(xs * own, depth)
    mate_rows = swap(my_rows)
    core_scalar = core.astype(jnp.int32).reshape(1)
    mate_out = feed_forward(mate_rows, weights, core_scalar, jnp.bfloat16)
    mate_sum = swap(mate_out)
    my_out = feed_forward(my_rows, weights, core_scalar, jnp.float32)
    ffn_sum = summed((my_out + mate_sum.astype(jnp.float32)).astype(jnp.bfloat16))
    return (mixed_rows + ffn_sum).astype(jnp.bfloat16)


def solution(mesh):
    return jax.shard_map(
        shards,
        mesh=mesh,
        in_specs=(
            P("sp", "tp"),
            P("sp", "tp"),
            P("sp", "tp"),
            P("tp"),
            P(("sp", "tp"), None),
            P("tp", None),
            P(),
            P("sp", "tp"),
            P("sp", "tp"),
            P("tp", "sp"),
        ),
        out_specs=P(("sp", "tp"), None),
        check_vma=False,
    )
```

time: 171 us -> 148 us (0.87)
  the two profiles are of different devices: /device:TPU:1 before, /device:TPU:248 now
where the time goes in v1:
time: 148 us; the launch traced here: 147 us
  blocking collectives  77.7 us (52%)
  starting transfers between devices  16 us (11%)
  between operations  13.8 us (9%)
  Pallas kernels  12.3 us (8%)
  waiting for transfers between devices  11.8 us (8%)
  local copies, waits for them, and re-layouts  9.49 us (6%)
  other arithmetic  3.68 us (2%)
  matrix products  2.53 us (2%)
    all_to_all x2, blocking collectives, summed(): lax.all_to_all(partial.reshape(xs, own, depth), 'tp', 0, 0, tiled=True, a...  37.8 us
    all_to_all x1, blocking collectives, shards(): lax.all_to_all(jnp.broadcast_to(mine[None], (SIDE, *mine.shape)), both_ax...  23.2 us
    all_to_all x1, blocking collectives, shards(): lax.all_to_all(jnp.broadcast_to(normed[None], (xs, own, depth)), 'tp', 0,...  16.7 us
    pallas_call x2, Pallas kernels, feed_forward(): pl.pallas_call(functools.partial(ffn_kernel, hid=hid), out_shape=jax.Shap...  12.3 us
    ppermute x1, starting transfers between devices, with_halo(): low = lax.ppermute(block[-width:], axis, forward)  8.13 us
    ppermute x1, waiting for transfers between devices, with_halo(): high = lax.ppermute(block[:width], axis, backward)  6.56 us
    ppermute x3, starting transfers between devices, swap(): return lax.ppermute(array, 'tp', core_swap(tps))  5.89 us
    ppermute x3, waiting for transfers between devices, swap(): return lax.ppermute(array, 'tp', core_swap(tps))  5.25 us
  transfers between devices with their start and end apart: 6, of which 3 were waited for; matrix products, arithmetic and copies ran while one was open for 5% of the time, Pallas kernels for 4%

profile of v1, /device:TPU:248, one launch (start us, length us, event | category | flops | bytes accessed | tf_op | source)
XLA Modules:
  0.0 147.3 jit_solution(15359366910845390290)
XLA Ops:
  6.6 0.8 slice.82
  7.4 0.7 slice.83
  8.1 0.8 fusion.18
  8.9 0.9 concatenate.16
  9.8 0.1 broadcast_in_dim.12
  9.9 23.2 %all_to_all.20 = bf16[8,32,2112]{2,1,0:T(8,128)(2,1)} all-to-all(bf16[8,32,2112]{2,1,0:T(8,128)(2,1)S(1)} %broadcast_in_dim.12), channel_id=1, replica_groups={{0,8,16,24,32,40,48,56},{64,72,80,88,96,104,112,120},{128,136,144,152,1..., dimensions={0} | all-to-all | bytes 2162688 | tf_op jit(solution)/shard_map/all_to_all | solution.py:193
  33.1 0.1 compare_and_fusion
  33.4 0.1 copy.22
  33.5 0.1 copy.23
  33.6 0.1 fusion.13
  33.7 8.1 %collective-permute-start = (bf16[128,128]{1,0:T(8,128)(2,1)S(1)}, bf16[128,128]{1,0:T(8,128)(2,1)S(1)}, u32[]{:S(2)}, u32[]{:S(2)}) collective-permute-start(bf16[128,128]{1,0:T(8,128)(2,1)S(1)} %get-tuple-element.20), channel_id=1, source_target_pairs={{0,8},{8,16},{16,24},{24,32},{32,40},{40,48},{48,56},{56,64},{64,7... | collective-permute-start | bytes 98312 | tf_op jit(solution)/shard_map/ppermute | solution.py:122
  41.9 1.9 %collective-permute-start.1 = (bf16[128,128]{1,0:T(8,128)(2,1)S(1)}, bf16[128,128]{1,0:T(8,128)(2,1)S(1)}, u32[]{:S(2)}, u32[]{:S(2)}) collective-permute-start(bf16[128,128]{1,0:T(8,128)(2,1)S(1)} %get-tuple-element.21), channel_id=1, source_target_pairs={{8,0},{16,8},{24,16},{32,24},{40,32},{48,40},{56,48},{64,56},{72,6... | collective-permute-start | bytes 98312 | tf_op jit(solution)/shard_map/ppermute | solution.py:123
  43.8 0.6 fusion.10
  44.4 0.2 reshape.164
  44.7 6.6 %collective-permute-done.1 = bf16[128,128]{1,0:T(8,128)(2,1)S(1)} collective-permute-done((bf16[128,128]{1,0:T(8,128)(2,1)S(1)}, bf16[128,128]{1,0:T(8,128)(2,1)S(1)}, u32[]{:S(2)}, u32[]{:S(2)}) %collective-permute-start.1) | collective-permute-done | bytes 32800 | tf_op jit(solution)/shard_map/ppermute | solution.py:123
  51.2 0.2 pad_maximum_fusion.3
  51.4 0.1 copy.24
  51.5 0.1 copy.26
  51.7 0.1 copy.25
  51.9 0.7 fusion.1
  52.6 0.1 broadcast_maximum_fusion
  52.7 0.7 fusion
  53.4 0.1 exponential_add_fusion
  53.4 1.0 fusion.7
  54.4 0.2 reshape.165
  54.6 0.7 fusion.17
  55.4 0.3 copy.38
  55.7 0.3 copy.37
  56.1 0.4 convolution_convert_fusion
  56.5 1.9 %collective-permute-start.2 = (bf16[256,2048]{1,0:T(8,128)(2,1)S(1)}, bf16[256,2048]{1,0:T(8,128)(2,1)S(1)}, u32[]{:S(2)}, u32[]{:S(2)}) collective-permute-start(bf16[256,2048]{1,0:T(8,128)(2,1)S(1)} %convolution_convert_fusion), channel_id=1, source_target_pairs={{0,1},{1,0},{2,3},{3,2},{4,5},{5,4},{6,7},{7,6},{8,9},{9,8},{10,11... | collective-permute-start | bytes 3145736 | tf_op jit(solution)/shard_map/ppermute | solution.py:217
  58.4 2.6 %collective-permute-done.2 = bf16[256,2048]{1,0:T(8,128)(2,1)S(1)} collective-permute-done((bf16[256,2048]{1,0:T(8,128)(2,1)S(1)}, bf16[256,2048]{1,0:T(8,128)(2,1)S(1)}, u32[]{:S(2)}, u32[]{:S(2)}) %collective-permute-start.2) | collective-permute-done | bytes 1048608 | tf_op jit(solution)/shard_map/ppermute | solution.py:217
  61.1 0.4 add_convert_fusion.1
  61.5 19.5 %all_to_all.21 = bf16[4,64,2048]{2,1,0:T(8,128)(2,1)S(1)} all-to-all(bf16[4,64,2048]{2,1,0:T(8,128)(2,1)S(1)} %bitcast.63), channel_id=1, replica_groups={{0,2,4,6},{1,3,5,7},{8,10,12,14},{9,11,13,15},{16,18,20,22},{17,19,21,2..., dimensions={0} | all-to-all | bytes 2097152 | tf_op jit(solution)/shard_map/all_to_all | solution.py:220
  81.0 0.2 convert_reduce_fusion.1
  81.2 0.2 multiply_reduce_fusion
  81.4 0.1 multiply_convert_fusion
  81.5 0.1 broadcast_in_dim.19
  81.6 16.7 %all_to_all.22 = bf16[4,64,2048]{2,1,0:T(8,128)(2,1)S(1)} all-to-all(bf16[4,64,2048]{2,1,0:T(8,128)(2,1)S(1)} %broadcast_in_dim.19), channel_id=1, replica_groups={{0,2,4,6},{1,3,5,7},{8,10,12,14},{9,11,13,15},{16,18,20,22},{17,19,21,2..., dimensions={0} | all-to-all | bytes 2097152 | tf_op jit(solution)/shard_map/all_to_all | solution.py:233
  98.4 1.9 %collective-permute-start.3 = (bf16[256,2048]{1,0:T(8,128)(2,1)S(1)}, bf16[256,2048]{1,0:T(8,128)(2,1)S(1)}, u32[]{:S(2)}, u32[]{:S(2)}) collective-permute-start(bf16[256,2048]{1,0:T(8,128)(2,1)S(1)} %bitcast.61), channel_id=1, source_target_pairs={{0,1},{1,0},{2,3},{3,2},{4,5},{5,4},{6,7},{7,6},{8,9},{9,8},{10,11... | collective-permute-start | bytes 3145736 | tf_op jit(solution)/shard_map/ppermute | solution.py:217
  100.3 2.6 %collective-permute-done.3.rows_ref = bf16[256,2048]{1,0:T(8,128)(2,1)S(1)} collective-permute-done((bf16[256,2048]{1,0:T(8,128)(2,1)S(1)}, bf16[256,2048]{1,0:T(8,128)(2,1)S(1)}, u32[]{:S(2)}, u32[]{:S(2)}) %collective-permute-start.3) | collective-permute-done | bytes 1048608 | tf_op jit(solution)/shard_map/ppermute | solution.py:217
  102.9 3.5 %copy-done.1 = bf16[64,32,2112]{2,1,0:T(8,128)(2,1)S(1)} copy-done((bf16[64,32,2112]{2,1,0:T(8,128)(2,1)S(1)}, bf16[64,32,2112]{2,1,0:T(8,128)(2,1)}, u32[]{:S(2)}) %copy-start.1) | copy-done | bytes 8650776
  106.4 6.3 %ffn.3 = bf16[256,2048]{1,0:T(8,128)(2,1)S(1)} custom-call(s32[1]{0:T(128)} %bitcast.17.core_ref, bf16[256,2048]{1,0:T(8,128)(2,1)S(1)} %collective-permute-done.3.rows_ref, bf16[8,8,32,2112]{3,2,1,0:T(8,128)(2,1)S(1)} %bitcast.59), custom_call_target="tpu_custom_call" | custom-call | flops 2214592512 | bytes 10747904 | tf_op jit(solution)/shard_map/ffn/pallas_call | solution.py:94
  112.7 2.1 %collective-permute-start.4 = (bf16[256,2048]{1,0:T(8,128)(2,1)S(1)}, bf16[256,2048]{1,0:T(8,128)(2,1)S(1)}, u32[]{:S(2)}, u32[]{:S(2)}) collective-permute-start(bf16[256,2048]{1,0:T(8,128)(2,1)S(1)} %ffn.3), channel_id=1, source_target_pairs={{0,1},{1,0},{2,3},{3,2},{4,5},{5,4},{6,7},{7,6},{8,9},{9,8},{10,11... | collective-permute-start | bytes 3145736 | tf_op jit(solution)/shard_map/ppermute | solution.py:217
  114.8 6.1 %ffn.2 = f32[256,2048]{1,0:T(8,128)S(1)} custom-call(s32[1]{0:T(128)} %bitcast.17.core_ref, bf16[256,2048]{1,0:T(8,128)(2,1)S(1)} %bitcast.62, bf16[8,8,32,2112]{3,2,1,0:T(8,128)(2,1)S(1)} %bitcast.60), custom_call_target="tpu_custom_call" | custom-call | flops 2214592512 | bytes 10747904 | tf_op jit(solution)/shard_map/ffn/pallas_call | solution.py:94
  120.9 0.3 add_convert_fusion
  121.2 18.3 %all_to_all.23 = bf16[4,64,2048]{2,1,0:T(8,128)(2,1)S(1)} all-to-all(bf16[4,64,2048]{2,1,0:T(8,128)(2,1)S(1)} %bitcast.64), channel_id=1, replica_groups={{0,2,4,6},{1,3,5,7},{8,10,12,14},{9,11,13,15},{16,18,20,22},{17,19,21,2..., dimensions={0} | all-to-all | bytes 2097152 | tf_op jit(solution)/shard_map/all_to_all | solution.py:220
  139.5 0.2 convert_reduce_fusion
  139.7 0.8 add_convert_fusion.2
  (32 shorter events, 0.3 us)
Async XLA Ops:
  6.5 49.5 %copy-start = (bf16[256,2048]{1,0:T(8,128)(2,1)S(1)}, bf16[256,2048]{1,0:T(8,128)(2,1)}, u32[]{:S(2)}) copy-start(bf16[256,2048]{1,0:T(8,128)(2,1)} %param.15) | copy-start | bytes 3145732
  6.5 26.9 %copy-start.8 = (bf16[512,64]{0,1:T(8,128)(2,1)S(1)}, bf16[512,64]{0,1:T(8,128)(2,1)}, u32[]{:S(2)}) copy-start(bf16[512,64]{0,1:T(8,128)(2,1)} %param.12) | copy-start | bytes 196612
  6.5 26.8 %copy-start.7 = (bf16[512,64]{0,1:T(8,128)(2,1)S(1)}, bf16[512,64]{0,1:T(8,128)(2,1)}, u32[]{:S(2)}) copy-start(bf16[512,64]{0,1:T(8,128)(2,1)} %param.11) | copy-start | bytes 196612
  6.5 37.9 %copy-start.6 = (bf16[512,256]{1,0:T(8,128)(2,1)S(1)}, bf16[512,256]{1,0:T(8,128)(2,1)}, u32[]{:S(2)}) copy-start(bf16[512,256]{1,0:T(8,128)(2,1)} %param.10) | copy-start | bytes 786436
  6.5 96.4 %all-gather.3.cloned.1.call-start = ((), (), s32[]{:S(2)}) async-start(), calls=%async_computation.4 | async-start | bytes 10027008 | tf_op jit(solution)/shard_map/all_gather | solution.py:202
  33.7 11.0 %collective-permute-start = (bf16[128,128]{1,0:T(8,128)(2,1)S(1)}, bf16[128,128]{1,0:T(8,128)(2,1)S(1)}, u32[]{:S(2)}, u32[]{:S(2)}) collective-permute-start(bf16[128,128]{1,0:T(8,128)(2,1)S(1)} %get-tuple-element.20), channel_id=1, source_target_pairs={{0,8},{8,16},{16,24},{24,32},{32,40},{40,48},{48,56},{56,64},{64,7... | collective-permute-start | bytes 98312 | tf_op jit(solution)/shard_map/ppermute | solution.py:122
  41.9 9.4 %collective-permute-start.1 = (bf16[128,128]{1,0:T(8,128)(2,1)S(1)}, bf16[128,128]{1,0:T(8,128)(2,1)S(1)}, u32[]{:S(2)}, u32[]{:S(2)}) collective-permute-start(bf16[128,128]{1,0:T(8,128)(2,1)S(1)} %get-tuple-element.21), channel_id=1, source_target_pairs={{8,0},{16,8},{24,16},{32,24},{40,32},{48,40},{56,48},{64,56},{72,6... | collective-permute-start | bytes 98312 | tf_op jit(solution)/shard_map/ppermute | solution.py:123
  44.7 7.9 %copy-start.10 = (f32[4]{0:T(128)S(1)}, f32[4]{0:T(128)}, u32[]{:S(2)}) copy-start(f32[4]{0:T(128)} %param.13) | copy-start | bytes 52
  56.5 4.6 %collective-permute-start.2 = (bf16[256,2048]{1,0:T(8,128)(2,1)S(1)}, bf16[256,2048]{1,0:T(8,128)(2,1)S(1)}, u32[]{:S(2)}, u32[]{:S(2)}) collective-permute-start(bf16[256,2048]{1,0:T(8,128)(2,1)S(1)} %convolution_convert_fusion), channel_id=1, source_target_pairs={{0,1},{1,0},{2,3},{3,2},{4,5},{5,4},{6,7},{7,6},{8,9},{9,8},{10,11... | collective-permute-start | bytes 3145736 | tf_op jit(solution)/shard_map/ppermute | solution.py:217
  61.1 20.1 %copy-start.5 = (bf16[64,2048]{1,0:T(8,128)(2,1)S(1)}, bf16[64,2048]{1,0:T(8,128)(2,1)}, u32[]{:S(2)}) copy-start(bf16[64,2048]{1,0:T(8,128)(2,1)} %param.14) | copy-start | bytes 786436
  61.1 20.3 %copy-start.9 = (f32[2048]{0:T(1024)S(1)}, f32[2048]{0:T(1024)}, u32[]{:S(2)}) copy-start(f32[2048]{0:T(1024)} %param.16) | copy-start | bytes 24580
  81.2 17.2 %copy-start.3 = (f32[64,2048]{1,0:T(8,128)}, f32[64,2048]{1,0:T(8,128)S(1)}, u32[]{:S(2)}) copy-start(f32[64,2048]{1,0:T(8,128)S(1)} %convert_reduce_fusion.1) | copy-start | bytes 1572868
  98.4 4.5 %collective-permute-start.3 = (bf16[256,2048]{1,0:T(8,128)(2,1)S(1)}, bf16[256,2048]{1,0:T(8,128)(2,1)S(1)}, u32[]{:S(2)}, u32[]{:S(2)}) collective-permute-start(bf16[256,2048]{1,0:T(8,128)(2,1)S(1)} %bitcast.61), channel_id=1, source_target_pairs={{0,1},{1,0},{2,3},{3,2},{4,5},{5,4},{6,7},{7,6},{8,9},{9,8},{10,11... | collective-permute-start | bytes 3145736 | tf_op jit(solution)/shard_map/ppermute | solution.py:217
  102.9 3.5 %copy-start.1 = (bf16[64,32,2112]{2,1,0:T(8,128)(2,1)S(1)}, bf16[64,32,2112]{2,1,0:T(8,128)(2,1)}, u32[]{:S(2)}) copy-start(bf16[64,32,2112]{2,1,0:T(8,128)(2,1)} %all-gather.3.cloned.1.call-done) | copy-start | bytes 25952260
  106.4 8.3 %copy-start.2 = (bf16[64,32,2112]{2,1,0:T(8,128)(2,1)S(1)}, bf16[64,32,2112]{2,1,0:T(8,128)(2,1)}, u32[]{:S(2)}) copy-start(bf16[64,32,2112]{2,1,0:T(8,128)(2,1)} %all-gather.3.cloned.1.call-done) | copy-start | bytes 25952260
  112.7 8.2 %collective-permute-start.4 = (bf16[256,2048]{1,0:T(8,128)(2,1)S(1)}, bf16[256,2048]{1,0:T(8,128)(2,1)S(1)}, u32[]{:S(2)}, u32[]{:S(2)}) collective-permute-start(bf16[256,2048]{1,0:T(8,128)(2,1)S(1)} %ffn.3), channel_id=1, source_target_pairs={{0,1},{1,0},{2,3},{3,2},{4,5},{5,4},{6,7},{7,6},{8,9},{9,8},{10,11... | collective-permute-start | bytes 3145736 | tf_op jit(solution)/shard_map/ppermute | solution.py:217
  120.9 18.8 %copy-start.4 = (f32[64,2048]{1,0:T(8,128)S(1)}, f32[64,2048]{1,0:T(8,128)}, u32[]{:S(2)}) copy-start(f32[64,2048]{1,0:T(8,128)} %copy-done.3) | copy-start | bytes 1572868
Sparse Core Ops, SparseCore 0:
  33.2 60.1 all-gather.2

commit v2 on v1

--- a/solution.py
+++ b/solution.py
@@ -11,7 +11,7 @@
 WINDOW = 128
 SIDE = 8
 CORES = 2
-LANES = 128
+FIRST_VMEM = 40 * 1024 * 1024
 
 
 def device_index(sp, tp, tps):
@@ -36,83 +36,122 @@
     return [(i, i ^ 1) for i in range(tps)]
 
 
-def ffn_kernel(core_ref, rows_ref, weights_ref, out_ref, held, hidden, sems, *, hid):
-    full = hid // LANES
-    rest = hid - full * LANES
-    gated = 2 * hid
-    parts = [(2 * LANES * j, 2 * LANES) for j in range(full)] + [(2 * LANES * full, 2 * rest)]
-    parts.append((gated, hid))
+def joined_kernel(gate_ref, up_ref, down_ref, out_ref):
+    mine = jnp.concatenate([gate_ref[...], up_ref[...], down_ref[...]], axis=1)
+    for i in range(out_ref.shape[0]):
+        out_ref[i] = mine
+
+
+def joined_weights(gate_weight, up_weight, down_weight):
+    piece, hid = gate_weight.shape
+    return pl.pallas_call(
+        joined_kernel,
+        out_shape=jax.ShapeDtypeStruct((SIDE, piece, 3 * hid), gate_weight.dtype),
+        in_specs=[pl.BlockSpec(memory_space=pltpu.VMEM)] * 3,
+        out_specs=pl.BlockSpec(memory_space=pltpu.VMEM),
+        compiler_params=pltpu.CompilerParams(vmem_limit_bytes=4 * 1024 * 1024),
+        name="joined",
+    )(gate_weight, up_weight, down_weight.T)
+
+
+def gated_product(both, hid):
+    gate, up = both[:, :hid], both[:, hid:]
+    return (gate / (1.0 + jnp.exp(-gate)) * up).astype(jnp.bfloat16)
+
+
+def down_product(hidden, down):
+    return lax.dot_general(hidden, down, (((1,), (1,)), ((), ())), preferred_element_type=jnp.float32)
+
+
+def first_kernel(core_ref, rows_ref, weights_ref, out_ref, held, total, sems, *, hid):
+    piece = held.shape[2]
+    per = 2
+    span = per * SIDE * piece
     core = core_ref[0]
 
-    def copies(part, swapped):
-        at, size = parts[part]
-        return [
-            pltpu.make_async_copy(
-                weights_ref.at[:, i, :, pl.ds(at, size)]
-                if swapped
-                else weights_ref.at[i, :, :, pl.ds(at, size)],
-                held.at[i, :, :, pl.ds(at, size)],
-                sems.at[part],
-            )
-            for i in range(SIDE)
-        ]
+    def copy(i, swapped):
+        source = weights_ref.at[:, i] if swapped else weights_ref.at[i]
+        return pltpu.make_async_copy(source, held.at[i], sems.at[i])
 
     for swapped in (False, True):
 
         @pl.when(core == int(swapped))
         def _():
-            for part in range(len(parts)):
-                for copy in copies(part, swapped):
-                    copy.start()
-
-    depth = rows_ref.shape[1]
-    for part in range(full + 1):
-        at, size = parts[part]
-        for copy in copies(part, False):
-            copy.wait()
-        tile = held[:, :, :, at : at + size].reshape(depth, size)
-        both = jnp.dot(rows_ref[...], tile, preferred_element_type=jnp.float32)
-        gate, up = both[:, : size // 2], both[:, size // 2 :]
-        hidden[:, at // 2 : at // 2 + size // 2] = (gate / (1.0 + jnp.exp(-gate)) * up).astype(
-            hidden.dtype
+            for i in range(SIDE):
+                copy(i, swapped).start()
+
+    both = None
+    for step in range(SIDE // per):
+        for i in range(step * per, (step + 1) * per):
+            copy(i, False).wait()
+        tile = held[step * per : (step + 1) * per, :, :, : 2 * hid].reshape(span, 2 * hid)
+        part = jnp.dot(
+            rows_ref[:, step * span : (step + 1) * span], tile, preferred_element_type=jnp.float32
         )
-    for copy in copies(full + 1, False):
-        copy.wait()
-    for i in range(SIDE):
-        tile = held[i, :, :, gated : gated + hid].reshape(-1, hid)
-        width = tile.shape[0]
-        out_ref[:, i * width : (i + 1) * width] = lax.dot_general(
-            hidden[...], tile, (((1,), (1,)), ((), ())), preferred_element_type=jnp.float32
-        ).astype(out_ref.dtype)
-
-
-def feed_forward(rows, weights, core, out_dtype):
+        if step == 0:
+            total[...] = part
+        elif step < SIDE // per - 1:
+            total[...] += part
+        else:
+            both = total[...] + part
+    down = held[:, :, :, 2 * hid :].reshape(-1, hid)
+    out_ref[...] = down_product(gated_product(both, hid), down).astype(out_ref.dtype)
+
+
+def second_kernel(rows_ref, held, out_ref, *, hid):
+    tile = held[:, :, :, : 2 * hid].reshape(-1, 2 * hid)
+    both = jnp.dot(rows_ref[...], tile, preferred_element_type=jnp.float32)
+    down = held[:, :, :, 2 * hid :].reshape(-1, hid)
+    out_ref[...] = down_product(gated_product(both, hid), down).astype(out_ref.dtype)
+
+
+def ffn_cost(rows, width):
     count, depth = rows.shape
-    piece, width = weights.shape[2:]
-    hid = width // 3
-    parts = hid // LANES + 2
+    return pl.CostEstimate(
+        flops=2 * count * depth * width,
+        bytes_accessed=2 * depth * width + 4 * rows.size,
+        transcendentals=count * width // 3,
+    )
+
+
+def feed_forward_first(rows, weights, core):
+    count, depth = rows.shape
+    width = weights.shape[3]
+    vmem = pl.BlockSpec(memory_space=pltpu.VMEM)
     return pl.pallas_call(
-        functools.partial(ffn_kernel, hid=hid),
-        out_shape=jax.ShapeDtypeStruct((count, depth), out_dtype),
+        functools.partial(first_kernel, hid=width // 3),
+        out_shape=(
+            jax.ShapeDtypeStruct((count, depth), jnp.bfloat16),
+            jax.ShapeDtypeStruct(weights.shape, weights.dtype),
+        ),
         in_specs=[
             pl.BlockSpec(memory_space=pltpu.SMEM),
-            pl.BlockSpec(memory_space=pltpu.VMEM),
+            vmem,
             pl.BlockSpec(memory_space=pl.ANY),
         ],
-        out_specs=pl.BlockSpec(memory_space=pltpu.VMEM),
+        out_specs=(vmem, vmem),
         scratch_shapes=[
-            pltpu.VMEM((SIDE, SIDE, piece, width), jnp.bfloat16),
-            pltpu.VMEM((count, hid), jnp.bfloat16),
-            pltpu.SemaphoreType.DMA((parts,)),
+            pltpu.VMEM((count, 2 * width // 3), jnp.float32),
+            pltpu.SemaphoreType.DMA((SIDE,)),
         ],
-        cost_estimate=pl.CostEstimate(
-            flops=2 * count * depth * width,
-            bytes_accessed=2 * weights.size + 4 * rows.size,
-            transcendentals=count * hid,
-        ),
-        compiler_params=pltpu.CompilerParams(vmem_limit_bytes=40 * 1024 * 1024),
-        name="ffn",
+        cost_estimate=ffn_cost(rows, width),
+        compiler_params=pltpu.CompilerParams(vmem_limit_bytes=FIRST_VMEM),
+        name="ffn_first",
     )(core, rows, weights)
+
+
+def feed_forward_second(rows, held):
+    width = held.shape[3]
+    vmem = pl.BlockSpec(memory_space=pltpu.VMEM)
+    return pl.pallas_call(
+        functools.partial(second_kernel, hid=width // 3),
+        out_shape=jax.ShapeDtypeStruct(rows.shape, jnp.float32),
+        in_specs=[vmem, vmem],
+        out_specs=vmem,
+        cost_estimate=ffn_cost(rows, width),
+        compiler_params=pltpu.CompilerParams(vmem_limit_bytes=24 * 1024 * 1024),
+        name="ffn_second",
+    )(rows, held)
 
 
 def with_halo(block, axis, width):
@@ -160,14 +199,6 @@
 def rms_scale(mixed_rows, norm_gain):
     inverse = lax.rsqrt(jnp.mean(mixed_rows * mixed_rows, axis=-1, keepdims=True) + 1e-06)
     return (mixed_rows * inverse * norm_gain).astype(jnp.bfloat16)
-
-
-def joined_weights(gate_weight, up_weight, down_weight):
-    hid = gate_weight.shape[1]
-    pieces = []
-    for at in range(0, hid, LANES):
-        pieces += [gate_weight[:, at : at + LANES], up_weight[:, at : at + LANES]]
-    return jnp.concatenate(pieces + [down_weight.T], axis=1)
 
 
 def shards(
@@ -191,7 +222,7 @@
 
     mine = joined_weights(gate_weight, up_weight, down_weight)
     line = lax.all_to_all(
-        jnp.broadcast_to(mine[None], (SIDE, *mine.shape)),
+        mine,
         both_axes,
         0,
         0,
@@ -240,9 +271,9 @@
     ).reshape(xs * own, depth)
     mate_rows = swap(my_rows)
     core_scalar = core.astype(jnp.int32).reshape(1)
-    mate_out = feed_forward(mate_rows, weights, core_scalar, jnp.bfloat16)
+    mate_out, held = feed_forward_first(mate_rows, weights, core_scalar)
     mate_sum = swap(mate_out)
-    my_out = feed_forward(my_rows, weights, core_scalar, jnp.float32)
+    my_out = feed_forward_second(my_rows, held)
     ffn_sum = summed((my_out + mate_sum.astype(jnp.float32)).astype(jnp.bfloat16))
     return (mixed_rows + ffn_sum).astype(jnp.bfloat16)
 

time: 148 us -> 139 us (0.939)
  local copies, waits for them, and re-layouts: 9.49 us -> 5.12 us
  Pallas kernels: 12.3 us -> 8.01 us
    pallas_call x2 -> x3, Pallas kernels: 12.3 us -> 8.01 us  [the longest x1 5.15 us: feed_forward_first(): pl.pallas_call(functools.partial(first_kernel, hid=width // 3), out_shape...]
    slice x3 -> x0, local copies, waits for them, and re-layouts: 2.34 us -> none  [joined_weights(): pieces += [gate_weight[:, at:at + LANES], up_weight[:, at:at + LANES]]]
    unnamed x24 -> x26, local copies, waits for them, and re-layouts: 4.21 us -> 3.16 us
  transfers between devices with their start and end apart: 6 -> 6, of which waited for: 3 -> 3; matrix products, arithmetic and copies ran while one was open for 5% -> 5% of each run, Pallas kernels for 4% -> 2%
where the time goes in v2:
time: 139 us
  blocking collectives  77.8 us (56%)
  starting transfers between devices  16.1 us (12%)
  between operations  13.7 us (10%)
  waiting for transfers between devices  11.8 us (8%)
  Pallas kernels  8.01 us (6%)
  local copies, waits for them, and re-layouts  5.12 us (4%)
  other arithmetic  3.7 us (3%)
  matrix products  2.53 us (2%)
    all_to_all x2, blocking collectives, summed(): lax.all_to_all(partial.reshape(xs, own, depth), 'tp', 0, 0, tiled=True, a...  37.8 us
    all_to_all x1, blocking collectives, shards(): lax.all_to_all(mine, both_axes, 0, 0, tiled=True, axis_index_groups=line_...  23.3 us
    all_to_all x1, blocking collectives, shards(): lax.all_to_all(jnp.broadcast_to(normed[None], (xs, own, depth)), 'tp', 0,...  16.7 us
    ppermute x1, starting transfers between devices, with_halo(): low = lax.ppermute(block[-width:], axis, forward)  8.13 us
    ppermute x1, waiting for transfers between devices, with_halo(): high = lax.ppermute(block[:width], axis, backward)  6.55 us
    ppermute x3, starting transfers between devices, swap(): return lax.ppermute(array, 'tp', core_swap(tps))  6.06 us
    ppermute x3, waiting for transfers between devices, swap(): return lax.ppermute(array, 'tp', core_swap(tps))  5.25 us
    pallas_call x1, Pallas kernels, feed_forward_first(): pl.pallas_call(functools.partial(first_kernel, hid=width // 3), out_shape...  5.15 us
  transfers between devices with their start and end apart: 6, of which 3 were waited for; matrix products, arithmetic and copies ran while one was open for 5% of the time, Pallas kernels for 2%

profile of v2, /device:TPU:248, one launch (start us, length us, event | category | flops | bytes accessed | tf_op | source)
XLA Modules:
  0.0 138.9 jit_solution(7223932100250975270)
XLA Ops:
  6.5 0.9 copy-done.1
  7.4 0.8 copy-done.2
  8.2 0.8 copy-done.3
  9.0 0.1 joined.1
  9.1 23.3 %all_to_all.20 = bf16[8,32,2112]{2,1,0:T(8,128)(2,1)} all-to-all(bf16[8,32,2112]{2,1,0:T(8,128)(2,1)S(1)} %joined.1), channel_id=1, replica_groups={{0,8,16,24,32,40,48,56},{64,72,80,88,96,104,112,120},{128,136,144,152,1..., dimensions={0} | all-to-all | bytes 2162688 | tf_op jit(solution)/shard_map/all_to_all | solution.py:224
  32.5 0.1 compare_and_fusion
  32.6 0.1 iota_add_fusion.1
  32.6 0.1 iota_add_fusion
  32.7 0.1 copy.22
  32.9 0.1 copy.23
  33.0 0.1 fusion.13
  33.1 8.1 %collective-permute-start = (bf16[128,128]{1,0:T(8,128)(2,1)S(1)}, bf16[128,128]{1,0:T(8,128)(2,1)S(1)}, u32[]{:S(2)}, u32[]{:S(2)}) collective-permute-start(bf16[128,128]{1,0:T(8,128)(2,1)S(1)} %get-tuple-element.24), channel_id=1, source_target_pairs={{0,8},{8,16},{16,24},{24,32},{32,40},{40,48},{48,56},{56,64},{64,7... | collective-permute-start | bytes 98312 | tf_op jit(solution)/shard_map/ppermute | solution.py:161
  41.2 1.9 %collective-permute-start.1 = (bf16[128,128]{1,0:T(8,128)(2,1)S(1)}, bf16[128,128]{1,0:T(8,128)(2,1)S(1)}, u32[]{:S(2)}, u32[]{:S(2)}) collective-permute-start(bf16[128,128]{1,0:T(8,128)(2,1)S(1)} %get-tuple-element.25), channel_id=1, source_target_pairs={{8,0},{16,8},{24,16},{32,24},{40,32},{48,40},{56,48},{64,56},{72,6... | collective-permute-start | bytes 98312 | tf_op jit(solution)/shard_map/ppermute | solution.py:162
  43.1 0.6 fusion.10
  43.8 0.2 reshape.163
  44.0 6.6 %collective-permute-done.1 = bf16[128,128]{1,0:T(8,128)(2,1)S(1)} collective-permute-done((bf16[128,128]{1,0:T(8,128)(2,1)S(1)}, bf16[128,128]{1,0:T(8,128)(2,1)S(1)}, u32[]{:S(2)}, u32[]{:S(2)}) %collective-permute-start.1) | collective-permute-done | bytes 32800 | tf_op jit(solution)/shard_map/ppermute | solution.py:162
  50.6 0.2 pad_maximum_fusion.3
  50.8 0.1 copy.24
  50.9 0.1 copy.26
  51.0 0.1 copy.25
  51.2 0.7 fusion.1
  51.9 0.1 broadcast_maximum_fusion
  52.0 0.7 fusion
  52.7 0.1 exponential_add_fusion
  52.8 1.0 fusion.7
  53.8 0.2 reshape.164
  54.0 0.7 fusion.17
  54.7 0.3 copy.38
  55.1 0.3 copy.37
  55.4 0.4 convolution_convert_fusion
  55.9 1.9 %collective-permute-start.2 = (bf16[256,2048]{1,0:T(8,128)(2,1)S(1)}, bf16[256,2048]{1,0:T(8,128)(2,1)S(1)}, u32[]{:S(2)}, u32[]{:S(2)}) collective-permute-start(bf16[256,2048]{1,0:T(8,128)(2,1)S(1)} %convolution_convert_fusion), channel_id=1, source_target_pairs={{0,1},{1,0},{2,3},{3,2},{4,5},{5,4},{6,7},{7,6},{8,9},{9,8},{10,11... | collective-permute-start | bytes 3145736 | tf_op jit(solution)/shard_map/ppermute | solution.py:248
  57.8 2.6 %collective-permute-done.2 = bf16[256,2048]{1,0:T(8,128)(2,1)S(1)} collective-permute-done((bf16[256,2048]{1,0:T(8,128)(2,1)S(1)}, bf16[256,2048]{1,0:T(8,128)(2,1)S(1)}, u32[]{:S(2)}, u32[]{:S(2)}) %collective-permute-start.2) | collective-permute-done | bytes 1048608 | tf_op jit(solution)/shard_map/ppermute | solution.py:248
  60.4 0.4 add_convert_fusion.1
  60.9 19.5 %all_to_all.21 = bf16[4,64,2048]{2,1,0:T(8,128)(2,1)S(1)} all-to-all(bf16[4,64,2048]{2,1,0:T(8,128)(2,1)S(1)} %bitcast.63), channel_id=1, replica_groups={{0,2,4,6},{1,3,5,7},{8,10,12,14},{9,11,13,15},{16,18,20,22},{17,19,21,2..., dimensions={0} | all-to-all | bytes 2097152 | tf_op jit(solution)/shard_map/all_to_all | solution.py:251
  80.4 0.2 convert_reduce_fusion.1
  80.6 0.2 multiply_reduce_fusion
  80.7 0.1 multiply_convert_fusion
  80.9 0.1 broadcast_in_dim.16
  81.0 16.7 %all_to_all.22 = bf16[4,64,2048]{2,1,0:T(8,128)(2,1)S(1)} all-to-all(bf16[4,64,2048]{2,1,0:T(8,128)(2,1)S(1)} %broadcast_in_dim.16), channel_id=1, replica_groups={{0,2,4,6},{1,3,5,7},{8,10,12,14},{9,11,13,15},{16,18,20,22},{17,19,21,2..., dimensions={0} | all-to-all | bytes 2097152 | tf_op jit(solution)/shard_map/all_to_all | solution.py:264
  97.7 1.9 %collective-permute-start.3 = (bf16[256,2048]{1,0:T(8,128)(2,1)S(1)}, bf16[256,2048]{1,0:T(8,128)(2,1)S(1)}, u32[]{:S(2)}, u32[]{:S(2)}) collective-permute-start(bf16[256,2048]{1,0:T(8,128)(2,1)S(1)} %bitcast.59), channel_id=1, source_target_pairs={{0,1},{1,0},{2,3},{3,2},{4,5},{5,4},{6,7},{7,6},{8,9},{9,8},{10,11... | collective-permute-start | bytes 3145736 | tf_op jit(solution)/shard_map/ppermute | solution.py:248
  99.6 2.6 %collective-permute-done.3.rows_ref = bf16[256,2048]{1,0:T(8,128)(2,1)S(1)} collective-permute-done((bf16[256,2048]{1,0:T(8,128)(2,1)S(1)}, bf16[256,2048]{1,0:T(8,128)(2,1)S(1)}, u32[]{:S(2)}, u32[]{:S(2)}) %collective-permute-start.3) | collective-permute-done | bytes 1048608 | tf_op jit(solution)/shard_map/ppermute | solution.py:248
  102.3 5.2 %ffn_first.1 = (bf16[256,2048]{1,0:T(8,128)(2,1)S(1)}, bf16[8,8,32,2112]{3,2,1,0:T(8,128)(2,1)S(1)}) custom-call(s32[1]{0:T(128)} %bitcast.18.core_ref, bf16[256,2048]{1,0:T(8,128)(2,1)S(1)} %collective-permute-done.3.rows_ref, bf16[8,8,32,2112]{3,2,1,0:T(8,128)(2,1)} %bitcast.62), custom_call_target="tpu_custom_call" | custom-call | flops 2214592512 | bytes 10747904 | tf_op jit(solution)/shard_map/ffn_first/pallas_call | solution.py:121
  107.4 2.2 %collective-permute-start.4 = (bf16[256,2048]{1,0:T(8,128)(2,1)S(1)}, bf16[256,2048]{1,0:T(8,128)(2,1)S(1)}, u32[]{:S(2)}, u32[]{:S(2)}) collective-permute-start(bf16[256,2048]{1,0:T(8,128)(2,1)S(1)} %get-tuple-element.16), channel_id=1, source_target_pairs={{0,1},{1,0},{2,3},{3,2},{4,5},{5,4},{6,7},{7,6},{8,9},{9,8},{10,11... | collective-permute-start | bytes 3145736 | tf_op jit(solution)/shard_map/ppermute | solution.py:248
  109.7 2.8 %ffn_second.1 = f32[256,2048]{1,0:T(8,128)S(1)} custom-call(bf16[256,2048]{1,0:T(8,128)(2,1)S(1)} %bitcast.60, bf16[8,8,32,2112]{3,2,1,0:T(8,128)(2,1)S(1)} %get-tuple-element.15.held), custom_call_target="tpu_custom_call" | custom-call | flops 2214592512 | bytes 10747904 | tf_op jit(solution)/shard_map/ffn_second/pallas_call | solution.py:146
  112.4 0.3 add_convert_fusion
  112.8 18.3 %all_to_all.23 = bf16[4,64,2048]{2,1,0:T(8,128)(2,1)S(1)} all-to-all(bf16[4,64,2048]{2,1,0:T(8,128)(2,1)S(1)} %bitcast.64), channel_id=1, replica_groups={{0,2,4,6},{1,3,5,7},{8,10,12,14},{9,11,13,15},{16,18,20,22},{17,19,21,2..., dimensions={0} | all-to-all | bytes 2097152 | tf_op jit(solution)/shard_map/all_to_all | solution.py:251
  131.1 0.2 convert_reduce_fusion
  131.3 0.8 add_convert_fusion.2
  (30 shorter events, 0.2 us)
Async XLA Ops:
  6.5 48.9 %copy-start = (bf16[256,2048]{1,0:T(8,128)(2,1)S(1)}, bf16[256,2048]{1,0:T(8,128)(2,1)}, u32[]{:S(2)}) copy-start(bf16[256,2048]{1,0:T(8,128)(2,1)} %param.15) | copy-start | bytes 3145732
  6.5 95.7 %all-gather.3.cloned.1.call-start = ((), (), s32[]{:S(2)}) async-start(), calls=%async_computation.4 | async-start | bytes 10027008 | tf_op jit(solution)/shard_map/all_gather | solution.py:233
  6.5 0.9 copy-start.1
  7.4 0.8 copy-start.2
  8.2 0.8 copy-start.3
  9.0 23.7 %copy-start.8 = (bf16[512,64]{0,1:T(8,128)(2,1)S(1)}, bf16[512,64]{0,1:T(8,128)(2,1)}, u32[]{:S(2)}) copy-start(bf16[512,64]{0,1:T(8,128)(2,1)} %param.11) | copy-start | bytes 196612
  9.0 23.8 %copy-start.9 = (bf16[512,64]{0,1:T(8,128)(2,1)S(1)}, bf16[512,64]{0,1:T(8,128)(2,1)}, u32[]{:S(2)}) copy-start(bf16[512,64]{0,1:T(8,128)(2,1)} %param.12) | copy-start | bytes 196612
  9.0 34.7 %copy-start.7 = (bf16[512,256]{1,0:T(8,128)(2,1)S(1)}, bf16[512,256]{1,0:T(8,128)(2,1)}, u32[]{:S(2)}) copy-start(bf16[512,256]{1,0:T(8,128)(2,1)} %param.10) | copy-start | bytes 786436
  33.1 11.0 %collective-permute-start = (bf16[128,128]{1,0:T(8,128)(2,1)S(1)}, bf16[128,128]{1,0:T(8,128)(2,1)S(1)}, u32[]{:S(2)}, u32[]{:S(2)}) collective-permute-start(bf16[128,128]{1,0:T(8,128)(2,1)S(1)} %get-tuple-element.24), channel_id=1, source_target_pairs={{0,8},{8,16},{16,24},{24,32},{32,40},{40,48},{48,56},{56,64},{64,7... | collective-permute-start | bytes 98312 | tf_op jit(solution)/shard_map/ppermute | solution.py:161
  41.2 9.4 %collective-permute-start.1 = (bf16[128,128]{1,0:T(8,128)(2,1)S(1)}, bf16[128,128]{1,0:T(8,128)(2,1)S(1)}, u32[]{:S(2)}, u32[]{:S(2)}) collective-permute-start(bf16[128,128]{1,0:T(8,128)(2,1)S(1)} %get-tuple-element.25), channel_id=1, source_target_pairs={{8,0},{16,8},{24,16},{32,24},{40,32},{48,40},{56,48},{64,56},{72,6... | collective-permute-start | bytes 98312 | tf_op jit(solution)/shard_map/ppermute | solution.py:162
  44.0 7.9 %copy-start.11 = (f32[4]{0:T(128)S(1)}, f32[4]{0:T(128)}, u32[]{:S(2)}) copy-start(f32[4]{0:T(128)} %param.13) | copy-start | bytes 52
  55.9 4.6 %collective-permute-start.2 = (bf16[256,2048]{1,0:T(8,128)(2,1)S(1)}, bf16[256,2048]{1,0:T(8,128)(2,1)S(1)}, u32[]{:S(2)}, u32[]{:S(2)}) collective-permute-start(bf16[256,2048]{1,0:T(8,128)(2,1)S(1)} %convolution_convert_fusion), channel_id=1, source_target_pairs={{0,1},{1,0},{2,3},{3,2},{4,5},{5,4},{6,7},{7,6},{8,9},{9,8},{10,11... | collective-permute-start | bytes 3145736 | tf_op jit(solution)/shard_map/ppermute | solution.py:248
  60.4 20.1 %copy-start.6 = (bf16[64,2048]{1,0:T(8,128)(2,1)S(1)}, bf16[64,2048]{1,0:T(8,128)(2,1)}, u32[]{:S(2)}) copy-start(bf16[64,2048]{1,0:T(8,128)(2,1)} %param.14) | copy-start | bytes 786436
  60.4 20.3 %copy-start.10 = (f32[2048]{0:T(1024)S(1)}, f32[2048]{0:T(1024)}, u32[]{:S(2)}) copy-start(f32[2048]{0:T(1024)} %param.16) | copy-start | bytes 24580
  80.5 17.2 %copy-start.4 = (f32[64,2048]{1,0:T(8,128)}, f32[64,2048]{1,0:T(8,128)S(1)}, u32[]{:S(2)}) copy-start(f32[64,2048]{1,0:T(8,128)S(1)} %convert_reduce_fusion.1) | copy-start | bytes 1572868
  97.7 4.5 %collective-permute-start.3 = (bf16[256,2048]{1,0:T(8,128)(2,1)S(1)}, bf16[256,2048]{1,0:T(8,128)(2,1)S(1)}, u32[]{:S(2)}, u32[]{:S(2)}) collective-permute-start(bf16[256,2048]{1,0:T(8,128)(2,1)S(1)} %bitcast.59), channel_id=1, source_target_pairs={{0,1},{1,0},{2,3},{3,2},{4,5},{5,4},{6,7},{7,6},{8,9},{9,8},{10,11... | collective-permute-start | bytes 3145736 | tf_op jit(solution)/shard_map/ppermute | solution.py:248
  107.4 5.0 %collective-permute-start.4 = (bf16[256,2048]{1,0:T(8,128)(2,1)S(1)}, bf16[256,2048]{1,0:T(8,128)(2,1)S(1)}, u32[]{:S(2)}, u32[]{:S(2)}) collective-permute-start(bf16[256,2048]{1,0:T(8,128)(2,1)S(1)} %get-tuple-element.16), channel_id=1, source_target_pairs={{0,1},{1,0},{2,3},{3,2},{4,5},{5,4},{6,7},{7,6},{8,9},{9,8},{10,11... | collective-permute-start | bytes 3145736 | tf_op jit(solution)/shard_map/ppermute | solution.py:248
  112.4 18.8 %copy-start.5 = (f32[64,2048]{1,0:T(8,128)S(1)}, f32[64,2048]{1,0:T(8,128)}, u32[]{:S(2)}) copy-start(f32[64,2048]{1,0:T(8,128)} %copy-done.4) | copy-start | bytes 1572868
Sparse Core Ops, SparseCore 0:
  32.6 60.1 all-gather.2

commit v3 on v2

--- a/solution.py
+++ b/solution.py
@@ -34,24 +34,6 @@
 
 def core_swap(tps):
     return [(i, i ^ 1) for i in range(tps)]
-
-
-def joined_kernel(gate_ref, up_ref, down_ref, out_ref):
-    mine = jnp.concatenate([gate_ref[...], up_ref[...], down_ref[...]], axis=1)
-    for i in range(out_ref.shape[0]):
-        out_ref[i] = mine
-
-
-def joined_weights(gate_weight, up_weight, down_weight):
-    piece, hid = gate_weight.shape
-    return pl.pallas_call(
-        joined_kernel,
-        out_shape=jax.ShapeDtypeStruct((SIDE, piece, 3 * hid), gate_weight.dtype),
-        in_specs=[pl.BlockSpec(memory_space=pltpu.VMEM)] * 3,
-        out_specs=pl.BlockSpec(memory_space=pltpu.VMEM),
-        compiler_params=pltpu.CompilerParams(vmem_limit_bytes=4 * 1024 * 1024),
-        name="joined",
-    )(gate_weight, up_weight, down_weight.T)
 
 
 def gated_product(both, hid):
@@ -154,46 +136,88 @@
     )(rows, held)
 
 
-def with_halo(block, axis, width):
+def halo_sides(block, axis, width):
     count = lax.axis_size(axis)
     forward = [(i, i + 1) for i in range(count - 1)]
     backward = [(target, source) for source, target in forward]
-    low = lax.ppermute(block[-width:], axis, forward)
-    high = lax.ppermute(block[:width], axis, backward)
-    return jnp.concatenate([low, block, high], axis=0)
-
-
-def attend_window(queries, padded, offset, total_rows, sink_logit):
-    rows_here = queries.shape[0]
-    block_count = rows_here // WINDOW
-    heads_here = queries.shape[1] // HEAD_DIM
-    kv_here = padded.shape[1] // (2 * HEAD_DIM)
-    group_size = heads_here // kv_here
-    blocks = padded.reshape(block_count + 2, WINDOW, padded.shape[1])
-    banded = jnp.concatenate([blocks[:-2], blocks[1:-1], blocks[2:]], axis=1)
-    key_band = banded[:, :, : kv_here * HEAD_DIM].reshape(
-        block_count, 3 * WINDOW, kv_here, HEAD_DIM
-    )
-    value_band = banded[:, :, kv_here * HEAD_DIM :].reshape(
-        block_count, 3 * WINDOW, kv_here, HEAD_DIM
-    )
-    grouped = queries.reshape(block_count, WINDOW, kv_here, group_size, HEAD_DIM)
-    scores = jnp.einsum(
-        "nqkgd,nskd->nkgqs", grouped, key_band, preferred_element_type=jnp.float32
-    ) * HEAD_DIM ** (-0.5)
-    block_start = offset + jnp.arange(block_count, dtype=jnp.int32)[:, None] * WINDOW
-    query_pos = block_start + jnp.arange(WINDOW, dtype=jnp.int32)[None, :]
-    key_pos = block_start - WINDOW + jnp.arange(3 * WINDOW, dtype=jnp.int32)[None, :]
-    valid = jnp.abs(query_pos[:, :, None] - key_pos[:, None, :]) <= WINDOW
-    valid = valid & ((key_pos >= 0) & (key_pos < total_rows))[:, None, :]
-    scores = jnp.where(valid[:, None, None], scores, -1e30)
-    sink_grid = sink_logit.reshape(kv_here, group_size)[None, :, :, None, None]
-    peak = jnp.maximum(jnp.max(scores, axis=-1, keepdims=True), sink_grid)
-    weights_raw = jnp.exp(scores - peak)
-    denom = jnp.sum(weights_raw, axis=-1, keepdims=True) + jnp.exp(sink_grid - peak)
-    probs = (weights_raw / denom).astype(jnp.bfloat16)
-    output = jnp.einsum("nkgqs,nskd->nqkgd", probs, value_band, preferred_element_type=jnp.float32)
-    return output.astype(jnp.bfloat16).reshape(rows_here, heads_here * HEAD_DIM)
+    low = lax.ppermute(block[:, -width:], axis, forward)
+    high = lax.ppermute(block[:, :width], axis, backward)
+    return low, high
+
+
+def attention_kernel(
+    place_ref, sink_ref, query_ref, low_ref, mid_ref, high_ref, proj_ref, mate_ref, mine_ref, padded, attended
+):
+    rows = query_ref.shape[0]
+    heads = query_ref.shape[1] // HEAD_DIM
+    piece = WINDOW // CORES
+    core, start, total = place_ref[0], place_ref[1], place_ref[2]
+    padded[:, :WINDOW] = low_ref[...]
+    padded[:, WINDOW : WINDOW + rows] = mid_ref[...]
+    padded[:, WINDOW + rows :] = high_ref[...]
+    query_at = lax.broadcasted_iota(jnp.int32, (WINDOW, 3 * WINDOW), 0)
+    key_at = lax.broadcasted_iota(jnp.int32, (WINDOW, 3 * WINDOW), 1)
+    near = (key_at >= query_at) & (key_at <= query_at + 2 * WINDOW)
+    for block in range(rows // WINDOW):
+        at = block * WINDOW
+        position = key_at + (start + at - WINDOW)
+        valid = near & (position >= 0) & (position < total)
+        keys = padded[:HEAD_DIM, at : at + 3 * WINDOW]
+        values = padded[HEAD_DIM:, at : at + 3 * WINDOW]
+        for head in range(heads):
+            lanes = slice(head * HEAD_DIM, (head + 1) * HEAD_DIM)
+            scores = jnp.dot(
+                query_ref[at : at + WINDOW, lanes], keys, preferred_element_type=jnp.float32
+            ) * HEAD_DIM ** (-0.5)
+            scores = jnp.where(valid, scores, -1e30)
+            sink = sink_ref[head]
+            peak = jnp.maximum(jnp.max(scores, axis=1, keepdims=True), sink)
+            raw = jnp.exp(scores - peak)
+            denom = jnp.sum(raw, axis=1, keepdims=True) + jnp.exp(sink - peak)
+            probs = (raw * (1.0 / denom)).astype(jnp.bfloat16)
+            attended[at : at + WINDOW, lanes] = lax.dot_general(
+                probs, values, (((1,), (1,)), ((), ())), preferred_element_type=jnp.float32
+            ).astype(jnp.bfloat16)
+    for target, which in ((mate_ref, 1 - core), (mine_ref, core)):
+        picked = jnp.concatenate(
+            [
+                attended[pl.ds(pl.multiple_of(at + which * piece, piece), piece), :]
+                for at in range(0, rows, WINDOW)
+            ],
+            axis=0,
+        )
+        target[...] = jnp.dot(picked, proj_ref[...], preferred_element_type=jnp.float32).astype(
+            target.dtype
+        )
+
+
+def attend_and_project(queries, sides, middle, sink_logit, out_weight, place):
+    rows, columns = queries.shape
+    depth = out_weight.shape[1]
+    low, high = sides
+    vmem = pl.BlockSpec(memory_space=pltpu.VMEM)
+    smem = pl.BlockSpec(memory_space=pltpu.SMEM)
+    half = rows // CORES
+    return pl.pallas_call(
+        attention_kernel,
+        out_shape=(
+            jax.ShapeDtypeStruct((half, depth), jnp.bfloat16),
+            jax.ShapeDtypeStruct((half, depth), jnp.float32),
+        ),
+        in_specs=[smem, smem, vmem, vmem, vmem, vmem, vmem],
+        out_specs=(vmem, vmem),
+        scratch_shapes=[
+            pltpu.VMEM((2 * HEAD_DIM, rows + 2 * WINDOW), jnp.bfloat16),
+            pltpu.VMEM((rows, columns), jnp.bfloat16),
+        ],
+        cost_estimate=pl.CostEstimate(
+            flops=2 * rows * columns * (6 * WINDOW + depth),
+            bytes_accessed=8 * half * depth,
+            transcendentals=3 * WINDOW * rows * columns // HEAD_DIM,
+        ),
+        compiler_params=pltpu.CompilerParams(vmem_limit_bytes=16 * 1024 * 1024),
+        name="attend",
+    )(place, sink_logit, queries, low, middle, high, out_weight)
 
 
 def rms_scale(mixed_rows, norm_gain):
@@ -220,9 +244,9 @@
     core = lax.axis_index("tp") % CORES
     both_axes = ("sp", "tp")
 
-    mine = joined_weights(gate_weight, up_weight, down_weight)
+    mine = jnp.concatenate([gate_weight, up_weight, down_weight.T], axis=1)
     line = lax.all_to_all(
-        mine,
+        jnp.broadcast_to(mine[None], (SIDE, *mine.shape)),
         both_axes,
         0,
         0,
@@ -234,15 +258,11 @@
         line, both_axes, axis=0, tiled=False, axis_index_groups=line_groups(sps, tps, False)
     )
 
-    joined = jnp.concatenate([key_rows, values], axis=1)
-    padded = with_halo(joined, "sp", WINDOW)
-    offset = lax.axis_index("sp") * rows_here
-    attended = attend_window(queries, padded, offset, rows_here * sps, sink_logit)
-
-    by_core = attended.reshape(xs, CORES, own, attended.shape[1])
-    even, odd = by_core[:, 0], by_core[:, 1]
-    for_me = jnp.where(core == 0, even, odd).reshape(xs * own, -1)
-    for_mate = jnp.where(core == 0, odd, even).reshape(xs * own, -1)
+    middle = jnp.concatenate([key_rows.T, values.T], axis=0)
+    sides = halo_sides(middle, "sp", WINDOW)
+    place = jnp.stack([core, lax.axis_index("sp") * rows_here, jnp.int32(rows_here * sps)]).astype(
+        jnp.int32
+    )
 
     def swap(array):
         return lax.ppermute(array, "tp", core_swap(tps))
@@ -253,11 +273,10 @@
         )
         return jnp.sum(pieces.astype(jnp.float32), axis=0)
 
-    mate_part = swap(
-        jnp.dot(for_mate, out_weight, preferred_element_type=jnp.float32).astype(jnp.bfloat16)
-    )
-    my_part = jnp.dot(for_me, out_weight, preferred_element_type=jnp.float32)
-    attn_sum = summed((my_part + mate_part.astype(jnp.float32)).astype(jnp.bfloat16))
+    mate_part, my_part = attend_and_project(
+        queries, sides, middle, sink_logit, out_weight, place
+    )
+    attn_sum = summed((my_part + swap(mate_part).astype(jnp.float32)).astype(jnp.bfloat16))
     mixed_rows = residual_in.astype(jnp.float32) + attn_sum
 
     normed = rms_scale(mixed_rows, norm_gain)

time: 139 us -> 138 us (level)
  the two profiles are of different devices: /device:TPU:248 before, /device:TPU:64 now
where the time goes in v3:
time: 138 us; the launch traced here: 137 us
  blocking collectives  82.1 us (59%)
  Pallas kernels  14.8 us (11%)
  starting transfers between devices  13.9 us (10%)
  between operations  13.6 us (10%)
  waiting for transfers between devices  9.44 us (7%)
  other arithmetic  2.07 us (1%)
    all_to_all x2, blocking collectives, summed(): lax.all_to_all(partial.reshape(xs, own, depth), 'tp', 0, 0, tiled=True, a...  38.2 us
    all_to_all x1, blocking collectives, shards(): lax.all_to_all(jnp.broadcast_to(mine[None], (SIDE, *mine.shape)), both_ax...  26.7 us
    all_to_all x1, blocking collectives, shards(): lax.all_to_all(jnp.broadcast_to(normed[None], (xs, own, depth)), 'tp', 0,...  17.2 us
    ppermute x3, starting transfers between devices, swap(): return lax.ppermute(array, 'tp', core_swap(tps))  8.02 us
    pallas_call x1, Pallas kernels, attend_and_project(): pl.pallas_call(attention_kernel, out_shape=(jax.ShapeDtypeStruct((half, d...  6.91 us
    pallas_call x1, Pallas kernels, feed_forward_first(): pl.pallas_call(functools.partial(first_kernel, hid=width // 3), out_shape...  5.16 us
    ppermute x3, waiting for transfers between devices, swap(): return lax.ppermute(array, 'tp', core_swap(tps))  4.89 us
    ppermute x1, waiting for transfers between devices, halo_sides(): low = lax.ppermute(block[:, -width:], axis, forward)  4.53 us
  transfers between devices with their start and end apart: 6, of which 3 were waited for; matrix products, arithmetic and copies ran while one was open for 1% of the time, Pallas kernels for 7%

profile of v3, /device:TPU:64, one launch (start us, length us, event | category | flops | bytes accessed | tf_op | source)
XLA Modules:
  0.0 137.1 jit_solution(8713245242255325112)
XLA Ops:
  6.5 0.0 all-gather.3.cloned.1.call-start
  6.5 0.9 concatenate.6
  7.5 0.0 copy-start.4
  7.5 0.0 copy-start.5
  7.5 0.1 broadcast_in_dim.4
  7.6 0.0 copy-start
  7.6 0.0 copy-start.1
  7.6 0.0 copy-start.2
  7.6 26.7 %all_to_all.20 = bf16[8,32,2112]{2,1,0:T(8,128)(2,1)} all-to-all(bf16[8,32,2112]{2,1,0:T(8,128)(2,1)S(1)} %broadcast_in_dim.4), channel_id=1, replica_groups={{0,8,16,24,32,40,48,56},{64,72,80,88,96,104,112,120},{128,136,144,152,1..., dimensions={0} | all-to-all | bytes 2162688 | tf_op jit(solution)/shard_map/all_to_all | solution.py:248
  34.4 0.0 all-gather.3.cloned.1.call-update
  34.4 0.1 pad_add_fusion.place_ref
  34.5 0.0 copy-done.4
  34.5 0.0 copy-done.5
  34.5 2.5 %collective-permute-start.1 = (bf16[128,128]{1,0:T(8,128)(2,1)S(1)}, bf16[128,128]{1,0:T(8,128)(2,1)S(1)}, u32[]{:S(2)}, u32[]{:S(2)}) collective-permute-start(bf16[128,128]{1,0:T(8,128)(2,1)S(1)} %get-tuple-element.21), channel_id=1, source_target_pairs={{8,0},{16,8},{24,16},{32,24},{40,32},{48,40},{56,48},{64,56},{72,6... | collective-permute-start | bytes 98312 | tf_op jit(solution)/shard_map/ppermute | solution.py:144
  37.0 3.4 %collective-permute-start = (bf16[128,128]{1,0:T(8,128)(2,1)S(1)}, bf16[128,128]{1,0:T(8,128)(2,1)S(1)}, u32[]{:S(2)}, u32[]{:S(2)}) collective-permute-start(bf16[128,128]{1,0:T(8,128)(2,1)S(1)} %get-tuple-element.22), channel_id=1, source_target_pairs={{0,8},{8,16},{16,24},{24,32},{32,40},{40,48},{48,56},{56,64},{64,7... | collective-permute-start | bytes 98312 | tf_op jit(solution)/shard_map/ppermute | solution.py:143
  40.4 0.0 collective-permute-done.1.high_ref
  40.4 4.5 %collective-permute-done.low_ref = bf16[128,128]{1,0:T(8,128)(2,1)S(1)} collective-permute-done((bf16[128,128]{1,0:T(8,128)(2,1)S(1)}, bf16[128,128]{1,0:T(8,128)(2,1)S(1)}, u32[]{:S(2)}, u32[]{:S(2)}) %collective-permute-start) | collective-permute-done | bytes 32800 | tf_op jit(solution)/shard_map/ppermute | solution.py:143
  44.9 0.0 copy-done
  44.9 0.0 copy-done.1
  44.9 0.0 copy-done.2
  44.9 6.9 %attend.1 = (bf16[256,2048]{1,0:T(8,128)(2,1)S(1)}, f32[256,2048]{1,0:T(8,128)S(1)}) custom-call(s32[3]{0:T(128)S(1)} %pad_add_fusion.place_ref, f32[4]{0:T(128)S(1)} %copy-done.2, bf16[512,256]{1,0:T(8,128)(2,1)S(1)} %copy-done.1, bf16[128,128]{1,0:T(8,128)(2,1)S(1)} %collective-permute-done.low_ref, bf16[128,512]{1,0:T(8,128)(2,1)S(1)} %pad_maximum_fusion.mid_ref, ...), custom_call_target="tpu_custom_call" | custom-call | flops 738197504 | bytes 4194304 | tf_op jit(solution)/shard_map/attend/pallas_call | solution.py:201
  51.9 4.1 %collective-permute-start.2 = (bf16[256,2048]{1,0:T(8,128)(2,1)S(1)}, bf16[256,2048]{1,0:T(8,128)(2,1)S(1)}, u32[]{:S(2)}, u32[]{:S(2)}) collective-permute-start(bf16[256,2048]{1,0:T(8,128)(2,1)S(1)} %get-tuple-element.17), channel_id=1, source_target_pairs={{0,1},{1,0},{2,3},{3,2},{4,5},{5,4},{6,7},{7,6},{8,9},{9,8},{10,11... | collective-permute-start | bytes 3145736 | tf_op jit(solution)/shard_map/ppermute | solution.py:268
  55.9 2.3 %collective-permute-done.2 = bf16[256,2048]{1,0:T(8,128)(2,1)S(1)} collective-permute-done((bf16[256,2048]{1,0:T(8,128)(2,1)S(1)}, bf16[256,2048]{1,0:T(8,128)(2,1)S(1)}, u32[]{:S(2)}, u32[]{:S(2)}) %collective-permute-start.2) | collective-permute-done | bytes 1048608 | tf_op jit(solution)/shard_map/ppermute | solution.py:268
  58.2 0.3 add_convert_fusion.1
  58.5 0.0 copy-start.3
  58.5 0.0 copy-start.6
  58.5 19.9 %all_to_all.21 = bf16[4,64,2048]{2,1,0:T(8,128)(2,1)S(1)} all-to-all(bf16[4,64,2048]{2,1,0:T(8,128)(2,1)S(1)} %bitcast.12), channel_id=1, replica_groups={{0,2,4,6},{1,3,5,7},{8,10,12,14},{9,11,13,15},{16,18,20,22},{17,19,21,2..., dimensions={0} | all-to-all | bytes 2097152 | tf_op jit(solution)/shard_map/all_to_all | solution.py:271
  78.4 0.2 convert_reduce_fusion.1
  78.5 0.0 copy-done.3
  78.6 0.2 multiply_reduce_fusion
  78.7 0.0 copy-done.6
  78.7 0.1 multiply_convert_fusion
  78.9 0.1 broadcast_in_dim.5
  79.0 17.2 %all_to_all.22 = bf16[4,64,2048]{2,1,0:T(8,128)(2,1)S(1)} all-to-all(bf16[4,64,2048]{2,1,0:T(8,128)(2,1)S(1)} %broadcast_in_dim.5), channel_id=1, replica_groups={{0,2,4,6},{1,3,5,7},{8,10,12,14},{9,11,13,15},{16,18,20,22},{17,19,21,2..., dimensions={0} | all-to-all | bytes 2097152 | tf_op jit(solution)/shard_map/all_to_all | solution.py:283
  96.2 1.9 %collective-permute-start.3 = (bf16[256,2048]{1,0:T(8,128)(2,1)S(1)}, bf16[256,2048]{1,0:T(8,128)(2,1)S(1)}, u32[]{:S(2)}, u32[]{:S(2)}) collective-permute-start(bf16[256,2048]{1,0:T(8,128)(2,1)S(1)} %bitcast.9), channel_id=1, source_target_pairs={{0,1},{1,0},{2,3},{3,2},{4,5},{5,4},{6,7},{7,6},{8,9},{9,8},{10,11... | collective-permute-start | bytes 3145736 | tf_op jit(solution)/shard_map/ppermute | solution.py:268
  98.1 2.6 %collective-permute-done.3.rows_ref = bf16[256,2048]{1,0:T(8,128)(2,1)S(1)} collective-permute-done((bf16[256,2048]{1,0:T(8,128)(2,1)S(1)}, bf16[256,2048]{1,0:T(8,128)(2,1)S(1)}, u32[]{:S(2)}, u32[]{:S(2)}) %collective-permute-start.3) | collective-permute-done | bytes 1048608 | tf_op jit(solution)/shard_map/ppermute | solution.py:268
  100.7 0.0 all-gather.3.cloned.1.call-done
  100.7 5.2 %ffn_first.1 = (bf16[256,2048]{1,0:T(8,128)(2,1)S(1)}, bf16[8,8,32,2112]{3,2,1,0:T(8,128)(2,1)S(1)}) custom-call(s32[1]{0:T(128)} %bitcast.core_ref, bf16[256,2048]{1,0:T(8,128)(2,1)S(1)} %collective-permute-done.3.rows_ref, bf16[8,8,32,2112]{3,2,1,0:T(8,128)(2,1)} %bitcast.11), custom_call_target="tpu_custom_call" | custom-call | flops 2214592512 | bytes 10747904 | tf_op jit(solution)/shard_map/ffn_first/pallas_call | solution.py:103
  105.9 2.0 %collective-permute-start.4 = (bf16[256,2048]{1,0:T(8,128)(2,1)S(1)}, bf16[256,2048]{1,0:T(8,128)(2,1)S(1)}, u32[]{:S(2)}, u32[]{:S(2)}) collective-permute-start(bf16[256,2048]{1,0:T(8,128)(2,1)S(1)} %get-tuple-element.20), channel_id=1, source_target_pairs={{0,1},{1,0},{2,3},{3,2},{4,5},{5,4},{6,7},{7,6},{8,9},{9,8},{10,11... | collective-permute-start | bytes 3145736 | tf_op jit(solution)/shard_map/ppermute | solution.py:268
  107.9 2.8 %ffn_second.1 = f32[256,2048]{1,0:T(8,128)S(1)} custom-call(bf16[256,2048]{1,0:T(8,128)(2,1)S(1)} %bitcast.10, bf16[8,8,32,2112]{3,2,1,0:T(8,128)(2,1)S(1)} %get-tuple-element.19.held), custom_call_target="tpu_custom_call" | custom-call | flops 2214592512 | bytes 10747904 | tf_op jit(solution)/shard_map/ffn_second/pallas_call | solution.py:128
  110.7 0.0 collective-permute-done.4
  110.7 0.3 add_convert_fusion
  111.0 18.3 %all_to_all.23 = bf16[4,64,2048]{2,1,0:T(8,128)(2,1)S(1)} all-to-all(bf16[4,64,2048]{2,1,0:T(8,128)(2,1)S(1)} %bitcast.13), channel_id=1, replica_groups={{0,2,4,6},{1,3,5,7},{8,10,12,14},{9,11,13,15},{16,18,20,22},{17,19,21,2..., dimensions={0} | all-to-all | bytes 2097152 | tf_op jit(solution)/shard_map/all_to_all | solution.py:271
  129.4 0.2 convert_reduce_fusion
  129.5 0.8 add_convert_fusion.2
  (3 shorter events, 0.0 us)
Async XLA Ops:
  6.5 94.2 %all-gather.3.cloned.1.call-start = ((), (), s32[]{:S(2)}) async-start(), calls=%async_computation.4 | async-start | bytes 10027008 | tf_op jit(solution)/shard_map/all_gather | solution.py:257
  7.5 27.0 %copy-start.4 = (bf16[512,64]{0,1:T(8,128)(2,1)S(1)}, bf16[512,64]{0,1:T(8,128)(2,1)}, u32[]{:S(2)}) copy-start(bf16[512,64]{0,1:T(8,128)(2,1)} %param.11) | copy-start | bytes 196612
  7.5 27.0 %copy-start.5 = (bf16[512,64]{0,1:T(8,128)(2,1)S(1)}, bf16[512,64]{0,1:T(8,128)(2,1)}, u32[]{:S(2)}) copy-start(bf16[512,64]{0,1:T(8,128)(2,1)} %param.12) | copy-start | bytes 196612
  7.6 37.3 %copy-start = (bf16[256,2048]{1,0:T(8,128)(2,1)S(1)}, bf16[256,2048]{1,0:T(8,128)(2,1)}, u32[]{:S(2)}) copy-start(bf16[256,2048]{1,0:T(8,128)(2,1)} %proj_ref.1) | copy-start | bytes 3145732
  7.6 37.3 %copy-start.1 = (bf16[512,256]{1,0:T(8,128)(2,1)S(1)}, bf16[512,256]{1,0:T(8,128)(2,1)}, u32[]{:S(2)}) copy-start(bf16[512,256]{1,0:T(8,128)(2,1)} %query_ref) | copy-start | bytes 786436
  7.6 37.3 %copy-start.2 = (f32[4]{0:T(128)S(1)}, f32[4]{0:T(128)}, u32[]{:S(2)}) copy-start(f32[4]{0:T(128)} %sink_ref.1) | copy-start | bytes 52
  34.5 5.9 %collective-permute-start.1 = (bf16[128,128]{1,0:T(8,128)(2,1)S(1)}, bf16[128,128]{1,0:T(8,128)(2,1)S(1)}, u32[]{:S(2)}, u32[]{:S(2)}) collective-permute-start(bf16[128,128]{1,0:T(8,128)(2,1)S(1)} %get-tuple-element.21), channel_id=1, source_target_pairs={{8,0},{16,8},{24,16},{32,24},{40,32},{48,40},{56,48},{64,56},{72,6... | collective-permute-start | bytes 98312 | tf_op jit(solution)/shard_map/ppermute | solution.py:144
  37.0 7.9 %collective-permute-start = (bf16[128,128]{1,0:T(8,128)(2,1)S(1)}, bf16[128,128]{1,0:T(8,128)(2,1)S(1)}, u32[]{:S(2)}, u32[]{:S(2)}) collective-permute-start(bf16[128,128]{1,0:T(8,128)(2,1)S(1)} %get-tuple-element.22), channel_id=1, source_target_pairs={{0,8},{8,16},{16,24},{24,32},{32,40},{40,48},{48,56},{56,64},{64,7... | collective-permute-start | bytes 98312 | tf_op jit(solution)/shard_map/ppermute | solution.py:143
  51.9 6.3 %collective-permute-start.2 = (bf16[256,2048]{1,0:T(8,128)(2,1)S(1)}, bf16[256,2048]{1,0:T(8,128)(2,1)S(1)}, u32[]{:S(2)}, u32[]{:S(2)}) collective-permute-start(bf16[256,2048]{1,0:T(8,128)(2,1)S(1)} %get-tuple-element.17), channel_id=1, source_target_pairs={{0,1},{1,0},{2,3},{3,2},{4,5},{5,4},{6,7},{7,6},{8,9},{9,8},{10,11... | collective-permute-start | bytes 3145736 | tf_op jit(solution)/shard_map/ppermute | solution.py:268
  58.5 20.0 %copy-start.3 = (bf16[64,2048]{1,0:T(8,128)(2,1)S(1)}, bf16[64,2048]{1,0:T(8,128)(2,1)}, u32[]{:S(2)}) copy-start(bf16[64,2048]{1,0:T(8,128)(2,1)} %param.14) | copy-start | bytes 786436
  58.5 20.2 %copy-start.6 = (f32[2048]{0:T(1024)S(1)}, f32[2048]{0:T(1024)}, u32[]{:S(2)}) copy-start(f32[2048]{0:T(1024)} %param.16) | copy-start | bytes 24580
  96.2 4.5 %collective-permute-start.3 = (bf16[256,2048]{1,0:T(8,128)(2,1)S(1)}, bf16[256,2048]{1,0:T(8,128)(2,1)S(1)}, u32[]{:S(2)}, u32[]{:S(2)}) collective-permute-start(bf16[256,2048]{1,0:T(8,128)(2,1)S(1)} %bitcast.9), channel_id=1, source_target_pairs={{0,1},{1,0},{2,3},{3,2},{4,5},{5,4},{6,7},{7,6},{8,9},{9,8},{10,11... | collective-permute-start | bytes 3145736 | tf_op jit(solution)/shard_map/ppermute | solution.py:268
  105.9 4.8 %collective-permute-start.4 = (bf16[256,2048]{1,0:T(8,128)(2,1)S(1)}, bf16[256,2048]{1,0:T(8,128)(2,1)S(1)}, u32[]{:S(2)}, u32[]{:S(2)}) collective-permute-start(bf16[256,2048]{1,0:T(8,128)(2,1)S(1)} %get-tuple-element.20), channel_id=1, source_target_pairs={{0,1},{1,0},{2,3},{3,2},{4,5},{5,4},{6,7},{7,6},{8,9},{9,8},{10,11... | collective-permute-start | bytes 3145736 | tf_op jit(solution)/shard_map/ppermute | solution.py:268
Sparse Core Ops, SparseCore 0:
  34.5 57.5 all-gather.2

commit v4 on v3

--- a/solution.py
+++ b/solution.py
@@ -51,21 +51,23 @@
     span = per * SIDE * piece
     core = core_ref[0]
 
-    def copy(i, swapped):
-        source = weights_ref.at[:, i] if swapped else weights_ref.at[i]
-        return pltpu.make_async_copy(source, held.at[i], sems.at[i])
+    def copy(i, swapped, part):
+        columns = (pl.ds(0, 2 * hid), pl.ds(2 * hid, hid))[part]
+        source = weights_ref.at[:, i, :, columns] if swapped else weights_ref.at[i, :, :, columns]
+        return pltpu.make_async_copy(source, held.at[i, :, :, columns], sems.at[part, i])
 
     for swapped in (False, True):
 
         @pl.when(core == int(swapped))
         def _():
-            for i in range(SIDE):
-                copy(i, swapped).start()
+            for part in range(2):
+                for i in range(SIDE):
+                    copy(i, swapped, part).start()
 
     both = None
     for step in range(SIDE // per):
         for i in range(step * per, (step + 1) * per):
-            copy(i, False).wait()
+            copy(i, False, 0).wait()
         tile = held[step * per : (step + 1) * per, :, :, : 2 * hid].reshape(span, 2 * hid)
         part = jnp.dot(
             rows_ref[:, step * span : (step + 1) * span], tile, preferred_element_type=jnp.float32
@@ -76,8 +78,11 @@
             total[...] += part
         else:
             both = total[...] + part
+    hidden = gated_product(both, hid)
+    for i in range(SIDE):
+        copy(i, False, 1).wait()
     down = held[:, :, :, 2 * hid :].reshape(-1, hid)
-    out_ref[...] = down_product(gated_product(both, hid), down).astype(out_ref.dtype)
+    out_ref[...] = down_product(hidden, down).astype(out_ref.dtype)
 
 
 def second_kernel(rows_ref, held, out_ref, *, hid):
@@ -114,7 +119,7 @@
         out_specs=(vmem, vmem),
         scratch_shapes=[
             pltpu.VMEM((count, 2 * width // 3), jnp.float32),
-            pltpu.SemaphoreType.DMA((SIDE,)),
+            pltpu.SemaphoreType.DMA((2, SIDE)),
         ],
         cost_estimate=ffn_cost(rows, width),
         compiler_params=pltpu.CompilerParams(vmem_limit_bytes=FIRST_VMEM),
@@ -158,26 +163,31 @@
     query_at = lax.broadcasted_iota(jnp.int32, (WINDOW, 3 * WINDOW), 0)
     key_at = lax.broadcasted_iota(jnp.int32, (WINDOW, 3 * WINDOW), 1)
     near = (key_at >= query_at) & (key_at <= query_at + 2 * WINDOW)
+    sink = jnp.concatenate(
+        [jnp.full((WINDOW, 1), sink_ref[head], jnp.float32) for head in range(heads)], axis=0
+    )
     for block in range(rows // WINDOW):
         at = block * WINDOW
         position = key_at + (start + at - WINDOW)
         valid = near & (position >= 0) & (position < total)
         keys = padded[:HEAD_DIM, at : at + 3 * WINDOW]
         values = padded[HEAD_DIM:, at : at + 3 * WINDOW]
-        for head in range(heads):
-            lanes = slice(head * HEAD_DIM, (head + 1) * HEAD_DIM)
-            scores = jnp.dot(
-                query_ref[at : at + WINDOW, lanes], keys, preferred_element_type=jnp.float32
-            ) * HEAD_DIM ** (-0.5)
-            scores = jnp.where(valid, scores, -1e30)
-            sink = sink_ref[head]
-            peak = jnp.maximum(jnp.max(scores, axis=1, keepdims=True), sink)
-            raw = jnp.exp(scores - peak)
-            denom = jnp.sum(raw, axis=1, keepdims=True) + jnp.exp(sink - peak)
-            probs = (raw * (1.0 / denom)).astype(jnp.bfloat16)
-            attended[at : at + WINDOW, lanes] = lax.dot_general(
-                probs, values, (((1,), (1,)), ((), ())), preferred_element_type=jnp.float32
-            ).astype(jnp.bfloat16)
+        scaled = query_ref[at : at + WINDOW, :] * jnp.bfloat16(HEAD_DIM ** (-0.5))
+        stacked = jnp.concatenate(
+            [scaled[:, head * HEAD_DIM : (head + 1) * HEAD_DIM] for head in range(heads)], axis=0
+        )
+        scores = jnp.dot(stacked, keys, preferred_element_type=jnp.float32)
+        scores = jnp.where(jnp.concatenate([valid] * heads, axis=0), scores, -1e30)
+        peak = jnp.maximum(jnp.max(scores, axis=1, keepdims=True), sink)
+        raw = jnp.exp(scores - peak)
+        denom = jnp.sum(raw, axis=1, keepdims=True) + jnp.exp(sink - peak)
+        probs = (raw * (1.0 / denom)).astype(jnp.bfloat16)
+        mixed = lax.dot_general(
+            probs, values, (((1,), (1,)), ((), ())), preferred_element_type=jnp.float32
+        ).astype(jnp.bfloat16)
+        attended[at : at + WINDOW, :] = jnp.concatenate(
+            [mixed[head * WINDOW : (head + 1) * WINDOW] for head in range(heads)], axis=1
+        )
     for target, which in ((mate_ref, 1 - core), (mine_ref, core)):
         picked = jnp.concatenate(
             [
@@ -220,9 +230,46 @@
     )(place, sink_logit, queries, low, middle, high, out_weight)
 
 
-def rms_scale(mixed_rows, norm_gain):
-    inverse = lax.rsqrt(jnp.mean(mixed_rows * mixed_rows, axis=-1, keepdims=True) + 1e-06)
-    return (mixed_rows * inverse * norm_gain).astype(jnp.bfloat16)
+def norm_kernel(pieces_ref, residual_ref, gain_ref, mixed_ref, spread_ref):
+    mixed = residual_ref[...].astype(jnp.float32)
+    mixed += jnp.sum(pieces_ref[...].astype(jnp.float32), axis=0)
+    mixed_ref[...] = mixed
+    inverse = lax.rsqrt(jnp.mean(mixed * mixed, axis=1, keepdims=True) + 1e-06)
+    normed = (mixed * inverse * gain_ref[...]).astype(spread_ref.dtype)
+    for i in range(spread_ref.shape[0]):
+        spread_ref[i] = normed
+
+
+def sum_and_norm(pieces, residual, norm_gain):
+    vmem = pl.BlockSpec(memory_space=pltpu.VMEM)
+    return pl.pallas_call(
+        norm_kernel,
+        out_shape=(
+            jax.ShapeDtypeStruct(residual.shape, jnp.float32),
+            jax.ShapeDtypeStruct(pieces.shape, residual.dtype),
+        ),
+        in_specs=[vmem] * 3,
+        out_specs=(vmem, vmem),
+        compiler_params=pltpu.CompilerParams(vmem_limit_bytes=8 * 1024 * 1024),
+        name="norm",
+    )(pieces, residual, norm_gain.reshape(1, -1))
+
+
+def last_kernel(pieces_ref, mixed_ref, out_ref):
+    total = mixed_ref[...] + jnp.sum(pieces_ref[...].astype(jnp.float32), axis=0)
+    out_ref[...] = total.astype(out_ref.dtype)
+
+
+def last_sum(pieces, mixed):
+    vmem = pl.BlockSpec(memory_space=pltpu.VMEM)
+    return pl.pallas_call(
+        last_kernel,
+        out_shape=jax.ShapeDtypeStruct(mixed.shape, pieces.dtype),
+        in_specs=[vmem] * 2,
+        out_specs=vmem,
+        compiler_params=pltpu.CompilerParams(vmem_limit_bytes=8 * 1024 * 1024),
+        name="last",
+    )(pieces, mixed)
 
 
 def shards(
@@ -267,34 +314,24 @@
     def swap(array):
         return lax.ppermute(array, "tp", core_swap(tps))
 
-    def summed(partial):
-        pieces = lax.all_to_all(
-            partial.reshape(xs, own, depth), "tp", 0, 0, tiled=True, axis_index_groups=x_groups(tps)
-        )
-        return jnp.sum(pieces.astype(jnp.float32), axis=0)
+    def exchange(blocks):
+        return lax.all_to_all(
+            blocks.reshape(xs, own, depth), "tp", 0, 0, tiled=True, axis_index_groups=x_groups(tps)
+        )
+
+    def added(mine, mates):
+        return exchange((mine + mates.astype(jnp.float32)).astype(jnp.bfloat16))
 
     mate_part, my_part = attend_and_project(
         queries, sides, middle, sink_logit, out_weight, place
     )
-    attn_sum = summed((my_part + swap(mate_part).astype(jnp.float32)).astype(jnp.bfloat16))
-    mixed_rows = residual_in.astype(jnp.float32) + attn_sum
-
-    normed = rms_scale(mixed_rows, norm_gain)
-    my_rows = lax.all_to_all(
-        jnp.broadcast_to(normed[None], (xs, own, depth)),
-        "tp",
-        0,
-        0,
-        tiled=True,
-        axis_index_groups=x_groups(tps),
-    ).reshape(xs * own, depth)
+    mixed_rows, spread = sum_and_norm(added(my_part, swap(mate_part)), residual_in, norm_gain)
+    my_rows = exchange(spread).reshape(xs * own, depth)
     mate_rows = swap(my_rows)
-    core_scalar = core.astype(jnp.int32).reshape(1)
-    mate_out, held = feed_forward_first(mate_rows, weights, core_scalar)
+    mate_out, held = feed_forward_first(mate_rows, weights, core.astype(jnp.int32).reshape(1))
     mate_sum = swap(mate_out)
     my_out = feed_forward_second(my_rows, held)
-    ffn_sum = summed((my_out + mate_sum.astype(jnp.float32)).astype(jnp.bfloat16))
-    return (mixed_rows + ffn_sum).astype(jnp.bfloat16)
+    return last_sum(added(my_out, mate_sum), mixed_rows)
 
 
 def solution(mesh):

time: 138 us -> 135 us (0.978)
    pallas_call x1, Pallas kernels: 6.91 us -> 5.35 us  [attend_and_project(): pl.pallas_call(attention_kernel, out_shape=(jax.ShapeDtypeStruct((half, d...]
  transfers between devices with their start and end apart: 6 -> 6, of which waited for: 3 -> 3; matrix products, arithmetic and copies ran while one was open for 1% -> 0% of each run, Pallas kernels for 7% -> 6%
where the time goes in v4:
time: 135 us
  blocking collectives  82.1 us (61%)
  Pallas kernels  14.2 us (11%)
  starting transfers between devices  13.9 us (10%)
  between operations  13.6 us (10%)
  waiting for transfers between devices  9.45 us (7%)
    all_to_all x3, blocking collectives, exchange(): lax.all_to_all(blocks.reshape(xs, own, depth), 'tp', 0, 0, tiled=True, ax...  55.4 us
    all_to_all x1, blocking collectives, shards(): lax.all_to_all(jnp.broadcast_to(mine[None], (SIDE, *mine.shape)), both_ax...  26.7 us
    ppermute x3, starting transfers between devices, swap(): return lax.ppermute(array, 'tp', core_swap(tps))  8.03 us
    pallas_call x1, Pallas kernels, attend_and_project(): pl.pallas_call(attention_kernel, out_shape=(jax.ShapeDtypeStruct((half, d...  5.35 us
    pallas_call x1, Pallas kernels, feed_forward_first(): pl.pallas_call(functools.partial(first_kernel, hid=width // 3), out_shape...  4.93 us
    ppermute x3, waiting for transfers between devices, swap(): return lax.ppermute(array, 'tp', core_swap(tps))  4.89 us
    ppermute x1, waiting for transfers between devices, halo_sides(): low = lax.ppermute(block[:, -width:], axis, forward)  4.54 us
    ppermute x1, starting transfers between devices, halo_sides(): low = lax.ppermute(block[:, -width:], axis, forward)  3.34 us
  transfers between devices with their start and end apart: 6, of which 3 were waited for; matrix products, arithmetic and copies ran while one was open for 0% of the time, Pallas kernels for 6%

profile of v4, /device:TPU:64, one launch (start us, length us, event | category | flops | bytes accessed | tf_op | source)
XLA Modules:
  0.0 135.0 jit_solution(11495690910141047426)
XLA Ops:
  6.5 0.0 all-gather.3.cloned.1.call-start
  6.5 0.9 concatenate.6
  7.5 0.0 copy-start.5
  7.5 0.0 copy-start.6
  7.5 0.1 broadcast_in_dim.2
  7.6 0.0 copy-start.2
  7.6 0.0 copy-start.3
  7.6 0.0 copy-start.4
  7.6 26.7 %all_to_all.20 = bf16[8,32,2112]{2,1,0:T(8,128)(2,1)} all-to-all(bf16[8,32,2112]{2,1,0:T(8,128)(2,1)S(1)} %broadcast_in_dim.2), channel_id=1, replica_groups={{0,8,16,24,32,40,48,56},{64,72,80,88,96,104,112,120},{128,136,144,152,1..., dimensions={0} | all-to-all | bytes 2162688 | tf_op jit(solution)/shard_map/all_to_all | solution.py:295
  34.4 0.0 all-gather.3.cloned.1.call-update
  34.4 0.1 pad_add_fusion.place_ref
  34.5 0.0 copy-done.5
  34.5 0.0 copy-done.6
  34.5 2.5 %collective-permute-start.1 = (bf16[128,128]{1,0:T(8,128)(2,1)S(1)}, bf16[128,128]{1,0:T(8,128)(2,1)S(1)}, u32[]{:S(2)}, u32[]{:S(2)}) collective-permute-start(bf16[128,128]{1,0:T(8,128)(2,1)S(1)} %get-tuple-element.25), channel_id=1, source_target_pairs={{8,0},{16,8},{24,16},{32,24},{40,32},{48,40},{56,48},{64,56},{72,6... | collective-permute-start | bytes 98312 | tf_op jit(solution)/shard_map/ppermute | solution.py:149
  37.0 3.3 %collective-permute-start = (bf16[128,128]{1,0:T(8,128)(2,1)S(1)}, bf16[128,128]{1,0:T(8,128)(2,1)S(1)}, u32[]{:S(2)}, u32[]{:S(2)}) collective-permute-start(bf16[128,128]{1,0:T(8,128)(2,1)S(1)} %get-tuple-element.26), channel_id=1, source_target_pairs={{0,8},{8,16},{16,24},{24,32},{32,40},{40,48},{48,56},{56,64},{64,7... | collective-permute-start | bytes 98312 | tf_op jit(solution)/shard_map/ppermute | solution.py:148
  40.4 0.0 collective-permute-done.1.high_ref
  40.4 4.5 %collective-permute-done.low_ref = bf16[128,128]{1,0:T(8,128)(2,1)S(1)} collective-permute-done((bf16[128,128]{1,0:T(8,128)(2,1)S(1)}, bf16[128,128]{1,0:T(8,128)(2,1)S(1)}, u32[]{:S(2)}, u32[]{:S(2)}) %collective-permute-start) | collective-permute-done | bytes 32800 | tf_op jit(solution)/shard_map/ppermute | solution.py:148
  44.9 0.0 copy-done.2
  44.9 0.0 copy-done.3
  44.9 0.0 copy-done.4
  44.9 5.4 %attend.1 = (bf16[256,2048]{1,0:T(8,128)(2,1)S(1)}, f32[256,2048]{1,0:T(8,128)S(1)}) custom-call(s32[3]{0:T(128)S(1)} %pad_add_fusion.place_ref, f32[4]{0:T(128)S(1)} %copy-done.4, bf16[512,256]{1,0:T(8,128)(2,1)S(1)} %copy-done.3, bf16[128,128]{1,0:T(8,128)(2,1)S(1)} %collective-permute-done.low_ref, bf16[128,512]{1,0:T(8,128)(2,1)S(1)} %pad_maximum_fusion.mid_ref, ...), custom_call_target="tpu_custom_call" | custom-call | flops 738197504 | bytes 4194304 | tf_op jit(solution)/shard_map/attend/pallas_call | solution.py:211
  50.3 4.1 %collective-permute-start.2 = (bf16[256,2048]{1,0:T(8,128)(2,1)S(1)}, bf16[256,2048]{1,0:T(8,128)(2,1)S(1)}, u32[]{:S(2)}, u32[]{:S(2)}) collective-permute-start(bf16[256,2048]{1,0:T(8,128)(2,1)S(1)} %get-tuple-element.19), channel_id=1, source_target_pairs={{0,1},{1,0},{2,3},{3,2},{4,5},{5,4},{6,7},{7,6},{8,9},{9,8},{10,11... | collective-permute-start | bytes 3145736 | tf_op jit(solution)/shard_map/ppermute | solution.py:315
  54.4 2.3 %collective-permute-done.2 = bf16[256,2048]{1,0:T(8,128)(2,1)S(1)} collective-permute-done((bf16[256,2048]{1,0:T(8,128)(2,1)S(1)}, bf16[256,2048]{1,0:T(8,128)(2,1)S(1)}, u32[]{:S(2)}, u32[]{:S(2)}) %collective-permute-start.2) | collective-permute-done | bytes 1048608 | tf_op jit(solution)/shard_map/ppermute | solution.py:315
  56.6 0.3 add_convert_fusion.1
  56.9 0.0 copy-start
  57.0 0.0 copy-start.1
  57.0 19.9 %all_to_all.21.pieces_ref = bf16[4,64,2048]{2,1,0:T(8,128)(2,1)S(1)} all-to-all(bf16[4,64,2048]{2,1,0:T(8,128)(2,1)S(1)} %bitcast.14), channel_id=1, replica_groups={{0,2,4,6},{1,3,5,7},{8,10,12,14},{9,11,13,15},{16,18,20,22},{17,19,21,2..., dimensions={0} | all-to-all | bytes 2097152 | tf_op jit(solution)/shard_map/all_to_all | solution.py:318
  76.8 0.0 copy-done
  76.8 0.0 copy-done.1
  76.8 0.3 norm.1
  77.2 17.2 %all_to_all.22 = bf16[4,64,2048]{2,1,0:T(8,128)(2,1)S(1)} all-to-all(bf16[4,64,2048]{2,1,0:T(8,128)(2,1)S(1)} %get-tuple-element.20), channel_id=1, replica_groups={{0,2,4,6},{1,3,5,7},{8,10,12,14},{9,11,13,15},{16,18,20,22},{17,19,21,2..., dimensions={0} | all-to-all | bytes 2097152 | tf_op jit(solution)/shard_map/all_to_all | solution.py:318
  94.4 1.9 %collective-permute-start.3 = (bf16[256,2048]{1,0:T(8,128)(2,1)S(1)}, bf16[256,2048]{1,0:T(8,128)(2,1)S(1)}, u32[]{:S(2)}, u32[]{:S(2)}) collective-permute-start(bf16[256,2048]{1,0:T(8,128)(2,1)S(1)} %bitcast.10), channel_id=1, source_target_pairs={{0,1},{1,0},{2,3},{3,2},{4,5},{5,4},{6,7},{7,6},{8,9},{9,8},{10,11... | collective-permute-start | bytes 3145736 | tf_op jit(solution)/shard_map/ppermute | solution.py:315
  96.3 2.6 %collective-permute-done.3.rows_ref = bf16[256,2048]{1,0:T(8,128)(2,1)S(1)} collective-permute-done((bf16[256,2048]{1,0:T(8,128)(2,1)S(1)}, bf16[256,2048]{1,0:T(8,128)(2,1)S(1)}, u32[]{:S(2)}, u32[]{:S(2)}) %collective-permute-start.3) | collective-permute-done | bytes 1048608 | tf_op jit(solution)/shard_map/ppermute | solution.py:315
  98.9 0.0 all-gather.3.cloned.1.call-done
  98.9 4.9 %ffn_first.1 = (bf16[256,2048]{1,0:T(8,128)(2,1)S(1)}, bf16[8,8,32,2112]{3,2,1,0:T(8,128)(2,1)S(1)}) custom-call(s32[1]{0:T(128)} %bitcast.core_ref, bf16[256,2048]{1,0:T(8,128)(2,1)S(1)} %collective-permute-done.3.rows_ref, bf16[8,8,32,2112]{3,2,1,0:T(8,128)(2,1)} %bitcast.13), custom_call_target="tpu_custom_call" | custom-call | flops 2214592512 | bytes 10747904 | tf_op jit(solution)/shard_map/ffn_first/pallas_call | solution.py:108
  103.8 2.0 %collective-permute-start.4 = (bf16[256,2048]{1,0:T(8,128)(2,1)S(1)}, bf16[256,2048]{1,0:T(8,128)(2,1)S(1)}, u32[]{:S(2)}, u32[]{:S(2)}) collective-permute-start(bf16[256,2048]{1,0:T(8,128)(2,1)S(1)} %get-tuple-element.23), channel_id=1, source_target_pairs={{0,1},{1,0},{2,3},{3,2},{4,5},{5,4},{6,7},{7,6},{8,9},{9,8},{10,11... | collective-permute-start | bytes 3145736 | tf_op jit(solution)/shard_map/ppermute | solution.py:315
  105.9 2.8 %ffn_second.1 = f32[256,2048]{1,0:T(8,128)S(1)} custom-call(bf16[256,2048]{1,0:T(8,128)(2,1)S(1)} %bitcast.11, bf16[8,8,32,2112]{3,2,1,0:T(8,128)(2,1)S(1)} %get-tuple-element.22.held), custom_call_target="tpu_custom_call" | custom-call | flops 2214592512 | bytes 10747904 | tf_op jit(solution)/shard_map/ffn_second/pallas_call | solution.py:133
  108.7 0.0 collective-permute-done.4
  108.7 0.3 add_convert_fusion
  109.0 18.3 %all_to_all.23.pieces_ref = bf16[4,64,2048]{2,1,0:T(8,128)(2,1)S(1)} all-to-all(bf16[4,64,2048]{2,1,0:T(8,128)(2,1)S(1)} %bitcast.15), channel_id=1, replica_groups={{0,2,4,6},{1,3,5,7},{8,10,12,14},{9,11,13,15},{16,18,20,22},{17,19,21,2..., dimensions={0} | all-to-all | bytes 2097152 | tf_op jit(solution)/shard_map/all_to_all | solution.py:318
  127.3 0.8 last.1
  (2 shorter events, 0.0 us)
Async XLA Ops:
  6.5 92.4 %all-gather.3.cloned.1.call-start = ((), (), s32[]{:S(2)}) async-start(), calls=%async_computation.4 | async-start | bytes 10027008 | tf_op jit(solution)/shard_map/all_gather | solution.py:304
  7.5 27.0 %copy-start.5 = (bf16[512,64]{0,1:T(8,128)(2,1)S(1)}, bf16[512,64]{0,1:T(8,128)(2,1)}, u32[]{:S(2)}) copy-start(bf16[512,64]{0,1:T(8,128)(2,1)} %param.11) | copy-start | bytes 196612
  7.5 27.0 %copy-start.6 = (bf16[512,64]{0,1:T(8,128)(2,1)S(1)}, bf16[512,64]{0,1:T(8,128)(2,1)}, u32[]{:S(2)}) copy-start(bf16[512,64]{0,1:T(8,128)(2,1)} %param.12) | copy-start | bytes 196612
  7.6 37.3 %copy-start.2 = (bf16[256,2048]{1,0:T(8,128)(2,1)S(1)}, bf16[256,2048]{1,0:T(8,128)(2,1)}, u32[]{:S(2)}) copy-start(bf16[256,2048]{1,0:T(8,128)(2,1)} %proj_ref.1) | copy-start | bytes 3145732
  7.6 37.3 %copy-start.3 = (bf16[512,256]{1,0:T(8,128)(2,1)S(1)}, bf16[512,256]{1,0:T(8,128)(2,1)}, u32[]{:S(2)}) copy-start(bf16[512,256]{1,0:T(8,128)(2,1)} %query_ref) | copy-start | bytes 786436
  7.6 37.3 %copy-start.4 = (f32[4]{0:T(128)S(1)}, f32[4]{0:T(128)}, u32[]{:S(2)}) copy-start(f32[4]{0:T(128)} %sink_ref.1) | copy-start | bytes 52
  34.5 5.9 %collective-permute-start.1 = (bf16[128,128]{1,0:T(8,128)(2,1)S(1)}, bf16[128,128]{1,0:T(8,128)(2,1)S(1)}, u32[]{:S(2)}, u32[]{:S(2)}) collective-permute-start(bf16[128,128]{1,0:T(8,128)(2,1)S(1)} %get-tuple-element.25), channel_id=1, source_target_pairs={{8,0},{16,8},{24,16},{32,24},{40,32},{48,40},{56,48},{64,56},{72,6... | collective-permute-start | bytes 98312 | tf_op jit(solution)/shard_map/ppermute | solution.py:149
  37.0 7.9 %collective-permute-start = (bf16[128,128]{1,0:T(8,128)(2,1)S(1)}, bf16[128,128]{1,0:T(8,128)(2,1)S(1)}, u32[]{:S(2)}, u32[]{:S(2)}) collective-permute-start(bf16[128,128]{1,0:T(8,128)(2,1)S(1)} %get-tuple-element.26), channel_id=1, source_target_pairs={{0,8},{8,16},{16,24},{24,32},{32,40},{40,48},{48,56},{56,64},{64,7... | collective-permute-start | bytes 98312 | tf_op jit(solution)/shard_map/ppermute | solution.py:148
  50.3 6.3 %collective-permute-start.2 = (bf16[256,2048]{1,0:T(8,128)(2,1)S(1)}, bf16[256,2048]{1,0:T(8,128)(2,1)S(1)}, u32[]{:S(2)}, u32[]{:S(2)}) collective-permute-start(bf16[256,2048]{1,0:T(8,128)(2,1)S(1)} %get-tuple-element.19), channel_id=1, source_target_pairs={{0,1},{1,0},{2,3},{3,2},{4,5},{5,4},{6,7},{7,6},{8,9},{9,8},{10,11... | collective-permute-start | bytes 3145736 | tf_op jit(solution)/shard_map/ppermute | solution.py:315
  56.9 19.9 %copy-start = (bf16[64,2048]{1,0:T(8,128)(2,1)S(1)}, bf16[64,2048]{1,0:T(8,128)(2,1)}, u32[]{:S(2)}) copy-start(bf16[64,2048]{1,0:T(8,128)(2,1)} %residual_ref.1) | copy-start | bytes 786436
  57.0 19.9 %copy-start.1 = (f32[2048]{0:T(1024)S(1)}, f32[2048]{0:T(1024)}, u32[]{:S(2)}) copy-start(f32[2048]{0:T(1024)} %param.16) | copy-start | bytes 24580
  94.4 4.5 %collective-permute-start.3 = (bf16[256,2048]{1,0:T(8,128)(2,1)S(1)}, bf16[256,2048]{1,0:T(8,128)(2,1)S(1)}, u32[]{:S(2)}, u32[]{:S(2)}) collective-permute-start(bf16[256,2048]{1,0:T(8,128)(2,1)S(1)} %bitcast.10), channel_id=1, source_target_pairs={{0,1},{1,0},{2,3},{3,2},{4,5},{5,4},{6,7},{7,6},{8,9},{9,8},{10,11... | collective-permute-start | bytes 3145736 | tf_op jit(solution)/shard_map/ppermute | solution.py:315
  103.8 4.8 %collective-permute-start.4 = (bf16[256,2048]{1,0:T(8,128)(2,1)S(1)}, bf16[256,2048]{1,0:T(8,128)(2,1)S(1)}, u32[]{:S(2)}, u32[]{:S(2)}) collective-permute-start(bf16[256,2048]{1,0:T(8,128)(2,1)S(1)} %get-tuple-element.23), channel_id=1, source_target_pairs={{0,1},{1,0},{2,3},{3,2},{4,5},{5,4},{6,7},{7,6},{8,9},{9,8},{10,11... | collective-permute-start | bytes 3145736 | tf_op jit(solution)/shard_map/ppermute | solution.py:315
Sparse Core Ops, SparseCore 0:
  34.5 57.4 all-gather.2

commit v5 on v4

--- a/solution.py
+++ b/solution.py
@@ -11,6 +11,7 @@
 WINDOW = 128
 SIDE = 8
 CORES = 2
+LANES = 128
 FIRST_VMEM = 40 * 1024 * 1024
 
 
@@ -36,6 +37,48 @@
     return [(i, i ^ 1) for i in range(tps)]
 
 
+def pack_kernel(joined_ref, out_ref):
+    piece, width = joined_ref.shape
+    whole = width // LANES
+    rows = [joined_ref[:, i * LANES : (i + 1) * LANES] for i in range(whole)]
+    last = joined_ref[:, whole * LANES :]
+    rows.append(jnp.concatenate([last[: piece // 2], last[piece // 2 :]], axis=1))
+    packed = jnp.concatenate(rows, axis=0)
+    for i in range(out_ref.shape[0]):
+        out_ref[i] = packed
+
+
+def pack_copies(joined):
+    piece, width = joined.shape
+    vmem = pl.BlockSpec(memory_space=pltpu.VMEM)
+    return pl.pallas_call(
+        pack_kernel,
+        out_shape=jax.ShapeDtypeStruct((SIDE, piece * width // LANES, LANES), joined.dtype),
+        in_specs=[vmem],
+        out_specs=vmem,
+        compiler_params=pltpu.CompilerParams(vmem_limit_bytes=4 * 1024 * 1024),
+        name="pack",
+    )(joined)
+
+
+def gate_up(held, first, count, piece, hid):
+    tiles = [
+        held[first : first + count, :, i * piece : (i + 1) * piece, :].reshape(-1, LANES)
+        for i in range(2 * hid // LANES)
+    ]
+    return jnp.concatenate(tiles, axis=1)
+
+
+def down_matrix(held, piece, hid):
+    tiles = [
+        held[:, :, i * piece : (i + 1) * piece, :].reshape(-1, LANES)
+        for i in range(2 * hid // LANES, 3 * hid // LANES)
+    ]
+    last = held[:, :, 3 * hid // LANES * piece :, :].reshape(SIDE * SIDE, piece // 2, LANES)
+    last = jnp.concatenate([last[:, :, : LANES // 2], last[:, :, LANES // 2 :]], axis=1)
+    return jnp.concatenate(tiles + [last.reshape(-1, LANES // 2)], axis=1)
+
+
 def gated_product(both, hid):
     gate, up = both[:, :hid], both[:, hid:]
     return (gate / (1.0 + jnp.exp(-gate)) * up).astype(jnp.bfloat16)
@@ -45,16 +88,16 @@
     return lax.dot_general(hidden, down, (((1,), (1,)), ((), ())), preferred_element_type=jnp.float32)
 
 
-def first_kernel(core_ref, rows_ref, weights_ref, out_ref, held, total, sems, *, hid):
-    piece = held.shape[2]
+def first_kernel(core_ref, rows_ref, weights_ref, out_ref, held, total, sems, *, piece, hid):
     per = 2
     span = per * SIDE * piece
+    down_at = 2 * hid // LANES * piece
     core = core_ref[0]
 
     def copy(i, swapped, part):
-        columns = (pl.ds(0, 2 * hid), pl.ds(2 * hid, hid))[part]
-        source = weights_ref.at[:, i, :, columns] if swapped else weights_ref.at[i, :, :, columns]
-        return pltpu.make_async_copy(source, held.at[i, :, :, columns], sems.at[part, i])
+        lines = (pl.ds(0, down_at), pl.ds(down_at, held.shape[2] - down_at))[part]
+        source = weights_ref.at[:, i, lines] if swapped else weights_ref.at[i, :, lines]
+        return pltpu.make_async_copy(source, held.at[i, :, lines], sems.at[part, i])
 
     for swapped in (False, True):
 
@@ -68,9 +111,10 @@
     for step in range(SIDE // per):
         for i in range(step * per, (step + 1) * per):
             copy(i, False, 0).wait()
-        tile = held[step * per : (step + 1) * per, :, :, : 2 * hid].reshape(span, 2 * hid)
         part = jnp.dot(
-            rows_ref[:, step * span : (step + 1) * span], tile, preferred_element_type=jnp.float32
+            rows_ref[:, step * span : (step + 1) * span],
+            gate_up(held, step * per, per, piece, hid),
+            preferred_element_type=jnp.float32,
         )
         if step == 0:
             total[...] = part
@@ -81,15 +125,16 @@
     hidden = gated_product(both, hid)
     for i in range(SIDE):
         copy(i, False, 1).wait()
-    down = held[:, :, :, 2 * hid :].reshape(-1, hid)
-    out_ref[...] = down_product(hidden, down).astype(out_ref.dtype)
-
-
-def second_kernel(rows_ref, held, out_ref, *, hid):
-    tile = held[:, :, :, : 2 * hid].reshape(-1, 2 * hid)
-    both = jnp.dot(rows_ref[...], tile, preferred_element_type=jnp.float32)
-    down = held[:, :, :, 2 * hid :].reshape(-1, hid)
-    out_ref[...] = down_product(gated_product(both, hid), down).astype(out_ref.dtype)
+    out_ref[...] = down_product(hidden, down_matrix(held, piece, hid)).astype(out_ref.dtype)
+
+
+def second_kernel(rows_ref, held, out_ref, *, piece, hid):
+    both = jnp.dot(
+        rows_ref[...], gate_up(held, 0, SIDE, piece, hid), preferred_element_type=jnp.float32
+    )
+    out_ref[...] = down_product(gated_product(both, hid), down_matrix(held, piece, hid)).astype(
+        out_ref.dtype
+    )
 
 
 def ffn_cost(rows, width):
@@ -101,12 +146,11 @@
     )
 
 
-def feed_forward_first(rows, weights, core):
+def feed_forward_first(rows, weights, core, piece, width):
     count, depth = rows.shape
-    width = weights.shape[3]
-    vmem = pl.BlockSpec(memory_space=pltpu.VMEM)
-    return pl.pallas_call(
-        functools.partial(first_kernel, hid=width // 3),
+    vmem = pl.BlockSpec(memory_space=pltpu.VMEM)
+    return pl.pallas_call(
+        functools.partial(first_kernel, piece=piece, hid=width // 3),
         out_shape=(
             jax.ShapeDtypeStruct((count, depth), jnp.bfloat16),
             jax.ShapeDtypeStruct(weights.shape, weights.dtype),
@@ -127,11 +171,10 @@
     )(core, rows, weights)
 
 
-def feed_forward_second(rows, held):
-    width = held.shape[3]
-    vmem = pl.BlockSpec(memory_space=pltpu.VMEM)
-    return pl.pallas_call(
-        functools.partial(second_kernel, hid=width // 3),
+def feed_forward_second(rows, held, piece, width):
+    vmem = pl.BlockSpec(memory_space=pltpu.VMEM)
+    return pl.pallas_call(
+        functools.partial(second_kernel, piece=piece, hid=width // 3),
         out_shape=jax.ShapeDtypeStruct(rows.shape, jnp.float32),
         in_specs=[vmem, vmem],
         out_specs=vmem,
@@ -293,7 +336,7 @@
 
     mine = jnp.concatenate([gate_weight, up_weight, down_weight.T], axis=1)
     line = lax.all_to_all(
-        jnp.broadcast_to(mine[None], (SIDE, *mine.shape)),
+        pack_copies(mine),
         both_axes,
         0,
         0,
@@ -328,9 +371,11 @@
     mixed_rows, spread = sum_and_norm(added(my_part, swap(mate_part)), residual_in, norm_gain)
     my_rows = exchange(spread).reshape(xs * own, depth)
     mate_rows = swap(my_rows)
-    mate_out, held = feed_forward_first(mate_rows, weights, core.astype(jnp.int32).reshape(1))
+    mate_out, held = feed_forward_first(
+        mate_rows, weights, core.astype(jnp.int32).reshape(1), *mine.shape
+    )
     mate_sum = swap(mate_out)
-    my_out = feed_forward_second(my_rows, held)
+    my_out = feed_forward_second(my_rows, held, *mine.shape)
     return last_sum(added(my_out, mate_sum), mixed_rows)
 
 

time: 135 us -> 135 us (level)
    pallas_call x2 -> x3, Pallas kernels: 7.68 us -> 7.81 us  [the longest x1 4.92 us: feed_forward_first(): pl.pallas_call(functools.partial(first_kernel, piece=piece, hid=width //...]
where the time goes in v5:
time: 135 us
  blocking collectives  81.8 us (61%)
  Pallas kernels  14.3 us (11%)
  starting transfers between devices  13.6 us (10%)
  between operations  13.6 us (10%)
  waiting for transfers between devices  9.74 us (7%)
    all_to_all x3, blocking collectives, exchange(): lax.all_to_all(blocks.reshape(xs, own, depth), 'tp', 0, 0, tiled=True, ax...  55.4 us
    all_to_all x1, blocking collectives, shards(): lax.all_to_all(pack_copies(mine), both_axes, 0, 0, tiled=True, axis_index...  26.4 us
    ppermute x3, starting transfers between devices, swap(): return lax.ppermute(array, 'tp', core_swap(tps))  7.74 us
    pallas_call x1, Pallas kernels, attend_and_project(): pl.pallas_call(attention_kernel, out_shape=(jax.ShapeDtypeStruct((half, d...  5.35 us
    pallas_call x1, Pallas kernels, feed_forward_first(): pl.pallas_call(functools.partial(first_kernel, piece=piece, hid=width //...  4.92 us
    ppermute x3, waiting for transfers between devices, swap(): return lax.ppermute(array, 'tp', core_swap(tps))  4.89 us
    ppermute x1, waiting for transfers between devices, halo_sides(): low = lax.ppermute(block[:, -width:], axis, forward)  4.82 us
    ppermute x1, starting transfers between devices, halo_sides(): low = lax.ppermute(block[:, -width:], axis, forward)  3.06 us
  transfers between devices with their start and end apart: 6, of which 3 were waited for; matrix products, arithmetic and copies ran while one was open for 0% of the time, Pallas kernels for 6%

profile of v5, /device:TPU:64, one launch (start us, length us, event | category | flops | bytes accessed | tf_op | source)
XLA Modules:
  0.0 134.7 jit_solution(15295827532989241104)
XLA Ops:
  6.5 0.0 all-gather.3.cloned.1.call-start
  6.5 0.9 concatenate.6.joined_ref
  7.5 0.0 copy-start.5
  7.5 0.0 copy-start.6
  7.5 0.1 pack.1
  7.7 0.0 copy-start.2
  7.7 0.0 copy-start.3
  7.7 0.0 copy-start.4
  7.7 26.4 %all_to_all.20 = bf16[8,528,128]{2,1,0:T(8,128)(2,1)} all-to-all(bf16[8,528,128]{2,1,0:T(8,128)(2,1)S(1)} %pack.1), channel_id=1, replica_groups={{0,8,16,24,32,40,48,56},{64,72,80,88,96,104,112,120},{128,136,144,152,1..., dimensions={0} | all-to-all | bytes 2162688 | tf_op jit(solution)/shard_map/all_to_all | solution.py:338
  34.1 0.0 all-gather.3.cloned.1.call-update
  34.1 0.1 pad_add_fusion.place_ref
  34.2 0.0 copy-done.5
  34.2 0.0 copy-done.6
  34.2 2.8 %collective-permute-start.1 = (bf16[128,128]{1,0:T(8,128)(2,1)S(1)}, bf16[128,128]{1,0:T(8,128)(2,1)S(1)}, u32[]{:S(2)}, u32[]{:S(2)}) collective-permute-start(bf16[128,128]{1,0:T(8,128)(2,1)S(1)} %get-tuple-element.25), channel_id=1, source_target_pairs={{8,0},{16,8},{24,16},{32,24},{40,32},{48,40},{56,48},{64,56},{72,6... | collective-permute-start | bytes 98312 | tf_op jit(solution)/shard_map/ppermute | solution.py:192
  37.0 3.1 %collective-permute-start = (bf16[128,128]{1,0:T(8,128)(2,1)S(1)}, bf16[128,128]{1,0:T(8,128)(2,1)S(1)}, u32[]{:S(2)}, u32[]{:S(2)}) collective-permute-start(bf16[128,128]{1,0:T(8,128)(2,1)S(1)} %get-tuple-element.26), channel_id=1, source_target_pairs={{0,8},{8,16},{16,24},{24,32},{32,40},{40,48},{48,56},{56,64},{64,7... | collective-permute-start | bytes 98312 | tf_op jit(solution)/shard_map/ppermute | solution.py:191
  40.1 0.0 collective-permute-done.1.high_ref
  40.1 4.8 %collective-permute-done.low_ref = bf16[128,128]{1,0:T(8,128)(2,1)S(1)} collective-permute-done((bf16[128,128]{1,0:T(8,128)(2,1)S(1)}, bf16[128,128]{1,0:T(8,128)(2,1)S(1)}, u32[]{:S(2)}, u32[]{:S(2)}) %collective-permute-start) | collective-permute-done | bytes 32800 | tf_op jit(solution)/shard_map/ppermute | solution.py:191
  44.9 0.0 copy-done.2
  44.9 0.0 copy-done.3
  44.9 0.0 copy-done.4
  44.9 5.3 %attend.1 = (bf16[256,2048]{1,0:T(8,128)(2,1)S(1)}, f32[256,2048]{1,0:T(8,128)S(1)}) custom-call(s32[3]{0:T(128)S(1)} %pad_add_fusion.place_ref, f32[4]{0:T(128)S(1)} %copy-done.4, bf16[512,256]{1,0:T(8,128)(2,1)S(1)} %copy-done.3, bf16[128,128]{1,0:T(8,128)(2,1)S(1)} %collective-permute-done.low_ref, bf16[128,512]{1,0:T(8,128)(2,1)S(1)} %pad_maximum_fusion.mid_ref, ...), custom_call_target="tpu_custom_call" | custom-call | flops 738197504 | bytes 4194304 | tf_op jit(solution)/shard_map/attend/pallas_call | solution.py:254
  50.3 3.8 %collective-permute-start.2 = (bf16[256,2048]{1,0:T(8,128)(2,1)S(1)}, bf16[256,2048]{1,0:T(8,128)(2,1)S(1)}, u32[]{:S(2)}, u32[]{:S(2)}) collective-permute-start(bf16[256,2048]{1,0:T(8,128)(2,1)S(1)} %get-tuple-element.19), channel_id=1, source_target_pairs={{0,1},{1,0},{2,3},{3,2},{4,5},{5,4},{6,7},{7,6},{8,9},{9,8},{10,11... | collective-permute-start | bytes 3145736 | tf_op jit(solution)/shard_map/ppermute | solution.py:358
  54.1 2.3 %collective-permute-done.2 = bf16[256,2048]{1,0:T(8,128)(2,1)S(1)} collective-permute-done((bf16[256,2048]{1,0:T(8,128)(2,1)S(1)}, bf16[256,2048]{1,0:T(8,128)(2,1)S(1)}, u32[]{:S(2)}, u32[]{:S(2)}) %collective-permute-start.2) | collective-permute-done | bytes 1048608 | tf_op jit(solution)/shard_map/ppermute | solution.py:358
  56.4 0.3 add_convert_fusion.1
  56.7 0.0 copy-start
  56.7 0.0 copy-start.1
  56.7 19.9 %all_to_all.21.pieces_ref = bf16[4,64,2048]{2,1,0:T(8,128)(2,1)S(1)} all-to-all(bf16[4,64,2048]{2,1,0:T(8,128)(2,1)S(1)} %bitcast.14), channel_id=1, replica_groups={{0,2,4,6},{1,3,5,7},{8,10,12,14},{9,11,13,15},{16,18,20,22},{17,19,21,2..., dimensions={0} | all-to-all | bytes 2097152 | tf_op jit(solution)/shard_map/all_to_all | solution.py:361
  76.5 0.0 copy-done
  76.5 0.0 copy-done.1
  76.5 0.3 norm.1
  76.9 17.2 %all_to_all.22 = bf16[4,64,2048]{2,1,0:T(8,128)(2,1)S(1)} all-to-all(bf16[4,64,2048]{2,1,0:T(8,128)(2,1)S(1)} %get-tuple-element.20), channel_id=1, replica_groups={{0,2,4,6},{1,3,5,7},{8,10,12,14},{9,11,13,15},{16,18,20,22},{17,19,21,2..., dimensions={0} | all-to-all | bytes 2097152 | tf_op jit(solution)/shard_map/all_to_all | solution.py:361
  94.1 1.9 %collective-permute-start.3 = (bf16[256,2048]{1,0:T(8,128)(2,1)S(1)}, bf16[256,2048]{1,0:T(8,128)(2,1)S(1)}, u32[]{:S(2)}, u32[]{:S(2)}) collective-permute-start(bf16[256,2048]{1,0:T(8,128)(2,1)S(1)} %bitcast.10), channel_id=1, source_target_pairs={{0,1},{1,0},{2,3},{3,2},{4,5},{5,4},{6,7},{7,6},{8,9},{9,8},{10,11... | collective-permute-start | bytes 3145736 | tf_op jit(solution)/shard_map/ppermute | solution.py:358
  96.0 2.6 %collective-permute-done.3.rows_ref = bf16[256,2048]{1,0:T(8,128)(2,1)S(1)} collective-permute-done((bf16[256,2048]{1,0:T(8,128)(2,1)S(1)}, bf16[256,2048]{1,0:T(8,128)(2,1)S(1)}, u32[]{:S(2)}, u32[]{:S(2)}) %collective-permute-start.3) | collective-permute-done | bytes 1048608 | tf_op jit(solution)/shard_map/ppermute | solution.py:358
  98.6 0.0 all-gather.3.cloned.1.call-done
  98.6 4.9 %ffn_first.1 = (bf16[256,2048]{1,0:T(8,128)(2,1)S(1)}, bf16[8,8,528,128]{3,2,1,0:T(8,128)(2,1)S(1)}) custom-call(s32[1]{0:T(128)} %bitcast.core_ref, bf16[256,2048]{1,0:T(8,128)(2,1)S(1)} %collective-permute-done.3.rows_ref, bf16[8,8,528,128]{3,2,1,0:T(8,128)(2,1)} %bitcast.13), custom_call_target="tpu_custom_call" | custom-call | flops 2214592512 | bytes 10747904 | tf_op jit(solution)/shard_map/ffn_first/pallas_call | solution.py:152
  103.5 2.0 %collective-permute-start.4 = (bf16[256,2048]{1,0:T(8,128)(2,1)S(1)}, bf16[256,2048]{1,0:T(8,128)(2,1)S(1)}, u32[]{:S(2)}, u32[]{:S(2)}) collective-permute-start(bf16[256,2048]{1,0:T(8,128)(2,1)S(1)} %get-tuple-element.23), channel_id=1, source_target_pairs={{0,1},{1,0},{2,3},{3,2},{4,5},{5,4},{6,7},{7,6},{8,9},{9,8},{10,11... | collective-permute-start | bytes 3145736 | tf_op jit(solution)/shard_map/ppermute | solution.py:358
  105.6 2.7 %ffn_second.1 = f32[256,2048]{1,0:T(8,128)S(1)} custom-call(bf16[256,2048]{1,0:T(8,128)(2,1)S(1)} %bitcast.11, bf16[8,8,528,128]{3,2,1,0:T(8,128)(2,1)S(1)} %get-tuple-element.22.held), custom_call_target="tpu_custom_call" | custom-call | flops 2214592512 | bytes 10747904 | tf_op jit(solution)/shard_map/ffn_second/pallas_call | solution.py:176
  108.4 0.0 collective-permute-done.4
  108.4 0.3 add_convert_fusion
  108.7 18.3 %all_to_all.23.pieces_ref = bf16[4,64,2048]{2,1,0:T(8,128)(2,1)S(1)} all-to-all(bf16[4,64,2048]{2,1,0:T(8,128)(2,1)S(1)} %bitcast.15), channel_id=1, replica_groups={{0,2,4,6},{1,3,5,7},{8,10,12,14},{9,11,13,15},{16,18,20,22},{17,19,21,2..., dimensions={0} | all-to-all | bytes 2097152 | tf_op jit(solution)/shard_map/all_to_all | solution.py:361
  127.0 0.8 last.1
  (2 shorter events, 0.0 us)
Async XLA Ops:
  6.5 92.1 %all-gather.3.cloned.1.call-start = ((), (), s32[]{:S(2)}) async-start(), calls=%async_computation.4 | async-start | bytes 9732096 | tf_op jit(solution)/shard_map/all_gather | solution.py:347
  7.5 26.7 %copy-start.5 = (bf16[512,64]{0,1:T(8,128)(2,1)S(1)}, bf16[512,64]{0,1:T(8,128)(2,1)}, u32[]{:S(2)}) copy-start(bf16[512,64]{0,1:T(8,128)(2,1)} %param.11) | copy-start | bytes 196612
  7.5 26.7 %copy-start.6 = (bf16[512,64]{0,1:T(8,128)(2,1)S(1)}, bf16[512,64]{0,1:T(8,128)(2,1)}, u32[]{:S(2)}) copy-start(bf16[512,64]{0,1:T(8,128)(2,1)} %param.12) | copy-start | bytes 196612
  7.7 37.3 %copy-start.2 = (bf16[256,2048]{1,0:T(8,128)(2,1)S(1)}, bf16[256,2048]{1,0:T(8,128)(2,1)}, u32[]{:S(2)}) copy-start(bf16[256,2048]{1,0:T(8,128)(2,1)} %proj_ref.1) | copy-start | bytes 3145732
  7.7 37.3 %copy-start.3 = (bf16[512,256]{1,0:T(8,128)(2,1)S(1)}, bf16[512,256]{1,0:T(8,128)(2,1)}, u32[]{:S(2)}) copy-start(bf16[512,256]{1,0:T(8,128)(2,1)} %query_ref) | copy-start | bytes 786436
  7.7 37.3 %copy-start.4 = (f32[4]{0:T(128)S(1)}, f32[4]{0:T(128)}, u32[]{:S(2)}) copy-start(f32[4]{0:T(128)} %sink_ref.1) | copy-start | bytes 52
  34.2 5.9 %collective-permute-start.1 = (bf16[128,128]{1,0:T(8,128)(2,1)S(1)}, bf16[128,128]{1,0:T(8,128)(2,1)S(1)}, u32[]{:S(2)}, u32[]{:S(2)}) collective-permute-start(bf16[128,128]{1,0:T(8,128)(2,1)S(1)} %get-tuple-element.25), channel_id=1, source_target_pairs={{8,0},{16,8},{24,16},{32,24},{40,32},{48,40},{56,48},{64,56},{72,6... | collective-permute-start | bytes 98312 | tf_op jit(solution)/shard_map/ppermute | solution.py:192
  37.0 7.9 %collective-permute-start = (bf16[128,128]{1,0:T(8,128)(2,1)S(1)}, bf16[128,128]{1,0:T(8,128)(2,1)S(1)}, u32[]{:S(2)}, u32[]{:S(2)}) collective-permute-start(bf16[128,128]{1,0:T(8,128)(2,1)S(1)} %get-tuple-element.26), channel_id=1, source_target_pairs={{0,8},{8,16},{16,24},{24,32},{32,40},{40,48},{48,56},{56,64},{64,7... | collective-permute-start | bytes 98312 | tf_op jit(solution)/shard_map/ppermute | solution.py:191
  50.3 6.1 %collective-permute-start.2 = (bf16[256,2048]{1,0:T(8,128)(2,1)S(1)}, bf16[256,2048]{1,0:T(8,128)(2,1)S(1)}, u32[]{:S(2)}, u32[]{:S(2)}) collective-permute-start(bf16[256,2048]{1,0:T(8,128)(2,1)S(1)} %get-tuple-element.19), channel_id=1, source_target_pairs={{0,1},{1,0},{2,3},{3,2},{4,5},{5,4},{6,7},{7,6},{8,9},{9,8},{10,11... | collective-permute-start | bytes 3145736 | tf_op jit(solution)/shard_map/ppermute | solution.py:358
  56.7 19.9 %copy-start = (bf16[64,2048]{1,0:T(8,128)(2,1)S(1)}, bf16[64,2048]{1,0:T(8,128)(2,1)}, u32[]{:S(2)}) copy-start(bf16[64,2048]{1,0:T(8,128)(2,1)} %residual_ref.1) | copy-start | bytes 786436
  56.7 19.9 %copy-start.1 = (f32[2048]{0:T(1024)S(1)}, f32[2048]{0:T(1024)}, u32[]{:S(2)}) copy-start(f32[2048]{0:T(1024)} %param.16) | copy-start | bytes 24580
  94.1 4.5 %collective-permute-start.3 = (bf16[256,2048]{1,0:T(8,128)(2,1)S(1)}, bf16[256,2048]{1,0:T(8,128)(2,1)S(1)}, u32[]{:S(2)}, u32[]{:S(2)}) collective-permute-start(bf16[256,2048]{1,0:T(8,128)(2,1)S(1)} %bitcast.10), channel_id=1, source_target_pairs={{0,1},{1,0},{2,3},{3,2},{4,5},{5,4},{6,7},{7,6},{8,9},{9,8},{10,11... | collective-permute-start | bytes 3145736 | tf_op jit(solution)/shard_map/ppermute | solution.py:358
  103.5 4.8 %collective-permute-start.4 = (bf16[256,2048]{1,0:T(8,128)(2,1)S(1)}, bf16[256,2048]{1,0:T(8,128)(2,1)S(1)}, u32[]{:S(2)}, u32[]{:S(2)}) collective-permute-start(bf16[256,2048]{1,0:T(8,128)(2,1)S(1)} %get-tuple-element.23), channel_id=1, source_target_pairs={{0,1},{1,0},{2,3},{3,2},{4,5},{5,4},{6,7},{7,6},{8,9},{9,8},{10,11... | collective-permute-start | bytes 3145736 | tf_op jit(solution)/shard_map/ppermute | solution.py:358
Sparse Core Ops, SparseCore 0:
  34.2 56.3 all-gather.2

commit v6 on v5

--- a/solution.py
+++ b/solution.py
@@ -193,44 +193,82 @@
     return low, high
 
 
+def attend_block(query, band, valid, sink):
+    heads = query.shape[1] // HEAD_DIM
+    scaled = query * jnp.bfloat16(HEAD_DIM ** (-0.5))
+    stacked = jnp.concatenate(
+        [scaled[:, head * HEAD_DIM : (head + 1) * HEAD_DIM] for head in range(heads)], axis=0
+    )
+    scores = jnp.dot(stacked, band[:HEAD_DIM], preferred_element_type=jnp.float32)
+    scores = jnp.where(jnp.concatenate([valid] * heads, axis=0), scores, -1e30)
+    peak = jnp.maximum(jnp.max(scores, axis=1, keepdims=True), sink)
+    raw = jnp.exp(scores - peak)
+    denom = jnp.sum(raw, axis=1, keepdims=True) + jnp.exp(sink - peak)
+    probs = (raw * (1.0 / denom)).astype(jnp.bfloat16)
+    mixed = lax.dot_general(
+        probs, band[HEAD_DIM:], (((1,), (1,)), ((), ())), preferred_element_type=jnp.float32
+    ).astype(jnp.bfloat16)
+    return jnp.concatenate(
+        [mixed[head * WINDOW : (head + 1) * WINDOW] for head in range(heads)], axis=1
+    )
+
+
+def near_and_position():
+    query_at = lax.broadcasted_iota(jnp.int32, (WINDOW, 3 * WINDOW), 0)
+    key_at = lax.broadcasted_iota(jnp.int32, (WINDOW, 3 * WINDOW), 1)
+    return (key_at >= query_at) & (key_at <= query_at + 2 * WINDOW), key_at
+
+
+def sink_column(sink_ref, heads):
+    return jnp.concatenate(
+        [jnp.full((WINDOW, 1), sink_ref[head], jnp.float32) for head in range(heads)], axis=0
+    )
+
+
+def inner_kernel(sink_ref, query_ref, mid_ref, out_ref):
+    near, _ = near_and_position()
+    sink = sink_column(sink_ref, query_ref.shape[1] // HEAD_DIM)
+    for at in range(WINDOW, query_ref.shape[0] - WINDOW, WINDOW):
+        out_ref[at - WINDOW : at, :] = attend_block(
+            query_ref[at : at + WINDOW, :], mid_ref[:, at - WINDOW : at + 2 * WINDOW], near, sink
+        )
+
+
+def attend_inner(queries, middle, sink_logit):
+    rows, columns = queries.shape
+    vmem = pl.BlockSpec(memory_space=pltpu.VMEM)
+    return pl.pallas_call(
+        inner_kernel,
+        out_shape=jax.ShapeDtypeStruct((rows - 2 * WINDOW, columns), queries.dtype),
+        in_specs=[pl.BlockSpec(memory_space=pltpu.SMEM), vmem, vmem],
+        out_specs=vmem,
+        cost_estimate=pl.CostEstimate(
+            flops=12 * WINDOW * rows * columns,
+            bytes_accessed=4 * rows * columns,
+            transcendentals=WINDOW * rows * columns // HEAD_DIM,
+        ),
+        compiler_params=pltpu.CompilerParams(vmem_limit_bytes=16 * 1024 * 1024),
+        name="inner",
+    )(sink_logit, queries, middle)
+
+
 def attention_kernel(
-    place_ref, sink_ref, query_ref, low_ref, mid_ref, high_ref, proj_ref, mate_ref, mine_ref, padded, attended
+    place_ref, sink_ref, query_ref, low_ref, mid_ref, high_ref, inner_ref, proj_ref, mate_ref, mine_ref, attended
 ):
     rows = query_ref.shape[0]
-    heads = query_ref.shape[1] // HEAD_DIM
     piece = WINDOW // CORES
     core, start, total = place_ref[0], place_ref[1], place_ref[2]
-    padded[:, :WINDOW] = low_ref[...]
-    padded[:, WINDOW : WINDOW + rows] = mid_ref[...]
-    padded[:, WINDOW + rows :] = high_ref[...]
-    query_at = lax.broadcasted_iota(jnp.int32, (WINDOW, 3 * WINDOW), 0)
-    key_at = lax.broadcasted_iota(jnp.int32, (WINDOW, 3 * WINDOW), 1)
-    near = (key_at >= query_at) & (key_at <= query_at + 2 * WINDOW)
-    sink = jnp.concatenate(
-        [jnp.full((WINDOW, 1), sink_ref[head], jnp.float32) for head in range(heads)], axis=0
-    )
-    for block in range(rows // WINDOW):
-        at = block * WINDOW
+    near, key_at = near_and_position()
+    sink = sink_column(sink_ref, query_ref.shape[1] // HEAD_DIM)
+    first = jnp.concatenate([low_ref[...], mid_ref[:, : 2 * WINDOW]], axis=1)
+    last = jnp.concatenate([mid_ref[:, rows - 2 * WINDOW :], high_ref[...]], axis=1)
+    for at, band in ((0, first), (rows - WINDOW, last)):
         position = key_at + (start + at - WINDOW)
         valid = near & (position >= 0) & (position < total)
-        keys = padded[:HEAD_DIM, at : at + 3 * WINDOW]
-        values = padded[HEAD_DIM:, at : at + 3 * WINDOW]
-        scaled = query_ref[at : at + WINDOW, :] * jnp.bfloat16(HEAD_DIM ** (-0.5))
-        stacked = jnp.concatenate(
-            [scaled[:, head * HEAD_DIM : (head + 1) * HEAD_DIM] for head in range(heads)], axis=0
-        )
-        scores = jnp.dot(stacked, keys, preferred_element_type=jnp.float32)
-        scores = jnp.where(jnp.concatenate([valid] * heads, axis=0), scores, -1e30)
-        peak = jnp.maximum(jnp.max(scores, axis=1, keepdims=True), sink)
-        raw = jnp.exp(scores - peak)
-        denom = jnp.sum(raw, axis=1, keepdims=True) + jnp.exp(sink - peak)
-        probs = (raw * (1.0 / denom)).astype(jnp.bfloat16)
-        mixed = lax.dot_general(
-            probs, values, (((1,), (1,)), ((), ())), preferred_element_type=jnp.float32
-        ).astype(jnp.bfloat16)
-        attended[at : at + WINDOW, :] = jnp.concatenate(
-            [mixed[head * WINDOW : (head + 1) * WINDOW] for head in range(heads)], axis=1
-        )
+        attended[at : at + WINDOW, :] = attend_block(
+            query_ref[at : at + WINDOW, :], band, valid, sink
+        )
+    attended[WINDOW : rows - WINDOW, :] = inner_ref[...]
     for target, which in ((mate_ref, 1 - core), (mine_ref, core)):
         picked = jnp.concatenate(
             [
@@ -244,7 +282,7 @@
         )
 
 
-def attend_and_project(queries, sides, middle, sink_logit, out_weight, place):
+def attend_and_project(queries, sides, middle, inner, sink_logit, out_weight, place):
     rows, columns = queries.shape
     depth = out_weight.shape[1]
     low, high = sides
@@ -257,12 +295,9 @@
             jax.ShapeDtypeStruct((half, depth), jnp.bfloat16),
             jax.ShapeDtypeStruct((half, depth), jnp.float32),
         ),
-        in_specs=[smem, smem, vmem, vmem, vmem, vmem, vmem],
+        in_specs=[smem, smem] + [vmem] * 6,
         out_specs=(vmem, vmem),
-        scratch_shapes=[
-            pltpu.VMEM((2 * HEAD_DIM, rows + 2 * WINDOW), jnp.bfloat16),
-            pltpu.VMEM((rows, columns), jnp.bfloat16),
-        ],
+        scratch_shapes=[pltpu.VMEM((rows, columns), jnp.bfloat16)],
         cost_estimate=pl.CostEstimate(
             flops=2 * rows * columns * (6 * WINDOW + depth),
             bytes_accessed=8 * half * depth,
@@ -270,7 +305,7 @@
         ),
         compiler_params=pltpu.CompilerParams(vmem_limit_bytes=16 * 1024 * 1024),
         name="attend",
-    )(place, sink_logit, queries, low, middle, high, out_weight)
+    )(place, sink_logit, queries, low, middle, high, inner, out_weight)
 
 
 def norm_kernel(pieces_ref, residual_ref, gain_ref, mixed_ref, spread_ref):
@@ -366,7 +401,7 @@
         return exchange((mine + mates.astype(jnp.float32)).astype(jnp.bfloat16))
 
     mate_part, my_part = attend_and_project(
-        queries, sides, middle, sink_logit, out_weight, place
+        queries, sides, middle, attend_inner(queries, middle, sink_logit), sink_logit, out_weight, place
     )
     mixed_rows, spread = sum_and_norm(added(my_part, swap(mate_part)), residual_in, norm_gain)
     my_rows = exchange(spread).reshape(xs * own, depth)

time: 135 us -> 133 us (0.985)
  waiting for transfers between devices: 9.74 us -> 6.78 us
    ppermute x1, waiting for transfers between devices: 4.82 us -> 1.87 us  [halo_sides(): low = lax.ppermute(block[:, -width:], axis, forward)]
    pallas_call x0 -> x1, Pallas kernels: none -> 2.94 us  [attend_inner(): pl.pallas_call(inner_kernel, out_shape=jax.ShapeDtypeStruct((rows - 2 * W...]
    pallas_call x1, Pallas kernels: 5.35 us -> 3.51 us  [attend_and_project(): pl.pallas_call(attention_kernel, out_shape=(jax.ShapeDtypeStruct((half, d...]
  transfers between devices with their start and end apart: 6 -> 6, of which waited for: 3 -> 3; matrix products, arithmetic and copies ran while one was open for 0% -> 0% of each run, Pallas kernels for 6% -> 7%
where the time goes in v6:
time: 133 us
  blocking collectives  81.8 us (62%)
  Pallas kernels  15.4 us (12%)
  starting transfers between devices  13.6 us (10%)
  between operations  13.6 us (10%)
  waiting for transfers between devices  6.78 us (5%)
    all_to_all x3, blocking collectives, exchange(): lax.all_to_all(blocks.reshape(xs, own, depth), 'tp', 0, 0, tiled=True, ax...  55.4 us
    all_to_all x1, blocking collectives, shards(): lax.all_to_all(pack_copies(mine), both_axes, 0, 0, tiled=True, axis_index...  26.4 us
    ppermute x3, starting transfers between devices, swap(): return lax.ppermute(array, 'tp', core_swap(tps))  7.74 us
    pallas_call x1, Pallas kernels, feed_forward_first(): pl.pallas_call(functools.partial(first_kernel, piece=piece, hid=width //...  4.92 us
    ppermute x3, waiting for transfers between devices, swap(): return lax.ppermute(array, 'tp', core_swap(tps))  4.89 us
    pallas_call x1, Pallas kernels, attend_and_project(): pl.pallas_call(attention_kernel, out_shape=(jax.ShapeDtypeStruct((half, d...  3.51 us
    ppermute x1, starting transfers between devices, halo_sides(): low = lax.ppermute(block[:, -width:], axis, forward)  3.06 us
    pallas_call x1, Pallas kernels, attend_inner(): pl.pallas_call(inner_kernel, out_shape=jax.ShapeDtypeStruct((rows - 2 * W...  2.94 us
  transfers between devices with their start and end apart: 6, of which 3 were waited for; matrix products, arithmetic and copies ran while one was open for 0% of the time, Pallas kernels for 7%

profile of v6, /device:TPU:64, one launch (start us, length us, event | category | flops | bytes accessed | tf_op | source)
XLA Modules:
  0.0 132.9 jit_solution(4368424848931184800)
XLA Ops:
  6.5 0.0 all-gather.3.cloned.1.call-start
  6.5 0.9 concatenate.6.joined_ref
  7.5 0.0 copy-start.5
  7.5 0.0 copy-start.6
  7.5 0.1 pack.1
  7.7 0.0 copy-start.3
  7.7 0.0 copy-start.4
  7.7 0.0 copy-start.2
  7.7 26.4 %all_to_all.20 = bf16[8,528,128]{2,1,0:T(8,128)(2,1)} all-to-all(bf16[8,528,128]{2,1,0:T(8,128)(2,1)S(1)} %pack.1), channel_id=1, replica_groups={{0,8,16,24,32,40,48,56},{64,72,80,88,96,104,112,120},{128,136,144,152,1..., dimensions={0} | all-to-all | bytes 2162688 | tf_op jit(solution)/shard_map/all_to_all | solution.py:373
  34.1 0.0 all-gather.3.cloned.1.call-update
  34.1 0.1 pad_add_fusion.place_ref
  34.2 0.0 copy-done.5
  34.2 0.0 copy-done.6
  34.2 2.8 %collective-permute-start.1 = (bf16[128,128]{1,0:T(8,128)(2,1)S(1)}, bf16[128,128]{1,0:T(8,128)(2,1)S(1)}, u32[]{:S(2)}, u32[]{:S(2)}) collective-permute-start(bf16[128,128]{1,0:T(8,128)(2,1)S(1)} %get-tuple-element.25), channel_id=1, source_target_pairs={{8,0},{16,8},{24,16},{32,24},{40,32},{48,40},{56,48},{64,56},{72,6... | collective-permute-start | bytes 98312 | tf_op jit(solution)/shard_map/ppermute | solution.py:192
  37.0 3.1 %collective-permute-start = (bf16[128,128]{1,0:T(8,128)(2,1)S(1)}, bf16[128,128]{1,0:T(8,128)(2,1)S(1)}, u32[]{:S(2)}, u32[]{:S(2)}) collective-permute-start(bf16[128,128]{1,0:T(8,128)(2,1)S(1)} %get-tuple-element.26), channel_id=1, source_target_pairs={{0,8},{8,16},{16,24},{24,32},{32,40},{40,48},{48,56},{56,64},{64,7... | collective-permute-start | bytes 98312 | tf_op jit(solution)/shard_map/ppermute | solution.py:191
  40.1 0.0 copy-done.3
  40.1 0.0 copy-done.4
  40.1 2.9 %inner.1.inner_ref = bf16[256,256]{1,0:T(8,128)(2,1)S(1)} custom-call(f32[4]{0:T(128)S(1)} %copy-done.4, bf16[512,256]{1,0:T(8,128)(2,1)S(1)} %copy-done.3, bf16[128,512]{1,0:T(8,128)(2,1)S(1)} %pad_maximum_fusion.mid_ref), custom_call_target="tpu_custom_call" | custom-call | flops 201326592 | bytes 524288 | tf_op jit(solution)/shard_map/inner/pallas_call | solution.py:240
  43.1 0.0 collective-permute-done.1.high_ref
  43.1 1.9 %collective-permute-done.low_ref = bf16[128,128]{1,0:T(8,128)(2,1)S(1)} collective-permute-done((bf16[128,128]{1,0:T(8,128)(2,1)S(1)}, bf16[128,128]{1,0:T(8,128)(2,1)S(1)}, u32[]{:S(2)}, u32[]{:S(2)}) %collective-permute-start) | collective-permute-done | bytes 32800 | tf_op jit(solution)/shard_map/ppermute | solution.py:191
  44.9 0.0 copy-done.2
  44.9 3.5 %attend.1 = (bf16[256,2048]{1,0:T(8,128)(2,1)S(1)}, f32[256,2048]{1,0:T(8,128)S(1)}) custom-call(s32[3]{0:T(128)S(1)} %pad_add_fusion.place_ref, f32[4]{0:T(128)S(1)} %copy-done.4, bf16[512,256]{1,0:T(8,128)(2,1)S(1)} %copy-done.3, bf16[128,128]{1,0:T(8,128)(2,1)S(1)} %collective-permute-done.low_ref, bf16[128,512]{1,0:T(8,128)(2,1)S(1)} %pad_maximum_fusion.mid_ref, ...), custom_call_target="tpu_custom_call" | custom-call | flops 738197504 | bytes 4194304 | tf_op jit(solution)/shard_map/attend/pallas_call | solution.py:292
  48.5 3.8 %collective-permute-start.2 = (bf16[256,2048]{1,0:T(8,128)(2,1)S(1)}, bf16[256,2048]{1,0:T(8,128)(2,1)S(1)}, u32[]{:S(2)}, u32[]{:S(2)}) collective-permute-start(bf16[256,2048]{1,0:T(8,128)(2,1)S(1)} %get-tuple-element.19), channel_id=1, source_target_pairs={{0,1},{1,0},{2,3},{3,2},{4,5},{5,4},{6,7},{7,6},{8,9},{9,8},{10,11... | collective-permute-start | bytes 3145736 | tf_op jit(solution)/shard_map/ppermute | solution.py:393
  52.2 2.3 %collective-permute-done.2 = bf16[256,2048]{1,0:T(8,128)(2,1)S(1)} collective-permute-done((bf16[256,2048]{1,0:T(8,128)(2,1)S(1)}, bf16[256,2048]{1,0:T(8,128)(2,1)S(1)}, u32[]{:S(2)}, u32[]{:S(2)}) %collective-permute-start.2) | collective-permute-done | bytes 1048608 | tf_op jit(solution)/shard_map/ppermute | solution.py:393
  54.5 0.3 add_convert_fusion.1
  54.8 0.0 copy-start
  54.8 0.0 copy-start.1
  54.8 19.9 %all_to_all.21.pieces_ref = bf16[4,64,2048]{2,1,0:T(8,128)(2,1)S(1)} all-to-all(bf16[4,64,2048]{2,1,0:T(8,128)(2,1)S(1)} %bitcast.14), channel_id=1, replica_groups={{0,2,4,6},{1,3,5,7},{8,10,12,14},{9,11,13,15},{16,18,20,22},{17,19,21,2..., dimensions={0} | all-to-all | bytes 2097152 | tf_op jit(solution)/shard_map/all_to_all | solution.py:396
  74.7 0.0 copy-done
  74.7 0.0 copy-done.1
  74.7 0.3 norm.1
  75.0 17.2 %all_to_all.22 = bf16[4,64,2048]{2,1,0:T(8,128)(2,1)S(1)} all-to-all(bf16[4,64,2048]{2,1,0:T(8,128)(2,1)S(1)} %get-tuple-element.20), channel_id=1, replica_groups={{0,2,4,6},{1,3,5,7},{8,10,12,14},{9,11,13,15},{16,18,20,22},{17,19,21,2..., dimensions={0} | all-to-all | bytes 2097152 | tf_op jit(solution)/shard_map/all_to_all | solution.py:396
  92.2 1.9 %collective-permute-start.3 = (bf16[256,2048]{1,0:T(8,128)(2,1)S(1)}, bf16[256,2048]{1,0:T(8,128)(2,1)S(1)}, u32[]{:S(2)}, u32[]{:S(2)}) collective-permute-start(bf16[256,2048]{1,0:T(8,128)(2,1)S(1)} %bitcast.10), channel_id=1, source_target_pairs={{0,1},{1,0},{2,3},{3,2},{4,5},{5,4},{6,7},{7,6},{8,9},{9,8},{10,11... | collective-permute-start | bytes 3145736 | tf_op jit(solution)/shard_map/ppermute | solution.py:393
  94.1 2.6 %collective-permute-done.3.rows_ref = bf16[256,2048]{1,0:T(8,128)(2,1)S(1)} collective-permute-done((bf16[256,2048]{1,0:T(8,128)(2,1)S(1)}, bf16[256,2048]{1,0:T(8,128)(2,1)S(1)}, u32[]{:S(2)}, u32[]{:S(2)}) %collective-permute-start.3) | collective-permute-done | bytes 1048608 | tf_op jit(solution)/shard_map/ppermute | solution.py:393
  96.8 0.0 all-gather.3.cloned.1.call-done
  96.8 4.9 %ffn_first.1 = (bf16[256,2048]{1,0:T(8,128)(2,1)S(1)}, bf16[8,8,528,128]{3,2,1,0:T(8,128)(2,1)S(1)}) custom-call(s32[1]{0:T(128)} %bitcast.core_ref, bf16[256,2048]{1,0:T(8,128)(2,1)S(1)} %collective-permute-done.3.rows_ref, bf16[8,8,528,128]{3,2,1,0:T(8,128)(2,1)} %bitcast.13), custom_call_target="tpu_custom_call" | custom-call | flops 2214592512 | bytes 10747904 | tf_op jit(solution)/shard_map/ffn_first/pallas_call | solution.py:152
  101.7 2.0 %collective-permute-start.4 = (bf16[256,2048]{1,0:T(8,128)(2,1)S(1)}, bf16[256,2048]{1,0:T(8,128)(2,1)S(1)}, u32[]{:S(2)}, u32[]{:S(2)}) collective-permute-start(bf16[256,2048]{1,0:T(8,128)(2,1)S(1)} %get-tuple-element.23), channel_id=1, source_target_pairs={{0,1},{1,0},{2,3},{3,2},{4,5},{5,4},{6,7},{7,6},{8,9},{9,8},{10,11... | collective-permute-start | bytes 3145736 | tf_op jit(solution)/shard_map/ppermute | solution.py:393
  103.8 2.7 %ffn_second.1 = f32[256,2048]{1,0:T(8,128)S(1)} custom-call(bf16[256,2048]{1,0:T(8,128)(2,1)S(1)} %bitcast.11, bf16[8,8,528,128]{3,2,1,0:T(8,128)(2,1)S(1)} %get-tuple-element.22.held), custom_call_target="tpu_custom_call" | custom-call | flops 2214592512 | bytes 10747904 | tf_op jit(solution)/shard_map/ffn_second/pallas_call | solution.py:176
  106.5 0.0 collective-permute-done.4
  106.5 0.3 add_convert_fusion
  106.8 18.3 %all_to_all.23.pieces_ref = bf16[4,64,2048]{2,1,0:T(8,128)(2,1)S(1)} all-to-all(bf16[4,64,2048]{2,1,0:T(8,128)(2,1)S(1)} %bitcast.15), channel_id=1, replica_groups={{0,2,4,6},{1,3,5,7},{8,10,12,14},{9,11,13,15},{16,18,20,22},{17,19,21,2..., dimensions={0} | all-to-all | bytes 2097152 | tf_op jit(solution)/shard_map/all_to_all | solution.py:396
  125.2 0.8 last.1
  (2 shorter events, 0.0 us)
Async XLA Ops:
  6.5 90.2 %all-gather.3.cloned.1.call-start = ((), (), s32[]{:S(2)}) async-start(), calls=%async_computation.4 | async-start | bytes 9732096 | tf_op jit(solution)/shard_map/all_gather | solution.py:382
  7.5 26.7 %copy-start.5 = (bf16[512,64]{0,1:T(8,128)(2,1)S(1)}, bf16[512,64]{0,1:T(8,128)(2,1)}, u32[]{:S(2)}) copy-start(bf16[512,64]{0,1:T(8,128)(2,1)} %param.11) | copy-start | bytes 196612
  7.5 26.7 %copy-start.6 = (bf16[512,64]{0,1:T(8,128)(2,1)S(1)}, bf16[512,64]{0,1:T(8,128)(2,1)}, u32[]{:S(2)}) copy-start(bf16[512,64]{0,1:T(8,128)(2,1)} %param.12) | copy-start | bytes 196612
  7.7 32.4 %copy-start.3 = (bf16[512,256]{1,0:T(8,128)(2,1)S(1)}, bf16[512,256]{1,0:T(8,128)(2,1)}, u32[]{:S(2)}) copy-start(bf16[512,256]{1,0:T(8,128)(2,1)} %query_ref.1) | copy-start | bytes 786436
  7.7 32.4 %copy-start.4 = (f32[4]{0:T(128)S(1)}, f32[4]{0:T(128)}, u32[]{:S(2)}) copy-start(f32[4]{0:T(128)} %sink_ref.3) | copy-start | bytes 52
  7.7 37.3 %copy-start.2 = (bf16[256,2048]{1,0:T(8,128)(2,1)S(1)}, bf16[256,2048]{1,0:T(8,128)(2,1)}, u32[]{:S(2)}) copy-start(bf16[256,2048]{1,0:T(8,128)(2,1)} %proj_ref.1) | copy-start | bytes 3145732
  34.2 8.8 %collective-permute-start.1 = (bf16[128,128]{1,0:T(8,128)(2,1)S(1)}, bf16[128,128]{1,0:T(8,128)(2,1)S(1)}, u32[]{:S(2)}, u32[]{:S(2)}) collective-permute-start(bf16[128,128]{1,0:T(8,128)(2,1)S(1)} %get-tuple-element.25), channel_id=1, source_target_pairs={{8,0},{16,8},{24,16},{32,24},{40,32},{48,40},{56,48},{64,56},{72,6... | collective-permute-start | bytes 98312 | tf_op jit(solution)/shard_map/ppermute | solution.py:192
  37.0 7.9 %collective-permute-start = (bf16[128,128]{1,0:T(8,128)(2,1)S(1)}, bf16[128,128]{1,0:T(8,128)(2,1)S(1)}, u32[]{:S(2)}, u32[]{:S(2)}) collective-permute-start(bf16[128,128]{1,0:T(8,128)(2,1)S(1)} %get-tuple-element.26), channel_id=1, source_target_pairs={{0,8},{8,16},{16,24},{24,32},{32,40},{40,48},{48,56},{56,64},{64,7... | collective-permute-start | bytes 98312 | tf_op jit(solution)/shard_map/ppermute | solution.py:191
  48.5 6.1 %collective-permute-start.2 = (bf16[256,2048]{1,0:T(8,128)(2,1)S(1)}, bf16[256,2048]{1,0:T(8,128)(2,1)S(1)}, u32[]{:S(2)}, u32[]{:S(2)}) collective-permute-start(bf16[256,2048]{1,0:T(8,128)(2,1)S(1)} %get-tuple-element.19), channel_id=1, source_target_pairs={{0,1},{1,0},{2,3},{3,2},{4,5},{5,4},{6,7},{7,6},{8,9},{9,8},{10,11... | collective-permute-start | bytes 3145736 | tf_op jit(solution)/shard_map/ppermute | solution.py:393
  54.8 19.9 %copy-start = (bf16[64,2048]{1,0:T(8,128)(2,1)S(1)}, bf16[64,2048]{1,0:T(8,128)(2,1)}, u32[]{:S(2)}) copy-start(bf16[64,2048]{1,0:T(8,128)(2,1)} %residual_ref.1) | copy-start | bytes 786436
  54.8 19.9 %copy-start.1 = (f32[2048]{0:T(1024)S(1)}, f32[2048]{0:T(1024)}, u32[]{:S(2)}) copy-start(f32[2048]{0:T(1024)} %param.16) | copy-start | bytes 24580
  92.2 4.5 %collective-permute-start.3 = (bf16[256,2048]{1,0:T(8,128)(2,1)S(1)}, bf16[256,2048]{1,0:T(8,128)(2,1)S(1)}, u32[]{:S(2)}, u32[]{:S(2)}) collective-permute-start(bf16[256,2048]{1,0:T(8,128)(2,1)S(1)} %bitcast.10), channel_id=1, source_target_pairs={{0,1},{1,0},{2,3},{3,2},{4,5},{5,4},{6,7},{7,6},{8,9},{9,8},{10,11... | collective-permute-start | bytes 3145736 | tf_op jit(solution)/shard_map/ppermute | solution.py:393
  101.7 4.8 %collective-permute-start.4 = (bf16[256,2048]{1,0:T(8,128)(2,1)S(1)}, bf16[256,2048]{1,0:T(8,128)(2,1)S(1)}, u32[]{:S(2)}, u32[]{:S(2)}) collective-permute-start(bf16[256,2048]{1,0:T(8,128)(2,1)S(1)} %get-tuple-element.23), channel_id=1, source_target_pairs={{0,1},{1,0},{2,3},{3,2},{4,5},{5,4},{6,7},{7,6},{8,9},{9,8},{10,11... | collective-permute-start | bytes 3145736 | tf_op jit(solution)/shard_map/ppermute | solution.py:393
Sparse Core Ops, SparseCore 0:
  34.2 56.3 all-gather.2

commit v7 on v6

--- a/solution.py
+++ b/solution.py
@@ -269,17 +269,19 @@
             query_ref[at : at + WINDOW, :], band, valid, sink
         )
     attended[WINDOW : rows - WINDOW, :] = inner_ref[...]
-    for target, which in ((mate_ref, 1 - core), (mine_ref, core)):
-        picked = jnp.concatenate(
+    def picked(which):
+        return jnp.concatenate(
             [
                 attended[pl.ds(pl.multiple_of(at + which * piece, piece), piece), :]
                 for at in range(0, rows, WINDOW)
             ],
             axis=0,
         )
-        target[...] = jnp.dot(picked, proj_ref[...], preferred_element_type=jnp.float32).astype(
-            target.dtype
-        )
+
+    mine_ref[...] = picked(core)
+    mate_ref[...] = jnp.dot(
+        picked(1 - core), proj_ref[...], preferred_element_type=jnp.float32
+    ).astype(mate_ref.dtype)
 
 
 def attend_and_project(queries, sides, middle, inner, sink_logit, out_weight, place):
@@ -293,7 +295,7 @@
         attention_kernel,
         out_shape=(
             jax.ShapeDtypeStruct((half, depth), jnp.bfloat16),
-            jax.ShapeDtypeStruct((half, depth), jnp.float32),
+            jax.ShapeDtypeStruct((half, columns), jnp.bfloat16),
         ),
         in_specs=[smem, smem] + [vmem] * 6,
         out_specs=(vmem, vmem),
@@ -400,9 +402,10 @@
     def added(mine, mates):
         return exchange((mine + mates.astype(jnp.float32)).astype(jnp.bfloat16))
 
-    mate_part, my_part = attend_and_project(
+    mate_part, my_heads = attend_and_project(
         queries, sides, middle, attend_inner(queries, middle, sink_logit), sink_logit, out_weight, place
     )
+    my_part = jnp.dot(my_heads, out_weight, preferred_element_type=jnp.float32)
     mixed_rows, spread = sum_and_norm(added(my_part, swap(mate_part)), residual_in, norm_gain)
     my_rows = exchange(spread).reshape(xs * own, depth)
     mate_rows = swap(my_rows)

time: 133 us -> 133 us (level)
  no operation moved by 1% of the time
where the time goes in v7:
time: 133 us
  blocking collectives  81.7 us (61%)
  Pallas kernels  15.2 us (11%)
  starting transfers between devices  13.6 us (10%)
  between operations  13.6 us (10%)
  waiting for transfers between devices  6.78 us (5%)
    all_to_all x3, blocking collectives, exchange(): lax.all_to_all(blocks.reshape(xs, own, depth), 'tp', 0, 0, tiled=True, ax...  55.3 us
    all_to_all x1, blocking collectives, shards(): lax.all_to_all(pack_copies(mine), both_axes, 0, 0, tiled=True, axis_index...  26.4 us
    ppermute x3, starting transfers between devices, swap(): return lax.ppermute(array, 'tp', core_swap(tps))  7.73 us
    pallas_call x1, Pallas kernels, feed_forward_first(): pl.pallas_call(functools.partial(first_kernel, piece=piece, hid=width //...  4.92 us
    ppermute x3, waiting for transfers between devices, swap(): return lax.ppermute(array, 'tp', core_swap(tps))  4.89 us
    pallas_call x1, Pallas kernels, attend_and_project(): pl.pallas_call(attention_kernel, out_shape=(jax.ShapeDtypeStruct((half, d...  3.25 us
    ppermute x1, starting transfers between devices, halo_sides(): low = lax.ppermute(block[:, -width:], axis, forward)  3.06 us
    pallas_call x1, Pallas kernels, attend_inner(): pl.pallas_call(inner_kernel, out_shape=jax.ShapeDtypeStruct((rows - 2 * W...  2.94 us
  transfers between devices with their start and end apart: 6, of which 3 were waited for; matrix products, arithmetic and copies ran while one was open for 0% of the time, Pallas kernels for 7%

profile of v7, /device:TPU:64, one launch (start us, length us, event | category | flops | bytes accessed | tf_op | source)
XLA Modules:
  0.0 132.6 jit_solution(16318352290355788439)
XLA Ops:
  6.5 0.0 all-gather.3.cloned.1.call-start
  6.5 0.9 concatenate.6.joined_ref
  7.5 0.0 copy-start.5
  7.5 0.0 copy-start.6
  7.5 0.1 pack.1
  7.7 0.0 copy-start.3
  7.7 0.0 copy-start.4
  7.7 0.0 copy-start
  7.7 26.4 %all_to_all.20 = bf16[8,528,128]{2,1,0:T(8,128)(2,1)} all-to-all(bf16[8,528,128]{2,1,0:T(8,128)(2,1)S(1)} %pack.1), channel_id=1, replica_groups={{0,8,16,24,32,40,48,56},{64,72,80,88,96,104,112,120},{128,136,144,152,1..., dimensions={0} | all-to-all | bytes 2162688 | tf_op jit(solution)/shard_map/all_to_all | solution.py:375
  34.1 0.0 all-gather.3.cloned.1.call-update
  34.1 0.1 pad_add_fusion.place_ref
  34.2 0.0 copy-done.5
  34.2 0.0 copy-done.6
  34.2 2.8 %collective-permute-start.1 = (bf16[128,128]{1,0:T(8,128)(2,1)S(1)}, bf16[128,128]{1,0:T(8,128)(2,1)S(1)}, u32[]{:S(2)}, u32[]{:S(2)}) collective-permute-start(bf16[128,128]{1,0:T(8,128)(2,1)S(1)} %get-tuple-element.25), channel_id=1, source_target_pairs={{8,0},{16,8},{24,16},{32,24},{40,32},{48,40},{56,48},{64,56},{72,6... | collective-permute-start | bytes 98312 | tf_op jit(solution)/shard_map/ppermute | solution.py:192
  37.0 3.1 %collective-permute-start = (bf16[128,128]{1,0:T(8,128)(2,1)S(1)}, bf16[128,128]{1,0:T(8,128)(2,1)S(1)}, u32[]{:S(2)}, u32[]{:S(2)}) collective-permute-start(bf16[128,128]{1,0:T(8,128)(2,1)S(1)} %get-tuple-element.26), channel_id=1, source_target_pairs={{0,8},{8,16},{16,24},{24,32},{32,40},{40,48},{48,56},{56,64},{64,7... | collective-permute-start | bytes 98312 | tf_op jit(solution)/shard_map/ppermute | solution.py:191
  40.1 0.0 copy-done.3
  40.1 0.0 copy-done.4
  40.1 2.9 %inner.1.inner_ref = bf16[256,256]{1,0:T(8,128)(2,1)S(1)} custom-call(f32[4]{0:T(128)S(1)} %copy-done.4, bf16[512,256]{1,0:T(8,128)(2,1)S(1)} %copy-done.3, bf16[128,512]{1,0:T(8,128)(2,1)S(1)} %pad_maximum_fusion.mid_ref), custom_call_target="tpu_custom_call" | custom-call | flops 201326592 | bytes 524288 | tf_op jit(solution)/shard_map/inner/pallas_call | solution.py:240
  43.1 0.0 collective-permute-done.1.high_ref
  43.1 1.9 %collective-permute-done.low_ref = bf16[128,128]{1,0:T(8,128)(2,1)S(1)} collective-permute-done((bf16[128,128]{1,0:T(8,128)(2,1)S(1)}, bf16[128,128]{1,0:T(8,128)(2,1)S(1)}, u32[]{:S(2)}, u32[]{:S(2)}) %collective-permute-start) | collective-permute-done | bytes 32800 | tf_op jit(solution)/shard_map/ppermute | solution.py:191
  44.9 0.0 copy-done
  44.9 3.2 %attend.1 = (bf16[256,2048]{1,0:T(8,128)(2,1)S(1)}, bf16[256,256]{1,0:T(8,128)(2,1)S(1)}) custom-call(s32[3]{0:T(128)S(1)} %pad_add_fusion.place_ref, f32[4]{0:T(128)S(1)} %copy-done.4, bf16[512,256]{1,0:T(8,128)(2,1)S(1)} %copy-done.3, bf16[128,128]{1,0:T(8,128)(2,1)S(1)} %collective-permute-done.low_ref, bf16[128,512]{1,0:T(8,128)(2,1)S(1)} %pad_maximum_fusion.mid_ref, ...), custom_call_target="tpu_custom_call" | custom-call | flops 738197504 | bytes 4194304 | tf_op jit(solution)/shard_map/attend/pallas_call | solution.py:294
  48.2 3.8 %collective-permute-start.2 = (bf16[256,2048]{1,0:T(8,128)(2,1)S(1)}, bf16[256,2048]{1,0:T(8,128)(2,1)S(1)}, u32[]{:S(2)}, u32[]{:S(2)}) collective-permute-start(bf16[256,2048]{1,0:T(8,128)(2,1)S(1)} %get-tuple-element.19), channel_id=1, source_target_pairs={{0,1},{1,0},{2,3},{3,2},{4,5},{5,4},{6,7},{7,6},{8,9},{9,8},{10,11... | collective-permute-start | bytes 3145736 | tf_op jit(solution)/shard_map/ppermute | solution.py:395
  52.0 2.3 %collective-permute-done.2 = bf16[256,2048]{1,0:T(8,128)(2,1)S(1)} collective-permute-done((bf16[256,2048]{1,0:T(8,128)(2,1)S(1)}, bf16[256,2048]{1,0:T(8,128)(2,1)S(1)}, u32[]{:S(2)}, u32[]{:S(2)}) %collective-permute-start.2) | collective-permute-done | bytes 1048608 | tf_op jit(solution)/shard_map/ppermute | solution.py:395
  54.2 0.0 copy-start.1
  54.2 0.0 copy-start.2
  54.3 0.5 fusion
  54.7 19.7 %all_to_all.21.pieces_ref = bf16[4,64,2048]{2,1,0:T(8,128)(2,1)S(1)} all-to-all(bf16[4,64,2048]{2,1,0:T(8,128)(2,1)S(1)} %bitcast.16), channel_id=1, replica_groups={{0,2,4,6},{1,3,5,7},{8,10,12,14},{9,11,13,15},{16,18,20,22},{17,19,21,2..., dimensions={0} | all-to-all | bytes 2097152 | tf_op jit(solution)/shard_map/all_to_all | solution.py:398
  74.4 0.0 copy-done.1
  74.4 0.0 copy-done.2
  74.4 0.3 norm.1
  74.8 17.2 %all_to_all.22 = bf16[4,64,2048]{2,1,0:T(8,128)(2,1)S(1)} all-to-all(bf16[4,64,2048]{2,1,0:T(8,128)(2,1)S(1)} %get-tuple-element.20), channel_id=1, replica_groups={{0,2,4,6},{1,3,5,7},{8,10,12,14},{9,11,13,15},{16,18,20,22},{17,19,21,2..., dimensions={0} | all-to-all | bytes 2097152 | tf_op jit(solution)/shard_map/all_to_all | solution.py:398
  92.0 1.9 %collective-permute-start.3 = (bf16[256,2048]{1,0:T(8,128)(2,1)S(1)}, bf16[256,2048]{1,0:T(8,128)(2,1)S(1)}, u32[]{:S(2)}, u32[]{:S(2)}) collective-permute-start(bf16[256,2048]{1,0:T(8,128)(2,1)S(1)} %bitcast.12), channel_id=1, source_target_pairs={{0,1},{1,0},{2,3},{3,2},{4,5},{5,4},{6,7},{7,6},{8,9},{9,8},{10,11... | collective-permute-start | bytes 3145736 | tf_op jit(solution)/shard_map/ppermute | solution.py:395
  93.9 2.6 %collective-permute-done.3.rows_ref = bf16[256,2048]{1,0:T(8,128)(2,1)S(1)} collective-permute-done((bf16[256,2048]{1,0:T(8,128)(2,1)S(1)}, bf16[256,2048]{1,0:T(8,128)(2,1)S(1)}, u32[]{:S(2)}, u32[]{:S(2)}) %collective-permute-start.3) | collective-permute-done | bytes 1048608 | tf_op jit(solution)/shard_map/ppermute | solution.py:395
  96.5 0.0 all-gather.3.cloned.1.call-done
  96.5 4.9 %ffn_first.1 = (bf16[256,2048]{1,0:T(8,128)(2,1)S(1)}, bf16[8,8,528,128]{3,2,1,0:T(8,128)(2,1)S(1)}) custom-call(s32[1]{0:T(128)} %bitcast.core_ref, bf16[256,2048]{1,0:T(8,128)(2,1)S(1)} %collective-permute-done.3.rows_ref, bf16[8,8,528,128]{3,2,1,0:T(8,128)(2,1)} %bitcast.15), custom_call_target="tpu_custom_call" | custom-call | flops 2214592512 | bytes 10747904 | tf_op jit(solution)/shard_map/ffn_first/pallas_call | solution.py:152
  101.5 2.0 %collective-permute-start.4 = (bf16[256,2048]{1,0:T(8,128)(2,1)S(1)}, bf16[256,2048]{1,0:T(8,128)(2,1)S(1)}, u32[]{:S(2)}, u32[]{:S(2)}) collective-permute-start(bf16[256,2048]{1,0:T(8,128)(2,1)S(1)} %get-tuple-element.23), channel_id=1, source_target_pairs={{0,1},{1,0},{2,3},{3,2},{4,5},{5,4},{6,7},{7,6},{8,9},{9,8},{10,11... | collective-permute-start | bytes 3145736 | tf_op jit(solution)/shard_map/ppermute | solution.py:395
  103.5 2.7 %ffn_second.1 = f32[256,2048]{1,0:T(8,128)S(1)} custom-call(bf16[256,2048]{1,0:T(8,128)(2,1)S(1)} %bitcast.13, bf16[8,8,528,128]{3,2,1,0:T(8,128)(2,1)S(1)} %get-tuple-element.22.held), custom_call_target="tpu_custom_call" | custom-call | flops 2214592512 | bytes 10747904 | tf_op jit(solution)/shard_map/ffn_second/pallas_call | solution.py:176
  106.3 0.0 collective-permute-done.4
  106.3 0.3 add_convert_fusion
  106.6 18.3 %all_to_all.23.pieces_ref = bf16[4,64,2048]{2,1,0:T(8,128)(2,1)S(1)} all-to-all(bf16[4,64,2048]{2,1,0:T(8,128)(2,1)S(1)} %bitcast.17), channel_id=1, replica_groups={{0,2,4,6},{1,3,5,7},{8,10,12,14},{9,11,13,15},{16,18,20,22},{17,19,21,2..., dimensions={0} | all-to-all | bytes 2097152 | tf_op jit(solution)/shard_map/all_to_all | solution.py:398
  124.9 0.8 last.1
  (2 shorter events, 0.0 us)
Async XLA Ops:
  6.5 90.0 %all-gather.3.cloned.1.call-start = ((), (), s32[]{:S(2)}) async-start(), calls=%async_computation.4 | async-start | bytes 9732096 | tf_op jit(solution)/shard_map/all_gather | solution.py:384
  7.5 26.7 %copy-start.5 = (bf16[512,64]{0,1:T(8,128)(2,1)S(1)}, bf16[512,64]{0,1:T(8,128)(2,1)}, u32[]{:S(2)}) copy-start(bf16[512,64]{0,1:T(8,128)(2,1)} %param.11) | copy-start | bytes 196612
  7.5 26.7 %copy-start.6 = (bf16[512,64]{0,1:T(8,128)(2,1)S(1)}, bf16[512,64]{0,1:T(8,128)(2,1)}, u32[]{:S(2)}) copy-start(bf16[512,64]{0,1:T(8,128)(2,1)} %param.12) | copy-start | bytes 196612
  7.7 32.4 %copy-start.3 = (bf16[512,256]{1,0:T(8,128)(2,1)S(1)}, bf16[512,256]{1,0:T(8,128)(2,1)}, u32[]{:S(2)}) copy-start(bf16[512,256]{1,0:T(8,128)(2,1)} %query_ref.1) | copy-start | bytes 786436
  7.7 32.4 %copy-start.4 = (f32[4]{0:T(128)S(1)}, f32[4]{0:T(128)}, u32[]{:S(2)}) copy-start(f32[4]{0:T(128)} %sink_ref.3) | copy-start | bytes 52
  7.7 37.3 %copy-start = (bf16[256,2048]{1,0:T(8,128)(2,1)S(1)}, bf16[256,2048]{1,0:T(8,128)(2,1)}, u32[]{:S(2)}) copy-start(bf16[256,2048]{1,0:T(8,128)(2,1)} %proj_ref.1) | copy-start | bytes 3145732
  34.2 8.8 %collective-permute-start.1 = (bf16[128,128]{1,0:T(8,128)(2,1)S(1)}, bf16[128,128]{1,0:T(8,128)(2,1)S(1)}, u32[]{:S(2)}, u32[]{:S(2)}) collective-permute-start(bf16[128,128]{1,0:T(8,128)(2,1)S(1)} %get-tuple-element.25), channel_id=1, source_target_pairs={{8,0},{16,8},{24,16},{32,24},{40,32},{48,40},{56,48},{64,56},{72,6... | collective-permute-start | bytes 98312 | tf_op jit(solution)/shard_map/ppermute | solution.py:192
  37.0 7.9 %collective-permute-start = (bf16[128,128]{1,0:T(8,128)(2,1)S(1)}, bf16[128,128]{1,0:T(8,128)(2,1)S(1)}, u32[]{:S(2)}, u32[]{:S(2)}) collective-permute-start(bf16[128,128]{1,0:T(8,128)(2,1)S(1)} %get-tuple-element.26), channel_id=1, source_target_pairs={{0,8},{8,16},{16,24},{24,32},{32,40},{40,48},{48,56},{56,64},{64,7... | collective-permute-start | bytes 98312 | tf_op jit(solution)/shard_map/ppermute | solution.py:191
  48.2 6.1 %collective-permute-start.2 = (bf16[256,2048]{1,0:T(8,128)(2,1)S(1)}, bf16[256,2048]{1,0:T(8,128)(2,1)S(1)}, u32[]{:S(2)}, u32[]{:S(2)}) collective-permute-start(bf16[256,2048]{1,0:T(8,128)(2,1)S(1)} %get-tuple-element.19), channel_id=1, source_target_pairs={{0,1},{1,0},{2,3},{3,2},{4,5},{5,4},{6,7},{7,6},{8,9},{9,8},{10,11... | collective-permute-start | bytes 3145736 | tf_op jit(solution)/shard_map/ppermute | solution.py:395
  54.2 20.2 %copy-start.1 = (bf16[64,2048]{1,0:T(8,128)(2,1)S(1)}, bf16[64,2048]{1,0:T(8,128)(2,1)}, u32[]{:S(2)}) copy-start(bf16[64,2048]{1,0:T(8,128)(2,1)} %residual_ref.1) | copy-start | bytes 786436
  54.2 20.2 %copy-start.2 = (f32[2048]{0:T(1024)S(1)}, f32[2048]{0:T(1024)}, u32[]{:S(2)}) copy-start(f32[2048]{0:T(1024)} %param.16) | copy-start | bytes 24580
  92.0 4.5 %collective-permute-start.3 = (bf16[256,2048]{1,0:T(8,128)(2,1)S(1)}, bf16[256,2048]{1,0:T(8,128)(2,1)S(1)}, u32[]{:S(2)}, u32[]{:S(2)}) collective-permute-start(bf16[256,2048]{1,0:T(8,128)(2,1)S(1)} %bitcast.12), channel_id=1, source_target_pairs={{0,1},{1,0},{2,3},{3,2},{4,5},{5,4},{6,7},{7,6},{8,9},{9,8},{10,11... | collective-permute-start | bytes 3145736 | tf_op jit(solution)/shard_map/ppermute | solution.py:395
  101.5 4.8 %collective-permute-start.4 = (bf16[256,2048]{1,0:T(8,128)(2,1)S(1)}, bf16[256,2048]{1,0:T(8,128)(2,1)S(1)}, u32[]{:S(2)}, u32[]{:S(2)}) collective-permute-start(bf16[256,2048]{1,0:T(8,128)(2,1)S(1)} %get-tuple-element.23), channel_id=1, source_target_pairs={{0,1},{1,0},{2,3},{3,2},{4,5},{5,4},{6,7},{7,6},{8,9},{9,8},{10,11... | collective-permute-start | bytes 3145736 | tf_op jit(solution)/shard_map/ppermute | solution.py:395
Sparse Core Ops, SparseCore 0:
  34.2 56.3 all-gather.2
